TPU v7x, 1024 devices: a whole 4x4x32 slice. The times are simulated.
1024 devices in a mesh: rep: 4 (over z_hi), fs: 32 (over z_lo, y), tp: 8 (over x, core).
Axes of the slice: x: 4, y: 4, z: 32 (z_hi: 4, z_lo: 8; z = z_hi * 8 + z_lo), core: 2. Of those that a mesh axis runs over, the one named last changes fastest.
Arguments:
- tokens: bfloat16 [65536, 2048], P(('rep', 'fs')), may hold values from -6 to 6
- mix_gain: float32 [2048], replicated, may hold values from 0.1 to 1.9
- w_gate_b: bfloat16 [2048, 1024], P('fs', 'tp'), may hold values from -0.125 to 0.125
- w_gate_c: bfloat16 [2048, 1024], P('fs', 'tp'), may hold values from -0.125 to 0.125
- w_conv_in: bfloat16 [2048, 1024], P('fs', 'tp'), may hold values from -0.125 to 0.125
- conv_taps: float32 [3, 1024], P(None, 'tp'), may hold values from -3 to 3
- w_mix_out: bfloat16 [1024, 2048], P('tp', 'fs'), may hold values from -0.1875 to 0.1875
- ffn_gain: float32 [2048], replicated, may hold values from 0.1 to 1.9
- w_ffn_gate: bfloat16 [2048, 2816], P('fs', 'tp'), may hold values from -0.125 to 0.125
- w_ffn_up: bfloat16 [2048, 2816], P('fs', 'tp'), may hold values from -0.125 to 0.125
- w_ffn_down: bfloat16 [2816, 2048], P('tp', 'fs'), may hold values from -0.109375 to 0.109375
Outputs:
- layer_out: bfloat16 [65536, 2048], P(('rep', 'fs', 'tp'))
All inputs are finite; a program needn't handle non-finite values.
Results may differ from a plain program's by a relative error of at most 0.014.
Values may be sent and summed in bfloat16 or wider, within the bound.
No kernel may reach another device: no remote copies, remote signals or barrier semaphores. Data moves between devices by JAX's collectives and lax.ppermute only.
A program may use at most 32 MiB of HBM per device.

v0:
```python
import jax
import jax.numpy as jnp
from jax import lax
from jax.sharding import PartitionSpec as P

LEN = 128


EPSILON = 1e-06


def side_by_side(arrays, axis, dim, along):
    widths = [a.shape[along] for a in arrays]
    both = jnp.concatenate(arrays, axis=along)
    out = lax.all_gather(both, axis, axis=dim, tiled=True)
    return tuple(jnp.split(out, [sum(widths[:k]) for k in range(1, len(widths))], axis=along))


def from_everyone(array, axis):
    peers = lax.axis_size(axis)
    return lax.all_to_all(
        jnp.broadcast_to(array[None], (peers, *array.shape)), axis, 0, 0, tiled=True
    )


def in_order(blocks, dim):
    blocks = jnp.moveaxis(blocks, 0, dim)
    lengths = blocks.shape
    return blocks.reshape(*lengths[:dim], lengths[dim] * lengths[dim + 1], *lengths[dim + 2 :])


def collect(array, axis, dim):
    blocks = from_everyone(array, axis)
    return in_order(blocks, dim)


def cut_along(array, dim, peers):
    before, after = (array.shape[:dim], array.shape[dim + 1 :])
    return jnp.moveaxis(array.reshape(*before, peers, -1, *after), dim, 0)


def sent_and_summed(array, axis, dim):
    peers = lax.axis_size(axis)
    blocks = lax.all_to_all(cut_along(array, dim, peers), axis, 0, 0, tiled=True)
    return jnp.sum(blocks.astype(jnp.float32), axis=0)


def rms_scale(values, gain):
    return values * lax.rsqrt(jnp.mean(values * values, axis=-1, keepdims=True) + EPSILON) * gain


def causal_mix(product_in, conv_taps):
    shaped = product_in.reshape(product_in.shape[0] // LEN, LEN, product_in.shape[1])
    padded = jnp.pad(shaped, ((0, 0), (2, 0), (0, 0)))
    convolved = (
        conv_taps[0] * padded[:, :-2]
        + conv_taps[1] * padded[:, 1:-1]
        + conv_taps[2] * padded[:, 2:]
    )
    return convolved.reshape(product_in.shape)


def local(
    tokens,
    mix_gain,
    w_gate_b,
    w_gate_c,
    w_conv_in,
    conv_taps,
    w_mix_out,
    ffn_gain,
    w_ffn_gate,
    w_ffn_up,
    w_ffn_down,
):
    normed = rms_scale(tokens.astype(jnp.float32), mix_gain).astype(jnp.bfloat16)
    shard_rows = side_by_side((w_gate_b, w_gate_c, w_conv_in), "fs", 0, 1)
    gate_b, gate_c, conv_in = tuple(
        (jnp.dot(normed, weight, preferred_element_type=jnp.float32) for weight in shard_rows)
    )
    gated = (gate_b * causal_mix(gate_c * conv_in, conv_taps)).astype(jnp.bfloat16)
    mix_columns = collect(w_mix_out, "fs", 1)
    row_count = normed.shape[0] // lax.axis_size("tp")
    branch = sent_and_summed(
        jnp.dot(gated, mix_columns, preferred_element_type=jnp.float32).astype(jnp.bfloat16),
        "tp",
        0,
    )
    own_rows = lax.dynamic_slice_in_dim(tokens, lax.axis_index("tp") * row_count, row_count, 0)
    stream = own_rows.astype(jnp.float32) + branch
    normed_two = rms_scale(stream, ffn_gain).astype(jnp.bfloat16)
    gate_rows, up_rows = side_by_side((w_ffn_gate, w_ffn_up), "fs", 0, 1)
    shard_rows = collect(normed_two, "tp", 0)
    gate_part = jnp.dot(shard_rows, gate_rows, preferred_element_type=jnp.float32)
    up_part = jnp.dot(shard_rows, up_rows, preferred_element_type=jnp.float32)
    hidden = (jax.nn.silu(gate_part) * up_part).astype(jnp.bfloat16)
    down_columns = collect(w_ffn_down, "fs", 1)
    ffn_branch = sent_and_summed(
        jnp.dot(hidden, down_columns, preferred_element_type=jnp.float32).astype(jnp.bfloat16),
        "tp",
        0,
    )
    return (stream + ffn_branch).astype(jnp.bfloat16)


def solution(mesh):
    in_specs = (
        P(("rep", "fs"), None),
        P(),
        P("fs", "tp"),
        P("fs", "tp"),
        P("fs", "tp"),
        P(None, "tp"),
        P("tp", "fs"),
        P(),
        P("fs", "tp"),
        P("fs", "tp"),
        P("tp", "fs"),
    )
    out_specs = P(("rep", "fs", "tp"), None)
    return jax.shard_map(local, mesh=mesh, in_specs=in_specs, out_specs=out_specs, check_vma=False)
```

profile of v0, /device:TPU:1, one launch (start us, length us, event | category | flops | bytes accessed | tf_op | source)
XLA Modules:
  0.0 634.1 jit_solution(6646735307539935185)
XLA Ops:
  6.5 1.6 broadcast_in_dim.6
  8.2 16.1 %all-to-all-start = ((bf16[32,128,64]{1,2,0:T(8,128)(2,1)}), bf16[32,128,64]{1,2,0:T(8,128)(2,1)S(1)}, u32[]{:S(2)}, u32[]{:S(2)}) async-start(bf16[32,128,64]{1,2,0:T(8,128)(2,1)} %broadcast_in_dim.6), calls=%async_computation | async-start | bytes 1048576 | tf_op jit(solution)/shard_map/all_to_all | solution.py:21
  24.3 1.4 pad_maximum_fusion.1
  25.7 0.9 slice_bitcast_fusion.2
  26.6 2.1 fusion
  28.7 0.5 fusion.2
  29.3 211.1 %all-gather.3.cloned.1.call-done = bf16[2048,384]{1,0:T(8,128)(2,1)} async-done(((bf16[64,384]{1,0:T(8,128)(2,1)}), bf16[2048,384]{1,0:T(8,128)(2,1)}) %all-gather.3.cloned.1.call-update) | async-done | bytes 1572880 | tf_op jit(solution)/shard_map/all_gather | solution.py:15
  240.4 1.8 fusion.22
  242.1 1.8 convolution_multiply_fusion
  244.0 4.7 convolution_convert_fusion
  248.7 28.0 %all-to-all-start.1 = ((bf16[8,64,2048]{2,1,0:T(8,128)(2,1)}), bf16[8,64,2048]{2,1,0:T(8,128)(2,1)S(1)}, u32[]{:S(2)}, u32[]{:S(2)}) async-start(bf16[8,64,2048]{2,1,0:T(8,128)(2,1)} %bitcast.24), calls=%async_computation.1 | async-start | bytes 4194304 | tf_op jit(solution)/shard_map/all_to_all | solution.py:44
  276.7 26.2 %all-to-all-done.1 = bf16[8,64,2048]{2,1,0:T(8,128)(2,1)S(1)} async-done(((bf16[8,64,2048]{2,1,0:T(8,128)(2,1)}), bf16[8,64,2048]{2,1,0:T(8,128)(2,1)S(1)}, u32[]{:S(2)}, u32[]{:S(2)}) %all-to-all-start.1) | async-done | bytes 2097184 | tf_op jit(solution)/shard_map/all_to_all | solution.py:44
  303.3 1.1 multiply_reduce_fusion
  304.4 1.1 multiply_convert_fusion
  305.8 29.7 %all_to_all.25 = bf16[8,64,2048]{2,1,0:T(8,128)(2,1)S(1)} all-to-all(bf16[8,64,2048]{2,1,0:T(8,128)(2,1)S(1)} %broadcast_in_dim.7), channel_id=1, replica_groups=mesh['rep'=4,'fs'=32,'tp'=8] {'tp'}, dimensions={0} | all-to-all | bytes 4194304 | tf_op jit(solution)/shard_map/all_to_all | solution.py:21
  335.5 1.4 broadcast_in_dim.8
  336.9 10.9 %all-to-all-start.3 = ((bf16[32,352,64]{1,2,0:T(8,128)(2,1)}), bf16[32,352,64]{1,2,0:T(8,128)(2,1)}, u32[]{:S(2)}, u32[]{:S(2)}) async-start(bf16[32,352,64]{1,2,0:T(8,128)(2,1)} %broadcast_in_dim.8), calls=%async_computation.3 | async-start | bytes 3145728 | tf_op jit(solution)/shard_map/all_to_all | solution.py:21
  347.8 0.7 pad_maximum_fusion
  348.6 215.1 %all-gather.5.cloned.1.call-done = bf16[2048,704]{1,0:T(8,128)(2,1)} async-done(((bf16[64,704]{1,0:T(8,128)(2,1)}), bf16[2048,704]{1,0:T(8,128)(2,1)}) %all-gather.5.cloned.1.call-update) | async-done | bytes 2883600 | tf_op jit(solution)/shard_map/all_gather | solution.py:15
  563.6 2.4 fusion.5
  566.0 6.3 convolution_convert_fusion.1
  572.3 52.8 %all_to_all.26 = bf16[8,64,2048]{2,1,0:T(8,128)(2,1)S(1)} all-to-all(bf16[8,64,2048]{2,1,0:T(8,128)(2,1)} %bitcast.27), channel_id=1, replica_groups=mesh['rep'=4,'fs'=32,'tp'=8] {'tp'}, dimensions={0} | all-to-all | bytes 4194304 | tf_op jit(solution)/shard_map/all_to_all | solution.py:44
  625.2 0.4 convert_reduce_fusion
  625.5 1.8 add_convert_fusion
  (23 shorter events, 0.8 us)
Async XLA Ops:
  6.5 22.2 %copy-start.4 = (f32[2048]{0:T(1024)S(1)}, f32[2048]{0:T(1024)}, u32[]{:S(2)}) copy-start(f32[2048]{0:T(1024)} %param.12) | copy-start | bytes 24580
  8.2 235.8 %all-to-all-start = ((bf16[32,128,64]{1,2,0:T(8,128)(2,1)}), bf16[32,128,64]{1,2,0:T(8,128)(2,1)S(1)}, u32[]{:S(2)}, u32[]{:S(2)}) async-start(bf16[32,128,64]{1,2,0:T(8,128)(2,1)} %broadcast_in_dim.6), calls=%async_computation | async-start | bytes 1048576 | tf_op jit(solution)/shard_map/all_to_all | solution.py:21
  24.3 216.1 %all-gather.3.cloned.1.call-start = ((), (), s32[]{:S(2)}) async-start(), calls=%async_computation.5 | async-start | bytes 1622016 | tf_op jit(solution)/shard_map/all_gather | solution.py:15
  25.7 3.0 copy-start
  248.7 54.2 %all-to-all-start.1 = ((bf16[8,64,2048]{2,1,0:T(8,128)(2,1)}), bf16[8,64,2048]{2,1,0:T(8,128)(2,1)S(1)}, u32[]{:S(2)}, u32[]{:S(2)}) async-start(bf16[8,64,2048]{2,1,0:T(8,128)(2,1)} %bitcast.24), calls=%async_computation.1 | async-start | bytes 4194304 | tf_op jit(solution)/shard_map/all_to_all | solution.py:44
  276.7 27.7 %copy-start.5 = (f32[2048]{0:T(1024)S(1)}, f32[2048]{0:T(1024)}, u32[]{:S(2)}) copy-start(f32[2048]{0:T(1024)} %param.18) | copy-start | bytes 24580
  305.8 29.7 %copy-start.1 = (bf16[352,64]{0,1:T(8,128)(2,1)S(1)}, bf16[352,64]{0,1:T(8,128)(2,1)}, u32[]{:S(2)}) copy-start(bf16[352,64]{0,1:T(8,128)(2,1)} %param.21) | copy-start | bytes 135172
  335.5 12.3 %copy-start.2 = (bf16[64,352]{1,0:T(8,128)(2,1)S(1)}, bf16[64,352]{1,0:T(8,128)(2,1)}, u32[]{:S(2)}) copy-start(bf16[64,352]{1,0:T(8,128)(2,1)} %param.20) | copy-start | bytes 135172
  335.5 12.3 %copy-start.3 = (bf16[64,352]{1,0:T(8,128)(2,1)S(1)}, bf16[64,352]{1,0:T(8,128)(2,1)}, u32[]{:S(2)}) copy-start(bf16[64,352]{1,0:T(8,128)(2,1)} %param.19) | copy-start | bytes 135172
  336.9 229.1 %all-to-all-start.3 = ((bf16[32,352,64]{1,2,0:T(8,128)(2,1)}), bf16[32,352,64]{1,2,0:T(8,128)(2,1)}, u32[]{:S(2)}, u32[]{:S(2)}) async-start(bf16[32,352,64]{1,2,0:T(8,128)(2,1)} %broadcast_in_dim.8), calls=%async_computation.3 | async-start | bytes 3145728 | tf_op jit(solution)/shard_map/all_to_all | solution.py:21
  347.7 215.9 %all-gather.5.cloned.1.call-start = ((), (), s32[]{:S(2)}) async-start(), calls=%async_computation.6 | async-start | bytes 3244032 | tf_op jit(solution)/shard_map/all_gather | solution.py:15
Sparse Core Ops, SparseCore 0:
  27.7 212.5 all-gather.2
  351.2 212.3 all-gather.4
where the time goes:
time: 635 us; the launch traced here: 634 us
  waiting for transfers between devices  452 us (71%)
  blocking collectives  82.5 us (13%)
  starting transfers between devices  55 us (9%)
  matrix products  16.9 us (3%)
  between operations  13.6 us (2%)
  other arithmetic  9.49 us (1%)
    all_gather x2, waiting for transfers between devices, side_by_side(): out = lax.all_gather(both, axis, axis=dim, tiled=True)  426 us
    all_to_all x1, blocking collectives, sent_and_summed(): lax.all_to_all(cut_along(array, dim, peers), axis, 0, 0, tiled=True)  52.8 us
    all_to_all x1, blocking collectives, from_everyone(): lax.all_to_all(jnp.broadcast_to(array[None], (peers, *array.shape)), axis...  29.7 us
    all_to_all x1, starting transfers between devices, sent_and_summed(): lax.all_to_all(cut_along(array, dim, peers), axis, 0, 0, tiled=True)  28 us
    all_to_all x2, starting transfers between devices, from_everyone(): lax.all_to_all(jnp.broadcast_to(array[None], (peers, *array.shape)), axis...  26.9 us
    all_to_all x1, waiting for transfers between devices, sent_and_summed(): lax.all_to_all(cut_along(array, dim, peers), axis, 0, 0, tiled=True)  26.2 us
  transfers between devices with their start and end apart: 5, of which 3 were waited for; matrix products, arithmetic and copies ran while one was open for 2% of the time, Pallas kernels for 0%

commit v1 on v0

v1 whole, which is shorter than its diff:
```python
import jax
import jax.numpy as jnp
from jax import lax
from jax.experimental import pallas as pl
from jax.experimental.pallas import tpu as pltpu
from jax.sharding import Mesh, PartitionSpec as P

LEN = 128
EPSILON = 1e-06
Z_LO = 8
Z = ("rep", "zl")
SWAP = [(0, 1), (1, 0)]

VMEM = pl.BlockSpec(memory_space=pltpu.VMEM)
SMEM = pl.BlockSpec(memory_space=pltpu.SMEM)


def shift(value, axis, size, distance):
    return lax.ppermute(value, axis, [((k + distance) % size, k) for k in range(size)])


def exchange(blocks, axis):
    return lax.all_to_all(blocks, axis, 0, 0, tiled=True)


def copies(array, count):
    return jnp.broadcast_to(array[None], (count, *array.shape))


def rms_scale(values, gain):
    return values * lax.rsqrt(jnp.mean(values * values, axis=-1, keepdims=True) + EPSILON) * gain


def dot_t(acts, weight_t):
    return lax.dot_general(acts, weight_t, (((1,), (1,)), ((), ())), preferred_element_type=jnp.float32)


def dot(acts, weight):
    return jnp.dot(acts, weight, preferred_element_type=jnp.float32)


def call(kernel, outs, pos, args, mib, scratch=()):
    args = [pltpu.with_memory_space_constraint(a, pltpu.VMEM) for a in args]
    specs = [VMEM] * len(args)
    if pos is not None:
        args, specs = [pos, *args], [SMEM, *specs]
    return pl.pallas_call(
        kernel,
        out_shape=outs,
        in_specs=specs,
        out_specs=(VMEM,) * len(outs),
        scratch_shapes=scratch,
        compiler_params=pltpu.CompilerParams(vmem_limit_bytes=mib * 1024 * 1024),
    )(*args)


def mixer_kernel(places, n_y, pos, normed, taps, gathered, mine, other, weights, gated):
    zl, core = pos[0], pos[1]
    rows = gathered.shape[2]
    width = taps.shape[1]
    for k, d in enumerate(places):
        z = lax.rem(zl + (d + Z_LO), Z_LO)
        for y in range(n_y):
            first = pl.multiple_of((z * n_y + y) * rows, rows)
            weights[pl.ds(first, rows), :] = gathered[y, k]
    products = dot(normed[...], weights[:, : 3 * width])
    p = products[:, width : 2 * width] * products[:, 2 * width : 3 * width]
    place = lax.broadcasted_iota(jnp.int32, p.shape, 0) % LEN
    before = jnp.where(place >= 1, pltpu.roll(p, 1, 0), 0.0)
    before_two = jnp.where(place >= 2, pltpu.roll(p, 2, 0), 0.0)
    convolved = taps[0:1, :] * before_two + taps[1:2, :] * before + taps[2:3, :] * p
    gated[...] = (products[:, :width] * convolved).astype(jnp.bfloat16)
    out_t = weights[:, 3 * width :]
    n_x = mine.shape[0]
    step = mine.shape[1]
    for half, out in ((core, mine), (1 - core, other)):
        for x in range(n_x):
            first = pl.multiple_of(x * 2 * step + half * step, step)
            out[x] = dot_t(gated[pl.ds(first, step), :], out_t).astype(jnp.bfloat16)


def tick_kernel(pos, out):
    for k in range(pos.shape[0]):
        out[k] = pos[k]


def tick(pos):
    return pl.pallas_call(
        tick_kernel,
        out_shape=jax.ShapeDtypeStruct(pos.shape, pos.dtype),
        in_specs=[SMEM],
        out_specs=SMEM,
        compiler_params=pltpu.CompilerParams(vmem_limit_bytes=1024 * 1024),
    )(pos)


def join_kernel(blocks, own, gain, stream, sent):
    total = own[...].astype(jnp.float32)
    for k in range(blocks.shape[0]):
        total += blocks[k].astype(jnp.float32)
    stream[...] = total
    normed = rms_scale(total, gain[...]).astype(jnp.bfloat16)
    for k in range(sent.shape[0]):
        sent[k] = normed


def last_kernel(blocks, stream, out):
    total = stream[...]
    for k in range(blocks.shape[0]):
        total += blocks[k].astype(jnp.float32)
    out[...] = total.astype(jnp.bfloat16)


def ffn_kernel(places, n_ff, down_at, pos, acts, *refs):
    chunks, out = refs[: len(places)], refs[len(places)]
    depth = acts.shape[1] // Z_LO
    both = None
    firsts = []
    for (d, row), chunk in zip(places, chunks):
        z = lax.rem(pos[0] + (d + Z_LO), Z_LO)
        first = pl.multiple_of(z * depth + row, chunk.shape[0])
        firsts.append(first)
        part = dot(acts[:, pl.ds(first, chunk.shape[0])], chunk[:, : 2 * n_ff])
        both = part if both is None else both + part
    hidden = (jax.nn.silu(both[:, :n_ff]) * both[:, n_ff:]).astype(jnp.bfloat16)
    for first, chunk in zip(firsts, chunks):
        part = dot_t(hidden, chunk[:, down_at : down_at + n_ff])
        out[:, pl.ds(first, chunk.shape[0])] = part.astype(jnp.bfloat16)


def local(
    tokens,
    mix_gain,
    w_gate_b,
    w_gate_c,
    w_conv_in,
    conv_taps,
    w_mix_out,
    ffn_gain,
    w_ffn_gate,
    w_ffn_up,
    w_ffn_down,
):
    nx, ny = lax.axis_size("x"), lax.axis_size("y")
    nz = lax.axis_size("rep") * lax.axis_size("zl")
    zl, core = lax.axis_index("zl"), lax.axis_index("core")
    pos = jnp.stack([zl, core]).astype(jnp.int32)
    count, feats = tokens.shape
    half_rows = count // 2
    own_rows = half_rows // nx

    mixer = jnp.concatenate([w_gate_b, w_gate_c, w_conv_in, w_mix_out.T], axis=1)
    places = [0, 4, 3, -3, 2, -2, 1, -1]
    held = [mixer] + [shift(mixer, Z, nz, d) for k, d in enumerate(places) if k]

    n_ff = w_ffn_gate.shape[1]
    down_at = -(-2 * n_ff // 128) * 128
    width = -(-(down_at + n_ff) // 128) * 128
    ffn = jnp.concatenate([w_ffn_gate, w_ffn_up], axis=1)
    ffn = jnp.concatenate(
        [jnp.pad(ffn, ((0, 0), (0, down_at - 2 * n_ff))), jnp.pad(w_ffn_down.T, ((0, 0), (0, width - down_at - n_ff)))],
        axis=1,
    )
    ffn_y = exchange(copies(ffn, ny), "y").reshape(-1, width)
    chunks, ffn_places = [ffn_y], [(0, 0)]
    up = down = ffn_y
    for k in (1, 2, 3):
        up, down = shift(up, Z, nz, 1), shift(down, Z, nz, -1)
        chunks += [up, down]
        ffn_places += [(k, 0), (-k, 0)]
    cut = ffn_y.shape[0] // 2
    chunks += [shift(up[:cut], Z, nz, 1), shift(down[cut:], Z, nz, -1)]
    ffn_places += [(4, 0), (4, cut)]

    normed = rms_scale(tokens.astype(jnp.float32), mix_gain).astype(jnp.bfloat16)
    own = lax.dynamic_slice_in_dim(tokens, (lax.axis_index("x") * 2 + core) * own_rows, own_rows, 0)
    held, normed, own = lax.optimization_barrier((jnp.stack(held), normed, own))
    gathered = exchange(copies(held, ny), "y").reshape(ny, Z_LO, *mixer.shape)

    bf, f32 = jnp.bfloat16, jnp.float32
    halves = (nx, own_rows, feats)

    def mixer_body(*refs):
        mixer_kernel(places, ny, *refs)

    pos = tick(tick(pos))
    scratch = [pltpu.VMEM((feats, mixer.shape[1]), bf), pltpu.VMEM((count, w_gate_b.shape[1]), bf)]
    mine, other = call(mixer_body, (pltpu.VMEM(halves, bf),) * 2, pos, (normed, conv_taps, gathered), 16, scratch)

    def over_tp(mine, other):
        got = lax.ppermute(other, "core", SWAP)
        pair = (mine.astype(f32) + got.astype(f32)).astype(bf)
        return exchange(pair, "x")

    pos = tick(pos)
    blocks = over_tp(mine, other)
    stream, sent = call(
        join_kernel,
        (pltpu.VMEM((own_rows, feats), f32), jax.ShapeDtypeStruct(halves, bf)),
        None,
        (blocks, own, ffn_gain.reshape(1, -1)),
        8,
    )
    pos = tick(pos)
    acts = exchange(sent, "x").reshape(half_rows, feats)
    acts_other = lax.ppermute(acts, "core", SWAP)

    def ffn_body(*refs):
        ffn_kernel(ffn_places, n_ff, down_at, *refs)

    def feed_forward(values):
        (out,) = call(ffn_body, (pltpu.VMEM((half_rows, feats), bf),), pos, (values, *chunks), 12)
        return out.reshape(nx, own_rows, feats)

    ffn_mine = feed_forward(acts)
    acts_other, ffn_mine = lax.optimization_barrier((acts_other, ffn_mine))
    blocks = over_tp(ffn_mine, feed_forward(acts_other))
    return call(last_kernel, (jax.ShapeDtypeStruct((own_rows, feats), bf),), None, (blocks, stream), 8)[0]


def solution(mesh):
    fine = Mesh(
        mesh.devices.reshape(mesh.shape["rep"], Z_LO, mesh.shape["fs"] // Z_LO, mesh.shape["tp"] // 2, 2),
        ("rep", "zl", "y", "x", "core"),
    )
    fs, tp = ("zl", "y"), ("x", "core")
    in_specs = (
        P(("rep", *fs), None),
        P(),
        P(fs, tp),
        P(fs, tp),
        P(fs, tp),
        P(None, tp),
        P(tp, fs),
        P(),
        P(fs, tp),
        P(fs, tp),
        P(tp, fs),
    )
    out_specs = P(("rep", *fs, *tp), None)
    return jax.shard_map(local, mesh=fine, in_specs=in_specs, out_specs=out_specs, check_vma=False)
```

time: 635 us -> 213 us (0.34)
  waiting for transfers between devices: 452 us -> 68.2 us
  blocking collectives: 82.5 us -> 17.2 us
  starting transfers between devices: 55 us -> 94.7 us
  Pallas kernels: 0 us -> 18.3 us
  matrix products: 16.9 us -> 0 us
  between operations: 13.6 us -> 0.58 us
    all_gather x2 -> x0, waiting for transfers between devices: 426 us -> none  [side_by_side(): out = lax.all_gather(both, axis, axis=dim, tiled=True)]
    ppermute x0 -> x18, starting transfers between devices: none -> 79.1 us  [the longest x15 63.1 us: shift(): lax.ppermute(value, axis, [((k + distance) % size, k) for k in range(size)])]
    all_to_all x2 -> x1, blocking collectives: 82.5 us -> 17.2 us  [exchange(): return lax.all_to_all(blocks, axis, 0, 0, tiled=True)]
    all_to_all x3 -> x4, starting transfers between devices: 55 us -> 15.6 us  [exchange(): return lax.all_to_all(blocks, axis, 0, 0, tiled=True)]
    ppermute x0 -> x18, waiting for transfers between devices: none -> 22.2 us  [the longest x15 19.9 us: shift(): lax.ppermute(value, axis, [((k + distance) % size, k) for k in range(size)])]
    all_to_all x3 -> x4, waiting for transfers between devices: 26.2 us -> 46 us  [exchange(): return lax.all_to_all(blocks, axis, 0, 0, tiled=True)]
    pallas_call x0 -> x9, Pallas kernels: none -> 18.3 us  [the longest x5 13.8 us: call(): pl.pallas_call(kernel, out_shape=outs, in_specs=specs, out_specs=(VMEM,)...]
    dot_general x5 -> x0, matrix products: 16.9 us -> none  [the longest x1 6.32 us: local(): jnp.dot(hidden, down_columns, preferred_element_type=jnp.float32)]
  transfers between devices with their start and end apart: 5 -> 22, of which waited for: 3 -> 9; matrix products, arithmetic and copies ran while one was open for 2% -> 4% of each run, Pallas kernels for 0% -> 4%
where the time goes in v1:
time: 213 us; the launch traced here: 211 us
  starting transfers between devices  94.7 us (44%)
  waiting for transfers between devices  68.2 us (32%)
  Pallas kernels  18.3 us (9%)
  blocking collectives  17.2 us (8%)
  other arithmetic  6.96 us (3%)
  local copies, waits for them, and re-layouts  5.33 us (3%)
    ppermute x15, starting transfers between devices, shift(): lax.ppermute(value, axis, [((k + distance) % size, k) for k in range(size)])  63.1 us
    all_to_all x4, waiting for transfers between devices, exchange(): return lax.all_to_all(blocks, axis, 0, 0, tiled=True)  46 us
    ppermute x15, waiting for transfers between devices, shift(): lax.ppermute(value, axis, [((k + distance) % size, k) for k in range(size)])  19.9 us
    all_to_all x1, blocking collectives, exchange(): return lax.all_to_all(blocks, axis, 0, 0, tiled=True)  17.2 us
    all_to_all x4, starting transfers between devices, exchange(): return lax.all_to_all(blocks, axis, 0, 0, tiled=True)  15.6 us
    pallas_call x5, Pallas kernels, call(): pl.pallas_call(kernel, out_shape=outs, in_specs=specs, out_specs=(VMEM,)...  13.8 us
    ppermute x2, starting transfers between devices, over_tp(): got = lax.ppermute(other, 'core', SWAP)  11.3 us
    ppermute x1, starting transfers between devices, local(): acts_other = lax.ppermute(acts, 'core', SWAP)  4.76 us
  transfers between devices with their start and end apart: 22, of which 9 were waited for; matrix products, arithmetic and copies ran while one was open for 4% of the time, Pallas kernels for 4%

profile of v1, /device:TPU:1, one launch (start us, length us, event | category | flops | bytes accessed | tf_op | source)
XLA Modules:
  0.0 211.3 jit_solution(6919151176999453341)
XLA Ops:
  0.8 20.5 %collective-permute-start = (bf16[64,512]{1,0:T(8,128)(2,1)S(1)}, bf16[64,512]{1,0:T(8,128)(2,1)S(1)}, u32[]{:S(2)}, u32[]{:S(2)}) collective-permute-start(bf16[64,512]{1,0:T(8,128)(2,1)S(1)} %pad_maximum_fusion), channel_id=1, source_target_pairs={{128,0},{160,32},{192,64},{224,96},{256,128},{288,160},{320,192},{... | collective-permute-start | bytes 196616 | tf_op jit(solution)/shard_map/ppermute | solution.py:19
  21.4 4.7 %collective-permute-start.1 = (bf16[64,512]{1,0:T(8,128)(2,1)S(1)}, bf16[64,512]{1,0:T(8,128)(2,1)S(1)}, u32[]{:S(2)}, u32[]{:S(2)}) collective-permute-start(bf16[64,512]{1,0:T(8,128)(2,1)S(1)} %pad_maximum_fusion), channel_id=1, source_target_pairs={{96,0},{128,32},{160,64},{192,96},{224,128},{256,160},{288,192},{3... | collective-permute-start | bytes 196616 | tf_op jit(solution)/shard_map/ppermute | solution.py:19
  28.4 5.5 %collective-permute-start.3 = (bf16[64,512]{1,0:T(8,128)(2,1)S(1)}, bf16[64,512]{1,0:T(8,128)(2,1)S(1)}, u32[]{:S(2)}, u32[]{:S(2)}) collective-permute-start(bf16[64,512]{1,0:T(8,128)(2,1)S(1)} %pad_maximum_fusion), channel_id=1, source_target_pairs={{64,0},{96,32},{128,64},{160,96},{192,128},{224,160},{256,192},{28... | collective-permute-start | bytes 196616 | tf_op jit(solution)/shard_map/ppermute | solution.py:19
  41.2 5.0 %collective-permute-start.5 = (bf16[64,512]{1,0:T(8,128)(2,1)S(1)}, bf16[64,512]{1,0:T(8,128)(2,1)S(1)}, u32[]{:S(2)}, u32[]{:S(2)}) collective-permute-start(bf16[64,512]{1,0:T(8,128)(2,1)S(1)} %pad_maximum_fusion), channel_id=1, source_target_pairs={{32,0},{64,32},{96,64},{128,96},{160,128},{192,160},{224,192},{256... | collective-permute-start | bytes 196616 | tf_op jit(solution)/shard_map/ppermute | solution.py:19
  48.3 4.2 %collective-permute-done.6 = bf16[64,512]{1,0:T(8,128)(2,1)S(1)} collective-permute-done((bf16[64,512]{1,0:T(8,128)(2,1)S(1)}, bf16[64,512]{1,0:T(8,128)(2,1)S(1)}, u32[]{:S(2)}, u32[]{:S(2)}) %collective-permute-start.6) | collective-permute-done | bytes 65568 | tf_op jit(solution)/shard_map/ppermute | solution.py:19
  54.1 4.6 %all-to-all-start = ((bf16[4,8,64,512]{3,2,1,0:T(8,128)(2,1)}), bf16[4,8,64,512]{3,2,1,0:T(8,128)(2,1)}, u32[]{:S(2)}, u32[]{:S(2)}) async-start(bf16[4,8,64,512]{3,2,1,0:T(8,128)(2,1)} %broadcast_in_dim.4), calls=%async_computation | async-start | bytes 4194304 | tf_op jit(solution)/shard_map/all_to_all | solution.py:23
  61.1 20.5 %all-to-all-done.refs_3_ = bf16[4,8,64,512]{3,2,1,0:T(8,128)(2,1)} async-done(((bf16[4,8,64,512]{3,2,1,0:T(8,128)(2,1)}), bf16[4,8,64,512]{3,2,1,0:T(8,128)(2,1)}, u32[]{:S(2)}, u32[]{:S(2)}) %all-to-all-start) | async-done | bytes 2097184 | tf_op jit(solution)/shard_map/all_to_all | solution.py:23
  81.6 5.5 %shard_map.111 = (bf16[4,64,2048]{2,1,0:T(8,128)(2,1)S(1)}, bf16[4,64,2048]{2,1,0:T(8,128)(2,1)}) custom-call(s32[2]{0:T(128)S(1)} %shard_map.110.refs_0_.pos, bf16[512,2048]{1,0:T(8,128)(2,1)S(1)} %fusion.2.refs_1_, f32[3,128]{1,0:T(4,128)S(1)} %copy-done.4, bf16[4,8,64,512]{3,2,1,0:T(8,128)(2,1)} %all-to-all-done.refs_3_), custom_call_target="tpu_custom_call" | custom-call | tf_op jit(solution)/shard_map/pallas_call | solution.py:47
  87.2 6.3 %collective-permute-start.7 = (bf16[4,64,2048]{2,1,0:T(8,128)(2,1)}, bf16[4,64,2048]{2,1,0:T(8,128)(2,1)S(1)}, u32[]{:S(2)}, u32[]{:S(2)}) collective-permute-start(bf16[4,64,2048]{2,1,0:T(8,128)(2,1)} %get-tuple-element.17), channel_id=1, source_target_pairs={{0,1},{1,0},{2,3},{3,2},{4,5},{5,4},{6,7},{7,6},{8,9},{9,8},{10,11... | collective-permute-start | bytes 3145736 | tf_op jit(solution)/shard_map/ppermute | solution.py:191
  94.5 3.5 %all-to-all-start.3 = ((bf16[4,64,1152]{2,1,0:T(8,128)(2,1)}), bf16[4,64,1152]{2,1,0:T(8,128)(2,1)S(1)}, u32[]{:S(2)}, u32[]{:S(2)}) async-start(bf16[4,64,1152]{2,1,0:T(8,128)(2,1)} %broadcast_in_dim.5), calls=%async_computation.3 | async-start | bytes 1179648 | tf_op jit(solution)/shard_map/all_to_all | solution.py:23
  99.4 8.8 %all-to-all-done.3 = bf16[4,64,1152]{2,1,0:T(8,128)(2,1)S(1)} async-done(((bf16[4,64,1152]{2,1,0:T(8,128)(2,1)}), bf16[4,64,1152]{2,1,0:T(8,128)(2,1)S(1)}, u32[]{:S(2)}, u32[]{:S(2)}) %all-to-all-start.3) | async-done | bytes 589856 | tf_op jit(solution)/shard_map/all_to_all | solution.py:23
  108.2 4.0 %all-to-all-start.1 = ((bf16[4,64,2048]{2,1,0:T(8,128)(2,1)}), bf16[4,64,2048]{2,1,0:T(8,128)(2,1)S(1)}, u32[]{:S(2)}, u32[]{:S(2)}) async-start(bf16[4,64,2048]{2,1,0:T(8,128)(2,1)} %add_convert_fusion.1), calls=%async_computation.1 | async-start | bytes 2097152 | tf_op jit(solution)/shard_map/all_to_all | solution.py:23
  114.1 3.4 %collective-permute-start.10 = (bf16[256,1152]{1,0:T(8,128)(2,1)S(1)}, bf16[256,1152]{1,0:T(8,128)(2,1)S(1)}, u32[]{:S(2)}, u32[]{:S(2)}) collective-permute-start(bf16[256,1152]{1,0:T(8,128)(2,1)S(1)} %bitcast.26), channel_id=1, source_target_pairs={{992,0},{0,32},{32,64},{64,96},{96,128},{128,160},{160,192},{192,2... | collective-permute-start | bytes 1769480 | tf_op jit(solution)/shard_map/ppermute | solution.py:19
  117.5 8.8 %all-to-all-done.1.blocks = bf16[4,64,2048]{2,1,0:T(8,128)(2,1)S(1)} async-done(((bf16[4,64,2048]{2,1,0:T(8,128)(2,1)}), bf16[4,64,2048]{2,1,0:T(8,128)(2,1)S(1)}, u32[]{:S(2)}, u32[]{:S(2)}) %all-to-all-start.1) | async-done | bytes 1048608 | tf_op jit(solution)/shard_map/all_to_all | solution.py:23
  128.4 3.5 %all-to-all-start.2 = ((bf16[4,64,2048]{2,1,0:T(8,128)(2,1)}), bf16[4,64,2048]{2,1,0:T(8,128)(2,1)S(1)}, u32[]{:S(2)}, u32[]{:S(2)}) async-start(bf16[4,64,2048]{2,1,0:T(8,128)(2,1)} %copy-done), calls=%async_computation.2 | async-start | bytes 2097152 | tf_op jit(solution)/shard_map/all_to_all | solution.py:23
  133.8 3.4 %collective-permute-start.12 = (bf16[256,1152]{1,0:T(8,128)(2,1)S(1)}, bf16[256,1152]{1,0:T(8,128)(2,1)}, u32[]{:S(2)}, u32[]{:S(2)}) collective-permute-start(bf16[256,1152]{1,0:T(8,128)(2,1)S(1)} %collective-permute-done.10.refs_4_), channel_id=1, source_target_pairs={{992,0},{0,32},{32,64},{64,96},{96,128},{128,160},{160,192},{192,2... | collective-permute-start | bytes 1769480 | tf_op jit(solution)/shard_map/ppermute | solution.py:19
  137.2 7.8 %all-to-all-done.2 = bf16[4,64,2048]{2,1,0:T(8,128)(2,1)S(1)} async-done(((bf16[4,64,2048]{2,1,0:T(8,128)(2,1)}), bf16[4,64,2048]{2,1,0:T(8,128)(2,1)S(1)}, u32[]{:S(2)}, u32[]{:S(2)}) %all-to-all-start.2) | async-done | bytes 1048608 | tf_op jit(solution)/shard_map/all_to_all | solution.py:23
  145.0 4.8 %collective-permute-start.8 = (bf16[256,2048]{1,0:T(8,128)(2,1)S(1)}, bf16[256,2048]{1,0:T(8,128)(2,1)S(1)}, u32[]{:S(2)}, u32[]{:S(2)}) collective-permute-start(bf16[256,2048]{1,0:T(8,128)(2,1)S(1)} %bitcast.30), channel_id=1, source_target_pairs={{0,1},{1,0},{2,3},{3,2},{4,5},{5,4},{6,7},{7,6},{8,9},{9,8},{10,11... | collective-permute-start | bytes 3145736 | tf_op jit(solution)/shard_map/ppermute | solution.py:206
  151.7 3.4 %collective-permute-start.14 = (bf16[256,1152]{1,0:T(8,128)(2,1)}, bf16[256,1152]{1,0:T(8,128)(2,1)S(1)}, u32[]{:S(2)}, u32[]{:S(2)}) collective-permute-start(bf16[256,1152]{1,0:T(8,128)(2,1)} %collective-permute-done.12.refs_6_), channel_id=1, source_target_pairs={{992,0},{0,32},{32,64},{64,96},{96,128},{128,160},{160,192},{192,2... | collective-permute-start | bytes 1769480 | tf_op jit(solution)/shard_map/ppermute | solution.py:19
  155.1 11.5 %collective-permute-done.13.refs_7_ = bf16[256,1152]{1,0:T(8,128)(2,1)S(1)} collective-permute-done((bf16[256,1152]{1,0:T(8,128)(2,1)S(1)}, bf16[256,1152]{1,0:T(8,128)(2,1)S(1)}, u32[]{:S(2)}, u32[]{:S(2)}) %collective-permute-start.13) | collective-permute-done | bytes 589856 | tf_op jit(solution)/shard_map/ppermute | solution.py:19
  178.5 3.5 %shard_map.115 = bf16[256,2048]{1,0:T(8,128)(2,1)S(1)} custom-call(s32[2]{0:T(128)S(1)} %shard_map.114.refs_0_, bf16[256,2048]{1,0:T(8,128)(2,1)S(1)} %bitcast.31, bf16[256,1152]{1,0:T(8,128)(2,1)S(1)} %bitcast.27, bf16[256,1152]{1,0:T(8,128)(2,1)S(1)} %collective-permute-done.9.refs_3_, bf16[256,1152]{1,0:T(8,128)(2,1)S(1)} %collective-permute-done.10.refs_4_, ...), custom_call_target="tpu_custom_call" | custom-call | tf_op jit(solution)/shard_map/pallas_call | solution.py:47
  182.0 3.5 %shard_map.116 = bf16[256,2048]{1,0:T(8,128)(2,1)S(1)} custom-call(s32[2]{0:T(128)S(1)} %shard_map.114.refs_0_, bf16[256,2048]{1,0:T(8,128)(2,1)S(1)} %collective-permute-done.8.refs_1_, bf16[256,1152]{1,0:T(8,128)(2,1)S(1)} %bitcast.28, bf16[256,1152]{1,0:T(8,128)(2,1)S(1)} %collective-permute-done.9.refs_3_, ...), custom_call_target="tpu_custom_call" | custom-call | tf_op jit(solution)/shard_map/pallas_call | solution.py:47
  185.6 4.9 %collective-permute-start.17 = (bf16[4,64,2048]{2,1,0:T(8,128)(2,1)S(1)}, bf16[4,64,2048]{2,1,0:T(8,128)(2,1)S(1)}, u32[]{:S(2)}, u32[]{:S(2)}) collective-permute-start(bf16[4,64,2048]{2,1,0:T(8,128)(2,1)S(1)} %bitcast.32), channel_id=1, source_target_pairs={{0,1},{1,0},{2,3},{3,2},{4,5},{5,4},{6,7},{7,6},{8,9},{9,8},{10,11... | collective-permute-start | bytes 3145736 | tf_op jit(solution)/shard_map/ppermute | solution.py:191
  193.2 17.2 %all_to_all.25.blocks = bf16[4,64,2048]{2,1,0:T(8,128)(2,1)S(1)} all-to-all(bf16[4,64,2048]{2,1,0:T(8,128)(2,1)S(1)} %add_convert_fusion), channel_id=1, replica_groups=mesh['rep'=4,'zl'=8,'y'=4,'x'=4,'core'=2] {'x'}, dimensions={0} | all-to-all | bytes 2097152 | tf_op jit(solution)/shard_map/all_to_all | solution.py:23
  (78 shorter events, 41.8 us)
Async XLA Ops:
  0.0 39.0 %copy-start.12 = (f32[2048]{0:T(1024)S(1)}, f32[2048]{0:T(1024)}, u32[]{:S(2)}) copy-start(f32[2048]{0:T(1024)} %param.12) | copy-start | bytes 24580
  0.8 40.4 %collective-permute-start = (bf16[64,512]{1,0:T(8,128)(2,1)S(1)}, bf16[64,512]{1,0:T(8,128)(2,1)S(1)}, u32[]{:S(2)}, u32[]{:S(2)}) collective-permute-start(bf16[64,512]{1,0:T(8,128)(2,1)S(1)} %pad_maximum_fusion), channel_id=1, source_target_pairs={{128,0},{160,32},{192,64},{224,96},{256,128},{288,160},{320,192},{... | collective-permute-start | bytes 196616 | tf_op jit(solution)/shard_map/ppermute | solution.py:19
  21.4 24.9 %collective-permute-start.1 = (bf16[64,512]{1,0:T(8,128)(2,1)S(1)}, bf16[64,512]{1,0:T(8,128)(2,1)S(1)}, u32[]{:S(2)}, u32[]{:S(2)}) collective-permute-start(bf16[64,512]{1,0:T(8,128)(2,1)S(1)} %pad_maximum_fusion), channel_id=1, source_target_pairs={{96,0},{128,32},{160,64},{192,96},{224,128},{256,160},{288,192},{3... | collective-permute-start | bytes 196616 | tf_op jit(solution)/shard_map/ppermute | solution.py:19
  26.1 22.1 %collective-permute-start.2 = (bf16[64,512]{1,0:T(8,128)(2,1)S(1)}, bf16[64,512]{1,0:T(8,128)(2,1)S(1)}, u32[]{:S(2)}, u32[]{:S(2)}) collective-permute-start(bf16[64,512]{1,0:T(8,128)(2,1)S(1)} %pad_maximum_fusion), channel_id=1, source_target_pairs={{928,0},{960,32},{992,64},{0,96},{32,128},{64,160},{96,192},{128,2... | collective-permute-start | bytes 196616 | tf_op jit(solution)/shard_map/ppermute | solution.py:19
  28.4 19.8 %collective-permute-start.3 = (bf16[64,512]{1,0:T(8,128)(2,1)S(1)}, bf16[64,512]{1,0:T(8,128)(2,1)S(1)}, u32[]{:S(2)}, u32[]{:S(2)}) collective-permute-start(bf16[64,512]{1,0:T(8,128)(2,1)S(1)} %pad_maximum_fusion), channel_id=1, source_target_pairs={{64,0},{96,32},{128,64},{160,96},{192,128},{224,160},{256,192},{28... | collective-permute-start | bytes 196616 | tf_op jit(solution)/shard_map/ppermute | solution.py:19
  34.0 14.3 %collective-permute-start.4 = (bf16[64,512]{1,0:T(8,128)(2,1)S(1)}, bf16[64,512]{1,0:T(8,128)(2,1)S(1)}, u32[]{:S(2)}, u32[]{:S(2)}) collective-permute-start(bf16[64,512]{1,0:T(8,128)(2,1)S(1)} %pad_maximum_fusion), channel_id=1, source_target_pairs={{960,0},{992,32},{0,64},{32,96},{64,128},{96,160},{128,192},{160,2... | collective-permute-start | bytes 196616 | tf_op jit(solution)/shard_map/ppermute | solution.py:19
  41.2 7.1 %collective-permute-start.5 = (bf16[64,512]{1,0:T(8,128)(2,1)S(1)}, bf16[64,512]{1,0:T(8,128)(2,1)S(1)}, u32[]{:S(2)}, u32[]{:S(2)}) collective-permute-start(bf16[64,512]{1,0:T(8,128)(2,1)S(1)} %pad_maximum_fusion), channel_id=1, source_target_pairs={{32,0},{64,32},{96,64},{128,96},{160,128},{192,160},{224,192},{256... | collective-permute-start | bytes 196616 | tf_op jit(solution)/shard_map/ppermute | solution.py:19
  46.3 6.2 %collective-permute-start.6 = (bf16[64,512]{1,0:T(8,128)(2,1)S(1)}, bf16[64,512]{1,0:T(8,128)(2,1)S(1)}, u32[]{:S(2)}, u32[]{:S(2)}) collective-permute-start(bf16[64,512]{1,0:T(8,128)(2,1)S(1)} %pad_maximum_fusion), channel_id=1, source_target_pairs={{992,0},{0,32},{32,64},{64,96},{96,128},{128,160},{160,192},{192,2... | collective-permute-start | bytes 196616 | tf_op jit(solution)/shard_map/ppermute | solution.py:19
  54.1 27.5 %all-to-all-start = ((bf16[4,8,64,512]{3,2,1,0:T(8,128)(2,1)}), bf16[4,8,64,512]{3,2,1,0:T(8,128)(2,1)}, u32[]{:S(2)}, u32[]{:S(2)}) async-start(bf16[4,8,64,512]{3,2,1,0:T(8,128)(2,1)} %broadcast_in_dim.4), calls=%async_computation | async-start | bytes 4194304 | tf_op jit(solution)/shard_map/all_to_all | solution.py:23
  61.1 32.5 %copy-start.9 = (bf16[352,64]{0,1:T(8,128)(2,1)S(1)}, bf16[352,64]{0,1:T(8,128)(2,1)}, u32[]{:S(2)}) copy-start(bf16[352,64]{0,1:T(8,128)(2,1)} %param.21) | copy-start | bytes 135172
  87.2 10.8 %collective-permute-start.7 = (bf16[4,64,2048]{2,1,0:T(8,128)(2,1)}, bf16[4,64,2048]{2,1,0:T(8,128)(2,1)S(1)}, u32[]{:S(2)}, u32[]{:S(2)}) collective-permute-start(bf16[4,64,2048]{2,1,0:T(8,128)(2,1)} %get-tuple-element.17), channel_id=1, source_target_pairs={{0,1},{1,0},{2,3},{3,2},{4,5},{5,4},{6,7},{7,6},{8,9},{9,8},{10,11... | collective-permute-start | bytes 3145736 | tf_op jit(solution)/shard_map/ppermute | solution.py:191
  94.5 13.7 %all-to-all-start.3 = ((bf16[4,64,1152]{2,1,0:T(8,128)(2,1)}), bf16[4,64,1152]{2,1,0:T(8,128)(2,1)S(1)}, u32[]{:S(2)}, u32[]{:S(2)}) async-start(bf16[4,64,1152]{2,1,0:T(8,128)(2,1)} %broadcast_in_dim.5), calls=%async_computation.3 | async-start | bytes 1179648 | tf_op jit(solution)/shard_map/all_to_all | solution.py:23
  108.2 18.1 %all-to-all-start.1 = ((bf16[4,64,2048]{2,1,0:T(8,128)(2,1)}), bf16[4,64,2048]{2,1,0:T(8,128)(2,1)S(1)}, u32[]{:S(2)}, u32[]{:S(2)}) async-start(bf16[4,64,2048]{2,1,0:T(8,128)(2,1)} %add_convert_fusion.1), calls=%async_computation.1 | async-start | bytes 2097152 | tf_op jit(solution)/shard_map/all_to_all | solution.py:23
  112.2 19.7 %collective-permute-start.9 = (bf16[256,1152]{1,0:T(8,128)(2,1)S(1)}, bf16[256,1152]{1,0:T(8,128)(2,1)S(1)}, u32[]{:S(2)}, u32[]{:S(2)}) collective-permute-start(bf16[256,1152]{1,0:T(8,128)(2,1)S(1)} %bitcast.25), channel_id=1, source_target_pairs={{32,0},{64,32},{96,64},{128,96},{160,128},{192,160},{224,192},{256... | collective-permute-start | bytes 1769480 | tf_op jit(solution)/shard_map/ppermute | solution.py:19
  114.1 19.7 %collective-permute-start.10 = (bf16[256,1152]{1,0:T(8,128)(2,1)S(1)}, bf16[256,1152]{1,0:T(8,128)(2,1)S(1)}, u32[]{:S(2)}, u32[]{:S(2)}) collective-permute-start(bf16[256,1152]{1,0:T(8,128)(2,1)S(1)} %bitcast.26), channel_id=1, source_target_pairs={{992,0},{0,32},{32,64},{64,96},{96,128},{128,160},{160,192},{192,2... | collective-permute-start | bytes 1769480 | tf_op jit(solution)/shard_map/ppermute | solution.py:19
  128.4 16.7 %all-to-all-start.2 = ((bf16[4,64,2048]{2,1,0:T(8,128)(2,1)}), bf16[4,64,2048]{2,1,0:T(8,128)(2,1)S(1)}, u32[]{:S(2)}, u32[]{:S(2)}) async-start(bf16[4,64,2048]{2,1,0:T(8,128)(2,1)} %copy-done), calls=%async_computation.2 | async-start | bytes 2097152 | tf_op jit(solution)/shard_map/all_to_all | solution.py:23
  131.9 17.9 %collective-permute-start.11 = (bf16[256,1152]{1,0:T(8,128)(2,1)S(1)}, bf16[256,1152]{1,0:T(8,128)(2,1)S(1)}, u32[]{:S(2)}, u32[]{:S(2)}) collective-permute-start(bf16[256,1152]{1,0:T(8,128)(2,1)S(1)} %collective-permute-done.9.refs_3_), channel_id=1, source_target_pairs={{32,0},{64,32},{96,64},{128,96},{160,128},{192,160},{224,192},{256... | collective-permute-start | bytes 1769480 | tf_op jit(solution)/shard_map/ppermute | solution.py:19
  133.8 17.9 %collective-permute-start.12 = (bf16[256,1152]{1,0:T(8,128)(2,1)S(1)}, bf16[256,1152]{1,0:T(8,128)(2,1)}, u32[]{:S(2)}, u32[]{:S(2)}) collective-permute-start(bf16[256,1152]{1,0:T(8,128)(2,1)S(1)} %collective-permute-done.10.refs_4_), channel_id=1, source_target_pairs={{992,0},{0,32},{32,64},{64,96},{96,128},{128,160},{160,192},{192,2... | collective-permute-start | bytes 1769480 | tf_op jit(solution)/shard_map/ppermute | solution.py:19
  145.0 37.0 %collective-permute-start.8 = (bf16[256,2048]{1,0:T(8,128)(2,1)S(1)}, bf16[256,2048]{1,0:T(8,128)(2,1)S(1)}, u32[]{:S(2)}, u32[]{:S(2)}) collective-permute-start(bf16[256,2048]{1,0:T(8,128)(2,1)S(1)} %bitcast.30), channel_id=1, source_target_pairs={{0,1},{1,0},{2,3},{3,2},{4,5},{5,4},{6,7},{7,6},{8,9},{9,8},{10,11... | collective-permute-start | bytes 3145736 | tf_op jit(solution)/shard_map/ppermute | solution.py:206
  149.8 16.8 %collective-permute-start.13 = (bf16[256,1152]{1,0:T(8,128)(2,1)S(1)}, bf16[256,1152]{1,0:T(8,128)(2,1)S(1)}, u32[]{:S(2)}, u32[]{:S(2)}) collective-permute-start(bf16[256,1152]{1,0:T(8,128)(2,1)S(1)} %collective-permute-done.11.refs_5_), channel_id=1, source_target_pairs={{32,0},{64,32},{96,64},{128,96},{160,128},{192,160},{224,192},{256... | collective-permute-start | bytes 1769480 | tf_op jit(solution)/shard_map/ppermute | solution.py:19
  151.7 17.1 %collective-permute-start.14 = (bf16[256,1152]{1,0:T(8,128)(2,1)}, bf16[256,1152]{1,0:T(8,128)(2,1)S(1)}, u32[]{:S(2)}, u32[]{:S(2)}) collective-permute-start(bf16[256,1152]{1,0:T(8,128)(2,1)} %collective-permute-done.12.refs_6_), channel_id=1, source_target_pairs={{992,0},{0,32},{32,64},{64,96},{96,128},{128,160},{160,192},{192,2... | collective-permute-start | bytes 1769480 | tf_op jit(solution)/shard_map/ppermute | solution.py:19
  166.6 9.6 %collective-permute-start.15 = (bf16[128,1152]{1,0:T(8,128)(2,1)S(1)}, bf16[128,1152]{1,0:T(8,128)(2,1)S(1)}, u32[]{:S(2)}, u32[]{:S(2)}) collective-permute-start(bf16[128,1152]{1,0:T(8,128)(2,1)S(1)} %slice.8), channel_id=1, source_target_pairs={{32,0},{64,32},{96,64},{128,96},{160,128},{192,160},{224,192},{256... | collective-permute-start | bytes 884744 | tf_op jit(solution)/shard_map/ppermute | solution.py:19
  168.9 9.6 %collective-permute-start.16 = (bf16[128,1152]{1,0:T(8,128)(2,1)S(1)}, bf16[128,1152]{1,0:T(8,128)(2,1)S(1)}, u32[]{:S(2)}, u32[]{:S(2)}) collective-permute-start(bf16[128,1152]{1,0:T(8,128)(2,1)S(1)} %slice.9), channel_id=1, source_target_pairs={{992,0},{0,32},{32,64},{64,96},{96,128},{128,160},{160,192},{192,2... | collective-permute-start | bytes 884744 | tf_op jit(solution)/shard_map/ppermute | solution.py:19
  185.6 7.2 %collective-permute-start.17 = (bf16[4,64,2048]{2,1,0:T(8,128)(2,1)S(1)}, bf16[4,64,2048]{2,1,0:T(8,128)(2,1)S(1)}, u32[]{:S(2)}, u32[]{:S(2)}) collective-permute-start(bf16[4,64,2048]{2,1,0:T(8,128)(2,1)S(1)} %bitcast.32), channel_id=1, source_target_pairs={{0,1},{1,0},{2,3},{3,2},{4,5},{5,4},{6,7},{7,6},{8,9},{9,8},{10,11... | collective-permute-start | bytes 3145736 | tf_op jit(solution)/shard_map/ppermute | solution.py:191
  (11 other events, 135.6 us)

commit v2 on v1

--- a/solution.py
+++ b/solution.py
@@ -21,10 +21,6 @@
 
 def exchange(blocks, axis):
     return lax.all_to_all(blocks, axis, 0, 0, tiled=True)
-
-
-def copies(array, count):
-    return jnp.broadcast_to(array[None], (count, *array.shape))
 
 
 def rms_scale(values, gain):
@@ -94,6 +90,36 @@
     )(pos)
 
 
+def norm_kernel(tokens, gain, normed):
+    normed[...] = rms_scale(tokens[...].astype(jnp.float32), gain[...]).astype(jnp.bfloat16)
+
+
+def stack_kernel(*refs):
+    for k, block in enumerate(refs[:-1]):
+        refs[-1][0, k] = block[...]
+
+
+def bundle_kernel(*refs):
+    out = refs[-1]
+    out[...] = jnp.zeros(out.shape, out.dtype)
+    step = out.shape[2] // (len(refs) - 1)
+    for k, array in enumerate(refs[:-1]):
+        out[0, :, k * step : k * step + array.shape[1]] = array[...]
+
+
+def for_exchange(kernel, args, count, shape, dtype):
+    args = [pltpu.with_memory_space_constraint(a, pltpu.VMEM) for a in args]
+    zeros = (0,) * len(shape)
+    return pl.pallas_call(
+        kernel,
+        grid=(count,),
+        out_shape=pltpu.HBM((count, *shape), dtype),
+        in_specs=[VMEM] * len(args),
+        out_specs=pl.BlockSpec((1, *shape), lambda k: (k, *zeros)),
+        compiler_params=pltpu.CompilerParams(vmem_limit_bytes=8 * 1024 * 1024),
+    )(*args)
+
+
 def join_kernel(blocks, own, gain, stream, sent):
     total = own[...].astype(jnp.float32)
     for k in range(blocks.shape[0]):
@@ -111,20 +137,21 @@
     out[...] = total.astype(jnp.bfloat16)
 
 
-def ffn_kernel(places, n_ff, down_at, pos, acts, *refs):
+def ffn_kernel(places, n_ff, pos, acts, *refs):
     chunks, out = refs[: len(places)], refs[len(places)]
     depth = acts.shape[1] // Z_LO
+    step = chunks[0].shape[1] // 3
     both = None
     firsts = []
     for (d, row), chunk in zip(places, chunks):
         z = lax.rem(pos[0] + (d + Z_LO), Z_LO)
         first = pl.multiple_of(z * depth + row, chunk.shape[0])
         firsts.append(first)
-        part = dot(acts[:, pl.ds(first, chunk.shape[0])], chunk[:, : 2 * n_ff])
+        part = dot(acts[:, pl.ds(first, chunk.shape[0])], chunk[:, : 2 * step])
         both = part if both is None else both + part
-    hidden = (jax.nn.silu(both[:, :n_ff]) * both[:, n_ff:]).astype(jnp.bfloat16)
+    hidden = (jax.nn.silu(both[:, :n_ff]) * both[:, step : step + n_ff]).astype(jnp.bfloat16)
     for first, chunk in zip(firsts, chunks):
-        part = dot_t(hidden, chunk[:, down_at : down_at + n_ff])
+        part = dot_t(hidden, chunk[:, 2 * step : 2 * step + n_ff])
         out[:, pl.ds(first, chunk.shape[0])] = part.astype(jnp.bfloat16)
 
 
@@ -154,14 +181,11 @@
     held = [mixer] + [shift(mixer, Z, nz, d) for k, d in enumerate(places) if k]
 
     n_ff = w_ffn_gate.shape[1]
-    down_at = -(-2 * n_ff // 128) * 128
-    width = -(-(down_at + n_ff) // 128) * 128
-    ffn = jnp.concatenate([w_ffn_gate, w_ffn_up], axis=1)
-    ffn = jnp.concatenate(
-        [jnp.pad(ffn, ((0, 0), (0, down_at - 2 * n_ff))), jnp.pad(w_ffn_down.T, ((0, 0), (0, width - down_at - n_ff)))],
-        axis=1,
-    )
-    ffn_y = exchange(copies(ffn, ny), "y").reshape(-1, width)
+    width = 3 * (-(-n_ff // 128) * 128)
+    sent_ffn = for_exchange(
+        bundle_kernel, (w_ffn_gate, w_ffn_up, w_ffn_down.T), ny, (w_ffn_gate.shape[0], width), w_ffn_gate.dtype
+    )
+    ffn_y = exchange(sent_ffn, "y").reshape(-1, width)
     chunks, ffn_places = [ffn_y], [(0, 0)]
     up = down = ffn_y
     for k in (1, 2, 3):
@@ -172,10 +196,9 @@
     chunks += [shift(up[:cut], Z, nz, 1), shift(down[cut:], Z, nz, -1)]
     ffn_places += [(4, 0), (4, cut)]
 
-    normed = rms_scale(tokens.astype(jnp.float32), mix_gain).astype(jnp.bfloat16)
     own = lax.dynamic_slice_in_dim(tokens, (lax.axis_index("x") * 2 + core) * own_rows, own_rows, 0)
-    held, normed, own = lax.optimization_barrier((jnp.stack(held), normed, own))
-    gathered = exchange(copies(held, ny), "y").reshape(ny, Z_LO, *mixer.shape)
+    sent_mixer = for_exchange(stack_kernel, held, ny, (Z_LO, *mixer.shape), mixer.dtype)
+    gathered = exchange(sent_mixer.reshape(-1, *mixer.shape), "y").reshape(ny, Z_LO, *mixer.shape)
 
     bf, f32 = jnp.bfloat16, jnp.float32
     halves = (nx, own_rows, feats)
@@ -183,7 +206,8 @@
     def mixer_body(*refs):
         mixer_kernel(places, ny, *refs)
 
-    pos = tick(tick(pos))
+    (normed,) = call(norm_kernel, (jax.ShapeDtypeStruct(tokens.shape, bf),), None, (tokens, mix_gain.reshape(1, -1)), 12)
+    pos = tick(pos)
     scratch = [pltpu.VMEM((feats, mixer.shape[1]), bf), pltpu.VMEM((count, w_gate_b.shape[1]), bf)]
     mine, other = call(mixer_body, (pltpu.VMEM(halves, bf),) * 2, pos, (normed, conv_taps, gathered), 16, scratch)
 
@@ -196,7 +220,7 @@
     blocks = over_tp(mine, other)
     stream, sent = call(
         join_kernel,
-        (pltpu.VMEM((own_rows, feats), f32), jax.ShapeDtypeStruct(halves, bf)),
+        (jax.ShapeDtypeStruct((own_rows, feats), f32), pltpu.HBM(halves, bf)),
         None,
         (blocks, own, ffn_gain.reshape(1, -1)),
         8,
@@ -206,7 +230,7 @@
     acts_other = lax.ppermute(acts, "core", SWAP)
 
     def ffn_body(*refs):
-        ffn_kernel(ffn_places, n_ff, down_at, *refs)
+        ffn_kernel(ffn_places, n_ff, *refs)
 
     def feed_forward(values):
         (out,) = call(ffn_body, (pltpu.VMEM((half_rows, feats), bf),), pos, (values, *chunks), 12)

time: 213 us -> 208 us (0.977)
  other arithmetic: 6.96 us -> 2.61 us
  waiting for transfers between devices: 68.2 us -> 64.4 us
  Pallas kernels: 18.3 us -> 21 us
    all_to_all x4, waiting for transfers between devices: 46 us -> 42.1 us  [exchange(): return lax.all_to_all(blocks, axis, 0, 0, tiled=True)]
    unnamed x32 -> x22, local copies, waits for them, and re-layouts: 1.87 us -> 5.33 us
    pallas_call x0 -> x2, Pallas kernels: none -> 3.3 us  [for_exchange(): pl.pallas_call(kernel, grid=(count,), out_shape=pltpu.HBM((count, *shape)...]
    broadcast_in_dim x2 -> x0, local copies, waits for them, and re-layouts: 2.44 us -> none  [copies(): return jnp.broadcast_to(array[None], (count, *array.shape))]
    convert_element_type x1 -> x0, other arithmetic: 2.15 us -> none  [local(): rms_scale(tokens.astype(jnp.float32), mix_gain).astype(jnp.bfloat16)]
    pallas_call x4 -> x3, Pallas kernels: 4.55 us -> 3.41 us  [tick(): pl.pallas_call(tick_kernel, out_shape=jax.ShapeDtypeStruct(pos.shape, pos...]
    pallas_call x5 -> x6, Pallas kernels: 13.8 us -> 14.3 us  [call(): pl.pallas_call(kernel, out_shape=outs, in_specs=specs, out_specs=(VMEM,)...]
  transfers between devices with their start and end apart: 22 -> 22, of which waited for: 9 -> 9; matrix products, arithmetic and copies ran while one was open for 4% -> 1% of each run, Pallas kernels for 4% -> 5%
where the time goes in v2:
time: 208 us; the launch traced here: 207 us
  starting transfers between devices  94.7 us (46%)
  waiting for transfers between devices  64.4 us (31%)
  Pallas kernels  21 us (10%)
  blocking collectives  17.2 us (8%)
  local copies, waits for them, and re-layouts  6.35 us (3%)
  other arithmetic  2.61 us (1%)
    ppermute x15, starting transfers between devices, shift(): lax.ppermute(value, axis, [((k + distance) % size, k) for k in range(size)])  63.1 us
    all_to_all x4, waiting for transfers between devices, exchange(): return lax.all_to_all(blocks, axis, 0, 0, tiled=True)  42.1 us
    ppermute x15, waiting for transfers between devices, shift(): lax.ppermute(value, axis, [((k + distance) % size, k) for k in range(size)])  20 us
    all_to_all x1, blocking collectives, exchange(): return lax.all_to_all(blocks, axis, 0, 0, tiled=True)  17.2 us
    all_to_all x4, starting transfers between devices, exchange(): return lax.all_to_all(blocks, axis, 0, 0, tiled=True)  15.3 us
    pallas_call x6, Pallas kernels, call(): pl.pallas_call(kernel, out_shape=outs, in_specs=specs, out_specs=(VMEM,)...  14.3 us
    ppermute x2, starting transfers between devices, over_tp(): got = lax.ppermute(other, 'core', SWAP)  11.5 us
    unnamed x22, local copies, waits for them, and re-layouts  5.33 us
  transfers between devices with their start and end apart: 22, of which 9 were waited for; matrix products, arithmetic and copies ran while one was open for 1% of the time, Pallas kernels for 5%

profile of v2, /device:TPU:1, one launch (start us, length us, event | category | flops | bytes accessed | tf_op | source)
XLA Modules:
  0.0 206.7 jit_solution(1666246358260663309)
XLA Ops:
  0.8 20.5 %collective-permute-start = (bf16[64,512]{1,0:T(8,128)(2,1)S(1)}, bf16[64,512]{1,0:T(8,128)(2,1)S(1)}, u32[]{:S(2)}, u32[]{:S(2)}) collective-permute-start(bf16[64,512]{1,0:T(8,128)(2,1)S(1)} %pad_maximum_fusion.refs_0_), channel_id=1, source_target_pairs={{128,0},{160,32},{192,64},{224,96},{256,128},{288,160},{320,192},{... | collective-permute-start | bytes 196616 | tf_op jit(solution)/shard_map/ppermute | solution.py:19
  21.3 4.7 %collective-permute-start.1 = (bf16[64,512]{1,0:T(8,128)(2,1)S(1)}, bf16[64,512]{1,0:T(8,128)(2,1)S(1)}, u32[]{:S(2)}, u32[]{:S(2)}) collective-permute-start(bf16[64,512]{1,0:T(8,128)(2,1)S(1)} %pad_maximum_fusion.refs_0_), channel_id=1, source_target_pairs={{96,0},{128,32},{160,64},{192,96},{224,128},{256,160},{288,192},{3... | collective-permute-start | bytes 196616 | tf_op jit(solution)/shard_map/ppermute | solution.py:19
  28.4 5.5 %collective-permute-start.3 = (bf16[64,512]{1,0:T(8,128)(2,1)S(1)}, bf16[64,512]{1,0:T(8,128)(2,1)S(1)}, u32[]{:S(2)}, u32[]{:S(2)}) collective-permute-start(bf16[64,512]{1,0:T(8,128)(2,1)S(1)} %pad_maximum_fusion.refs_0_), channel_id=1, source_target_pairs={{64,0},{96,32},{128,64},{160,96},{192,128},{224,160},{256,192},{28... | collective-permute-start | bytes 196616 | tf_op jit(solution)/shard_map/ppermute | solution.py:19
  35.9 5.0 %collective-permute-start.5 = (bf16[64,512]{1,0:T(8,128)(2,1)S(1)}, bf16[64,512]{1,0:T(8,128)(2,1)S(1)}, u32[]{:S(2)}, u32[]{:S(2)}) collective-permute-start(bf16[64,512]{1,0:T(8,128)(2,1)S(1)} %pad_maximum_fusion.refs_0_), channel_id=1, source_target_pairs={{32,0},{64,32},{96,64},{128,96},{160,128},{192,160},{224,192},{256... | collective-permute-start | bytes 196616 | tf_op jit(solution)/shard_map/ppermute | solution.py:19
  42.9 4.2 %collective-permute-done.6.refs_7_ = bf16[64,512]{1,0:T(8,128)(2,1)S(1)} collective-permute-done((bf16[64,512]{1,0:T(8,128)(2,1)S(1)}, bf16[64,512]{1,0:T(8,128)(2,1)S(1)}, u32[]{:S(2)}, u32[]{:S(2)}) %collective-permute-start.6) | collective-permute-done | bytes 65568 | tf_op jit(solution)/shard_map/ppermute | solution.py:19
  49.0 4.3 %all-to-all-start = ((bf16[32,64,512]{2,1,0:T(8,128)(2,1)}), bf16[32,64,512]{2,1,0:T(8,128)(2,1)S(1)}, u32[]{:S(2)}, u32[]{:S(2)}) async-start(bf16[32,64,512]{2,1,0:T(8,128)(2,1)} %bitcast.24), calls=%async_computation | async-start | bytes 4194304 | tf_op jit(solution)/shard_map/all_to_all | solution.py:23
  58.3 17.7 %all-to-all-done = bf16[32,64,512]{2,1,0:T(8,128)(2,1)S(1)} async-done(((bf16[32,64,512]{2,1,0:T(8,128)(2,1)}), bf16[32,64,512]{2,1,0:T(8,128)(2,1)S(1)}, u32[]{:S(2)}, u32[]{:S(2)}) %all-to-all-start) | async-done | bytes 2097184 | tf_op jit(solution)/shard_map/all_to_all | solution.py:23
  77.6 4.5 %shard_map.112 = (bf16[4,64,2048]{2,1,0:T(8,128)(2,1)S(1)}, bf16[4,64,2048]{2,1,0:T(8,128)(2,1)}) custom-call(s32[2]{0:T(128)S(1)} %shard_map.109.refs_0_.pos, bf16[512,2048]{1,0:T(8,128)(2,1)S(1)} %copy-done.1, f32[3,128]{1,0:T(4,128)S(1)} %copy-done.10, bf16[4,8,64,512]{3,2,1,0:T(8,128)(2,1)S(1)} %bitcast.12), custom_call_target="tpu_custom_call" | custom-call | tf_op jit(solution)/shard_map/pallas_call | solution.py:43
  82.0 6.5 %collective-permute-start.7 = (bf16[4,64,2048]{2,1,0:T(8,128)(2,1)}, bf16[4,64,2048]{2,1,0:T(8,128)(2,1)S(1)}, u32[]{:S(2)}, u32[]{:S(2)}) collective-permute-start(bf16[4,64,2048]{2,1,0:T(8,128)(2,1)} %get-tuple-element.12), channel_id=1, source_target_pairs={{0,1},{1,0},{2,3},{3,2},{4,5},{5,4},{6,7},{7,6},{8,9},{9,8},{10,11... | collective-permute-start | bytes 3145736 | tf_op jit(solution)/shard_map/ppermute | solution.py:215
  90.1 3.5 %all-to-all-start.3 = ((bf16[4,64,1152]{2,1,0:T(8,128)(2,1)}), bf16[4,64,1152]{2,1,0:T(8,128)(2,1)S(1)}, u32[]{:S(2)}, u32[]{:S(2)}) async-start(bf16[4,64,1152]{2,1,0:T(8,128)(2,1)} %shard_map.116), calls=%async_computation.3 | async-start | bytes 1179648 | tf_op jit(solution)/shard_map/all_to_all | solution.py:23
  94.9 8.8 %all-to-all-done.3 = bf16[4,64,1152]{2,1,0:T(8,128)(2,1)S(1)} async-done(((bf16[4,64,1152]{2,1,0:T(8,128)(2,1)}), bf16[4,64,1152]{2,1,0:T(8,128)(2,1)S(1)}, u32[]{:S(2)}, u32[]{:S(2)}) %all-to-all-start.3) | async-done | bytes 589856 | tf_op jit(solution)/shard_map/all_to_all | solution.py:23
  103.8 4.0 %all-to-all-start.1 = ((bf16[4,64,2048]{2,1,0:T(8,128)(2,1)}), bf16[4,64,2048]{2,1,0:T(8,128)(2,1)S(1)}, u32[]{:S(2)}, u32[]{:S(2)}) async-start(bf16[4,64,2048]{2,1,0:T(8,128)(2,1)} %add_convert_fusion.1), calls=%async_computation.1 | async-start | bytes 2097152 | tf_op jit(solution)/shard_map/all_to_all | solution.py:23
  109.7 3.4 %collective-permute-start.10 = (bf16[256,1152]{1,0:T(8,128)(2,1)S(1)}, bf16[256,1152]{1,0:T(8,128)(2,1)S(1)}, u32[]{:S(2)}, u32[]{:S(2)}) collective-permute-start(bf16[256,1152]{1,0:T(8,128)(2,1)S(1)} %bitcast.14), channel_id=1, source_target_pairs={{992,0},{0,32},{32,64},{64,96},{96,128},{128,160},{160,192},{192,2... | collective-permute-start | bytes 1769480 | tf_op jit(solution)/shard_map/ppermute | solution.py:19
  114.0 7.8 %all-to-all-done.1.blocks = bf16[4,64,2048]{2,1,0:T(8,128)(2,1)S(1)} async-done(((bf16[4,64,2048]{2,1,0:T(8,128)(2,1)}), bf16[4,64,2048]{2,1,0:T(8,128)(2,1)S(1)}, u32[]{:S(2)}, u32[]{:S(2)}) %all-to-all-start.1) | async-done | bytes 1048608 | tf_op jit(solution)/shard_map/all_to_all | solution.py:23
  123.9 3.5 %all-to-all-start.2 = ((bf16[4,64,2048]{2,1,0:T(8,128)(2,1)}), bf16[4,64,2048]{2,1,0:T(8,128)(2,1)S(1)}, u32[]{:S(2)}, u32[]{:S(2)}) async-start(bf16[4,64,2048]{2,1,0:T(8,128)(2,1)} %get-tuple-element.13), calls=%async_computation.2 | async-start | bytes 2097152 | tf_op jit(solution)/shard_map/all_to_all | solution.py:23
  129.4 3.4 %collective-permute-start.12 = (bf16[256,1152]{1,0:T(8,128)(2,1)S(1)}, bf16[256,1152]{1,0:T(8,128)(2,1)}, u32[]{:S(2)}, u32[]{:S(2)}) collective-permute-start(bf16[256,1152]{1,0:T(8,128)(2,1)S(1)} %collective-permute-done.10.refs_4_), channel_id=1, source_target_pairs={{992,0},{0,32},{32,64},{64,96},{96,128},{128,160},{160,192},{192,2... | collective-permute-start | bytes 1769480 | tf_op jit(solution)/shard_map/ppermute | solution.py:19
  132.7 7.8 %all-to-all-done.2 = bf16[4,64,2048]{2,1,0:T(8,128)(2,1)S(1)} async-done(((bf16[4,64,2048]{2,1,0:T(8,128)(2,1)}), bf16[4,64,2048]{2,1,0:T(8,128)(2,1)S(1)}, u32[]{:S(2)}, u32[]{:S(2)}) %all-to-all-start.2) | async-done | bytes 1048608 | tf_op jit(solution)/shard_map/all_to_all | solution.py:23
  140.6 4.8 %collective-permute-start.8 = (bf16[256,2048]{1,0:T(8,128)(2,1)S(1)}, bf16[256,2048]{1,0:T(8,128)(2,1)S(1)}, u32[]{:S(2)}, u32[]{:S(2)}) collective-permute-start(bf16[256,2048]{1,0:T(8,128)(2,1)S(1)} %bitcast.18), channel_id=1, source_target_pairs={{0,1},{1,0},{2,3},{3,2},{4,5},{5,4},{6,7},{7,6},{8,9},{9,8},{10,11... | collective-permute-start | bytes 3145736 | tf_op jit(solution)/shard_map/ppermute | solution.py:230
  147.3 3.4 %collective-permute-start.14 = (bf16[256,1152]{1,0:T(8,128)(2,1)}, bf16[256,1152]{1,0:T(8,128)(2,1)S(1)}, u32[]{:S(2)}, u32[]{:S(2)}) collective-permute-start(bf16[256,1152]{1,0:T(8,128)(2,1)} %collective-permute-done.12.refs_6_), channel_id=1, source_target_pairs={{992,0},{0,32},{32,64},{64,96},{96,128},{128,160},{160,192},{192,2... | collective-permute-start | bytes 1769480 | tf_op jit(solution)/shard_map/ppermute | solution.py:19
  150.7 11.5 %collective-permute-done.13.refs_7_ = bf16[256,1152]{1,0:T(8,128)(2,1)S(1)} collective-permute-done((bf16[256,1152]{1,0:T(8,128)(2,1)S(1)}, bf16[256,1152]{1,0:T(8,128)(2,1)S(1)}, u32[]{:S(2)}, u32[]{:S(2)}) %collective-permute-start.13) | collective-permute-done | bytes 589856 | tf_op jit(solution)/shard_map/ppermute | solution.py:19
  174.0 3.4 %shard_map.117 = bf16[256,2048]{1,0:T(8,128)(2,1)S(1)} custom-call(s32[2]{0:T(128)S(1)} %shard_map.115.refs_0_, bf16[256,2048]{1,0:T(8,128)(2,1)S(1)} %bitcast.19, bf16[256,1152]{1,0:T(8,128)(2,1)S(1)} %bitcast.15, bf16[256,1152]{1,0:T(8,128)(2,1)S(1)} %collective-permute-done.9.refs_3_, bf16[256,1152]{1,0:T(8,128)(2,1)S(1)} %collective-permute-done.10.refs_4_, ...), custom_call_target="tpu_custom_call" | custom-call | tf_op jit(solution)/shard_map/pallas_call | solution.py:43
  177.5 3.4 %shard_map.118 = bf16[256,2048]{1,0:T(8,128)(2,1)S(1)} custom-call(s32[2]{0:T(128)S(1)} %shard_map.115.refs_0_, bf16[256,2048]{1,0:T(8,128)(2,1)S(1)} %collective-permute-done.8.refs_1_, bf16[256,1152]{1,0:T(8,128)(2,1)S(1)} %bitcast.16, bf16[256,1152]{1,0:T(8,128)(2,1)S(1)} %collective-permute-done.9.refs_3_, ...), custom_call_target="tpu_custom_call" | custom-call | tf_op jit(solution)/shard_map/pallas_call | solution.py:43
  181.0 4.9 %collective-permute-start.17 = (bf16[4,64,2048]{2,1,0:T(8,128)(2,1)S(1)}, bf16[4,64,2048]{2,1,0:T(8,128)(2,1)S(1)}, u32[]{:S(2)}, u32[]{:S(2)}) collective-permute-start(bf16[4,64,2048]{2,1,0:T(8,128)(2,1)S(1)} %bitcast.20), channel_id=1, source_target_pairs={{0,1},{1,0},{2,3},{3,2},{4,5},{5,4},{6,7},{7,6},{8,9},{9,8},{10,11... | collective-permute-start | bytes 3145736 | tf_op jit(solution)/shard_map/ppermute | solution.py:215
  188.6 17.2 %all_to_all.25.blocks = bf16[4,64,2048]{2,1,0:T(8,128)(2,1)S(1)} all-to-all(bf16[4,64,2048]{2,1,0:T(8,128)(2,1)S(1)} %add_convert_fusion), channel_id=1, replica_groups=mesh['rep'=4,'zl'=8,'y'=4,'x'=4,'core'=2] {'x'}, dimensions={0} | all-to-all | bytes 2097152 | tf_op jit(solution)/shard_map/all_to_all | solution.py:23
  (61 shorter events, 42.4 us)
Async XLA Ops:
  0.8 35.1 %collective-permute-start = (bf16[64,512]{1,0:T(8,128)(2,1)S(1)}, bf16[64,512]{1,0:T(8,128)(2,1)S(1)}, u32[]{:S(2)}, u32[]{:S(2)}) collective-permute-start(bf16[64,512]{1,0:T(8,128)(2,1)S(1)} %pad_maximum_fusion.refs_0_), channel_id=1, source_target_pairs={{128,0},{160,32},{192,64},{224,96},{256,128},{288,160},{320,192},{... | collective-permute-start | bytes 196616 | tf_op jit(solution)/shard_map/ppermute | solution.py:19
  21.3 19.6 %collective-permute-start.1 = (bf16[64,512]{1,0:T(8,128)(2,1)S(1)}, bf16[64,512]{1,0:T(8,128)(2,1)S(1)}, u32[]{:S(2)}, u32[]{:S(2)}) collective-permute-start(bf16[64,512]{1,0:T(8,128)(2,1)S(1)} %pad_maximum_fusion.refs_0_), channel_id=1, source_target_pairs={{96,0},{128,32},{160,64},{192,96},{224,128},{256,160},{288,192},{3... | collective-permute-start | bytes 196616 | tf_op jit(solution)/shard_map/ppermute | solution.py:19
  26.1 16.8 %collective-permute-start.2 = (bf16[64,512]{1,0:T(8,128)(2,1)S(1)}, bf16[64,512]{1,0:T(8,128)(2,1)S(1)}, u32[]{:S(2)}, u32[]{:S(2)}) collective-permute-start(bf16[64,512]{1,0:T(8,128)(2,1)S(1)} %pad_maximum_fusion.refs_0_), channel_id=1, source_target_pairs={{928,0},{960,32},{992,64},{0,96},{32,128},{64,160},{96,192},{128,2... | collective-permute-start | bytes 196616 | tf_op jit(solution)/shard_map/ppermute | solution.py:19
  28.4 14.4 %collective-permute-start.3 = (bf16[64,512]{1,0:T(8,128)(2,1)S(1)}, bf16[64,512]{1,0:T(8,128)(2,1)S(1)}, u32[]{:S(2)}, u32[]{:S(2)}) collective-permute-start(bf16[64,512]{1,0:T(8,128)(2,1)S(1)} %pad_maximum_fusion.refs_0_), channel_id=1, source_target_pairs={{64,0},{96,32},{128,64},{160,96},{192,128},{224,160},{256,192},{28... | collective-permute-start | bytes 196616 | tf_op jit(solution)/shard_map/ppermute | solution.py:19
  33.9 8.9 %collective-permute-start.4 = (bf16[64,512]{1,0:T(8,128)(2,1)S(1)}, bf16[64,512]{1,0:T(8,128)(2,1)S(1)}, u32[]{:S(2)}, u32[]{:S(2)}) collective-permute-start(bf16[64,512]{1,0:T(8,128)(2,1)S(1)} %pad_maximum_fusion.refs_0_), channel_id=1, source_target_pairs={{960,0},{992,32},{0,64},{32,96},{64,128},{96,160},{128,192},{160,2... | collective-permute-start | bytes 196616 | tf_op jit(solution)/shard_map/ppermute | solution.py:19
  35.9 7.0 %collective-permute-start.5 = (bf16[64,512]{1,0:T(8,128)(2,1)S(1)}, bf16[64,512]{1,0:T(8,128)(2,1)S(1)}, u32[]{:S(2)}, u32[]{:S(2)}) collective-permute-start(bf16[64,512]{1,0:T(8,128)(2,1)S(1)} %pad_maximum_fusion.refs_0_), channel_id=1, source_target_pairs={{32,0},{64,32},{96,64},{128,96},{160,128},{192,160},{224,192},{256... | collective-permute-start | bytes 196616 | tf_op jit(solution)/shard_map/ppermute | solution.py:19
  40.9 6.2 %collective-permute-start.6 = (bf16[64,512]{1,0:T(8,128)(2,1)S(1)}, bf16[64,512]{1,0:T(8,128)(2,1)S(1)}, u32[]{:S(2)}, u32[]{:S(2)}) collective-permute-start(bf16[64,512]{1,0:T(8,128)(2,1)S(1)} %pad_maximum_fusion.refs_0_), channel_id=1, source_target_pairs={{992,0},{0,32},{32,64},{64,96},{96,128},{128,160},{160,192},{192,2... | collective-permute-start | bytes 196616 | tf_op jit(solution)/shard_map/ppermute | solution.py:19
  49.0 27.0 %all-to-all-start = ((bf16[32,64,512]{2,1,0:T(8,128)(2,1)}), bf16[32,64,512]{2,1,0:T(8,128)(2,1)S(1)}, u32[]{:S(2)}, u32[]{:S(2)}) async-start(bf16[32,64,512]{2,1,0:T(8,128)(2,1)} %bitcast.24), calls=%async_computation | async-start | bytes 4194304 | tf_op jit(solution)/shard_map/all_to_all | solution.py:23
  82.0 11.5 %collective-permute-start.7 = (bf16[4,64,2048]{2,1,0:T(8,128)(2,1)}, bf16[4,64,2048]{2,1,0:T(8,128)(2,1)S(1)}, u32[]{:S(2)}, u32[]{:S(2)}) collective-permute-start(bf16[4,64,2048]{2,1,0:T(8,128)(2,1)} %get-tuple-element.12), channel_id=1, source_target_pairs={{0,1},{1,0},{2,3},{3,2},{4,5},{5,4},{6,7},{7,6},{8,9},{9,8},{10,11... | collective-permute-start | bytes 3145736 | tf_op jit(solution)/shard_map/ppermute | solution.py:215
  90.1 13.7 %all-to-all-start.3 = ((bf16[4,64,1152]{2,1,0:T(8,128)(2,1)}), bf16[4,64,1152]{2,1,0:T(8,128)(2,1)S(1)}, u32[]{:S(2)}, u32[]{:S(2)}) async-start(bf16[4,64,1152]{2,1,0:T(8,128)(2,1)} %shard_map.116), calls=%async_computation.3 | async-start | bytes 1179648 | tf_op jit(solution)/shard_map/all_to_all | solution.py:23
  94.9 26.9 %copy-start.9 = (f32[2048]{0:T(1024)S(1)}, f32[2048]{0:T(1024)}, u32[]{:S(2)}) copy-start(f32[2048]{0:T(1024)} %param.18) | copy-start | bytes 24580
  103.8 18.1 %all-to-all-start.1 = ((bf16[4,64,2048]{2,1,0:T(8,128)(2,1)}), bf16[4,64,2048]{2,1,0:T(8,128)(2,1)S(1)}, u32[]{:S(2)}, u32[]{:S(2)}) async-start(bf16[4,64,2048]{2,1,0:T(8,128)(2,1)} %add_convert_fusion.1), calls=%async_computation.1 | async-start | bytes 2097152 | tf_op jit(solution)/shard_map/all_to_all | solution.py:23
  107.8 19.6 %collective-permute-start.9 = (bf16[256,1152]{1,0:T(8,128)(2,1)S(1)}, bf16[256,1152]{1,0:T(8,128)(2,1)S(1)}, u32[]{:S(2)}, u32[]{:S(2)}) collective-permute-start(bf16[256,1152]{1,0:T(8,128)(2,1)S(1)} %bitcast.13), channel_id=1, source_target_pairs={{32,0},{64,32},{96,64},{128,96},{160,128},{192,160},{224,192},{256... | collective-permute-start | bytes 1769480 | tf_op jit(solution)/shard_map/ppermute | solution.py:19
  109.7 19.7 %collective-permute-start.10 = (bf16[256,1152]{1,0:T(8,128)(2,1)S(1)}, bf16[256,1152]{1,0:T(8,128)(2,1)S(1)}, u32[]{:S(2)}, u32[]{:S(2)}) collective-permute-start(bf16[256,1152]{1,0:T(8,128)(2,1)S(1)} %bitcast.14), channel_id=1, source_target_pairs={{992,0},{0,32},{32,64},{64,96},{96,128},{128,160},{160,192},{192,2... | collective-permute-start | bytes 1769480 | tf_op jit(solution)/shard_map/ppermute | solution.py:19
  123.9 16.7 %all-to-all-start.2 = ((bf16[4,64,2048]{2,1,0:T(8,128)(2,1)}), bf16[4,64,2048]{2,1,0:T(8,128)(2,1)S(1)}, u32[]{:S(2)}, u32[]{:S(2)}) async-start(bf16[4,64,2048]{2,1,0:T(8,128)(2,1)} %get-tuple-element.13), calls=%async_computation.2 | async-start | bytes 2097152 | tf_op jit(solution)/shard_map/all_to_all | solution.py:23
  127.4 17.9 %collective-permute-start.11 = (bf16[256,1152]{1,0:T(8,128)(2,1)S(1)}, bf16[256,1152]{1,0:T(8,128)(2,1)S(1)}, u32[]{:S(2)}, u32[]{:S(2)}) collective-permute-start(bf16[256,1152]{1,0:T(8,128)(2,1)S(1)} %collective-permute-done.9.refs_3_), channel_id=1, source_target_pairs={{32,0},{64,32},{96,64},{128,96},{160,128},{192,160},{224,192},{256... | collective-permute-start | bytes 1769480 | tf_op jit(solution)/shard_map/ppermute | solution.py:19
  129.4 17.9 %collective-permute-start.12 = (bf16[256,1152]{1,0:T(8,128)(2,1)S(1)}, bf16[256,1152]{1,0:T(8,128)(2,1)}, u32[]{:S(2)}, u32[]{:S(2)}) collective-permute-start(bf16[256,1152]{1,0:T(8,128)(2,1)S(1)} %collective-permute-done.10.refs_4_), channel_id=1, source_target_pairs={{992,0},{0,32},{32,64},{64,96},{96,128},{128,160},{160,192},{192,2... | collective-permute-start | bytes 1769480 | tf_op jit(solution)/shard_map/ppermute | solution.py:19
  140.6 36.9 %collective-permute-start.8 = (bf16[256,2048]{1,0:T(8,128)(2,1)S(1)}, bf16[256,2048]{1,0:T(8,128)(2,1)S(1)}, u32[]{:S(2)}, u32[]{:S(2)}) collective-permute-start(bf16[256,2048]{1,0:T(8,128)(2,1)S(1)} %bitcast.18), channel_id=1, source_target_pairs={{0,1},{1,0},{2,3},{3,2},{4,5},{5,4},{6,7},{7,6},{8,9},{9,8},{10,11... | collective-permute-start | bytes 3145736 | tf_op jit(solution)/shard_map/ppermute | solution.py:230
  145.4 16.8 %collective-permute-start.13 = (bf16[256,1152]{1,0:T(8,128)(2,1)S(1)}, bf16[256,1152]{1,0:T(8,128)(2,1)S(1)}, u32[]{:S(2)}, u32[]{:S(2)}) collective-permute-start(bf16[256,1152]{1,0:T(8,128)(2,1)S(1)} %collective-permute-done.11.refs_5_), channel_id=1, source_target_pairs={{32,0},{64,32},{96,64},{128,96},{160,128},{192,160},{224,192},{256... | collective-permute-start | bytes 1769480 | tf_op jit(solution)/shard_map/ppermute | solution.py:19
  147.3 17.1 %collective-permute-start.14 = (bf16[256,1152]{1,0:T(8,128)(2,1)}, bf16[256,1152]{1,0:T(8,128)(2,1)S(1)}, u32[]{:S(2)}, u32[]{:S(2)}) collective-permute-start(bf16[256,1152]{1,0:T(8,128)(2,1)} %collective-permute-done.12.refs_6_), channel_id=1, source_target_pairs={{992,0},{0,32},{32,64},{64,96},{96,128},{128,160},{160,192},{192,2... | collective-permute-start | bytes 1769480 | tf_op jit(solution)/shard_map/ppermute | solution.py:19
  162.1 9.6 %collective-permute-start.15 = (bf16[128,1152]{1,0:T(8,128)(2,1)S(1)}, bf16[128,1152]{1,0:T(8,128)(2,1)S(1)}, u32[]{:S(2)}, u32[]{:S(2)}) collective-permute-start(bf16[128,1152]{1,0:T(8,128)(2,1)S(1)} %slice.8), channel_id=1, source_target_pairs={{32,0},{64,32},{96,64},{128,96},{160,128},{192,160},{224,192},{256... | collective-permute-start | bytes 884744 | tf_op jit(solution)/shard_map/ppermute | solution.py:19
  164.4 9.6 %collective-permute-start.16 = (bf16[128,1152]{1,0:T(8,128)(2,1)S(1)}, bf16[128,1152]{1,0:T(8,128)(2,1)S(1)}, u32[]{:S(2)}, u32[]{:S(2)}) collective-permute-start(bf16[128,1152]{1,0:T(8,128)(2,1)S(1)} %slice.9), channel_id=1, source_target_pairs={{992,0},{0,32},{32,64},{64,96},{96,128},{128,160},{160,192},{192,2... | collective-permute-start | bytes 884744 | tf_op jit(solution)/shard_map/ppermute | solution.py:19
  181.0 24.9 %copy-start.4 = (f32[64,2048]{1,0:T(8,128)S(1)}, f32[64,2048]{1,0:T(8,128)}, u32[]{:S(2)}) copy-start(f32[64,2048]{1,0:T(8,128)} %copy-done.3) | copy-start | bytes 1572868
  181.0 7.2 %collective-permute-start.17 = (bf16[4,64,2048]{2,1,0:T(8,128)(2,1)S(1)}, bf16[4,64,2048]{2,1,0:T(8,128)(2,1)S(1)}, u32[]{:S(2)}, u32[]{:S(2)}) collective-permute-start(bf16[4,64,2048]{2,1,0:T(8,128)(2,1)S(1)} %bitcast.20), channel_id=1, source_target_pairs={{0,1},{1,0},{2,3},{3,2},{4,5},{5,4},{6,7},{7,6},{8,9},{9,8},{10,11... | collective-permute-start | bytes 3145736 | tf_op jit(solution)/shard_map/ppermute | solution.py:215
  (9 other events, 63.8 us)

commit v3 on v2

--- a/solution.py
+++ b/solution.py
@@ -50,15 +50,14 @@
     )(*args)
 
 
-def mixer_kernel(places, n_y, pos, normed, taps, gathered, mine, other, weights, gated):
-    zl, core = pos[0], pos[1]
-    rows = gathered.shape[2]
+def mixer_kernel(pos, normed, taps, gathered, mine, other, weights, gated):
+    core = pos[1]
+    n_y, n_z, rows, _ = gathered.shape
     width = taps.shape[1]
-    for k, d in enumerate(places):
-        z = lax.rem(zl + (d + Z_LO), Z_LO)
+    for z in range(n_z):
         for y in range(n_y):
-            first = pl.multiple_of((z * n_y + y) * rows, rows)
-            weights[pl.ds(first, rows), :] = gathered[y, k]
+            first = (z * n_y + y) * rows
+            weights[first : first + rows, :] = gathered[y, z]
     products = dot(normed[...], weights[:, : 3 * width])
     p = products[:, width : 2 * width] * products[:, 2 * width : 3 * width]
     place = lax.broadcasted_iota(jnp.int32, p.shape, 0) % LEN
@@ -90,13 +89,15 @@
     )(pos)
 
 
-def norm_kernel(tokens, gain, normed):
-    normed[...] = rms_scale(tokens[...].astype(jnp.float32), gain[...]).astype(jnp.bfloat16)
-
-
-def stack_kernel(*refs):
-    for k, block in enumerate(refs[:-1]):
-        refs[-1][0, k] = block[...]
+def ordered_kernel(places, pos, *refs):
+    out = refs[-1]
+    for d, block in zip(places, refs[:-1]):
+        y = lax.rem(pos[2] + (d + len(places)), len(places))
+        out[pl.ds(pl.multiple_of(y * block.shape[0], block.shape[0]), block.shape[0]), :] = block[...]
+
+
+def copy_kernel(block, out):
+    out[0] = block[...]
 
 
 def bundle_kernel(*refs):
@@ -107,13 +108,13 @@
         out[0, :, k * step : k * step + array.shape[1]] = array[...]
 
 
-def for_exchange(kernel, args, count, shape, dtype):
-    args = [pltpu.with_memory_space_constraint(a, pltpu.VMEM) for a in args]
+def for_exchange(kernel, args, count, shape, dtype, space=pltpu.HBM, source=pltpu.HBM):
+    args = [pltpu.with_memory_space_constraint(a, source) for a in args]
     zeros = (0,) * len(shape)
     return pl.pallas_call(
         kernel,
         grid=(count,),
-        out_shape=pltpu.HBM((count, *shape), dtype),
+        out_shape=space((count, *shape), dtype),
         in_specs=[VMEM] * len(args),
         out_specs=pl.BlockSpec((1, *shape), lambda k: (k, *zeros)),
         compiler_params=pltpu.CompilerParams(vmem_limit_bytes=8 * 1024 * 1024),
@@ -171,21 +172,32 @@
     nx, ny = lax.axis_size("x"), lax.axis_size("y")
     nz = lax.axis_size("rep") * lax.axis_size("zl")
     zl, core = lax.axis_index("zl"), lax.axis_index("core")
-    pos = jnp.stack([zl, core]).astype(jnp.int32)
+    pos = jnp.stack([zl, core, lax.axis_index("y")]).astype(jnp.int32)
     count, feats = tokens.shape
     half_rows = count // 2
     own_rows = half_rows // nx
 
-    mixer = jnp.concatenate([w_gate_b, w_gate_c, w_conv_in, w_mix_out.T], axis=1)
-    places = [0, 4, 3, -3, 2, -2, 1, -1]
-    held = [mixer] + [shift(mixer, Z, nz, d) for k, d in enumerate(places) if k]
+    parts = (w_gate_b, w_gate_c, w_conv_in, w_mix_out.T)
+    mixer_shape = (w_gate_b.shape[0], sum(part.shape[1] for part in parts))
+    sent = for_exchange(bundle_kernel, parts, Z_LO, mixer_shape, w_gate_b.dtype)
+    along_z = exchange(sent, "zl")
+    sent = for_exchange(copy_kernel, (along_z,), ny, along_z.shape, along_z.dtype, source=pltpu.VMEM)
+    normed = rms_scale(tokens.astype(jnp.float32), mix_gain).astype(jnp.bfloat16)
+    own = lax.dynamic_slice_in_dim(tokens, (lax.axis_index("x") * 2 + core) * own_rows, own_rows, 0)
+    gathered = exchange(sent.reshape(-1, *mixer_shape), "y").reshape(ny, Z_LO, *mixer_shape)
 
     n_ff = w_ffn_gate.shape[1]
     width = 3 * (-(-n_ff // 128) * 128)
-    sent_ffn = for_exchange(
-        bundle_kernel, (w_ffn_gate, w_ffn_up, w_ffn_down.T), ny, (w_ffn_gate.shape[0], width), w_ffn_gate.dtype
-    )
-    ffn_y = exchange(sent_ffn, "y").reshape(-1, width)
+    ffn_shape = (w_ffn_gate.shape[0], width)
+    parts = (w_ffn_gate, w_ffn_up, w_ffn_down.T)
+    ffn = for_exchange(bundle_kernel, parts, 1, ffn_shape, w_ffn_gate.dtype, jax.ShapeDtypeStruct)[0]
+    y_places = [0, 2, 1, -1]
+    blocks = [shift(ffn, "y", ny, d) if d else ffn for d in y_places]
+
+    def ordered_body(*refs):
+        ordered_kernel(y_places, *refs)
+
+    (ffn_y,) = call(ordered_body, (jax.ShapeDtypeStruct((ny * ffn_shape[0], width), ffn.dtype),), pos, blocks, 4)
     chunks, ffn_places = [ffn_y], [(0, 0)]
     up = down = ffn_y
     for k in (1, 2, 3):
@@ -196,20 +208,12 @@
     chunks += [shift(up[:cut], Z, nz, 1), shift(down[cut:], Z, nz, -1)]
     ffn_places += [(4, 0), (4, cut)]
 
-    own = lax.dynamic_slice_in_dim(tokens, (lax.axis_index("x") * 2 + core) * own_rows, own_rows, 0)
-    sent_mixer = for_exchange(stack_kernel, held, ny, (Z_LO, *mixer.shape), mixer.dtype)
-    gathered = exchange(sent_mixer.reshape(-1, *mixer.shape), "y").reshape(ny, Z_LO, *mixer.shape)
-
     bf, f32 = jnp.bfloat16, jnp.float32
     halves = (nx, own_rows, feats)
 
-    def mixer_body(*refs):
-        mixer_kernel(places, ny, *refs)
-
-    (normed,) = call(norm_kernel, (jax.ShapeDtypeStruct(tokens.shape, bf),), None, (tokens, mix_gain.reshape(1, -1)), 12)
     pos = tick(pos)
-    scratch = [pltpu.VMEM((feats, mixer.shape[1]), bf), pltpu.VMEM((count, w_gate_b.shape[1]), bf)]
-    mine, other = call(mixer_body, (pltpu.VMEM(halves, bf),) * 2, pos, (normed, conv_taps, gathered), 16, scratch)
+    scratch = [pltpu.VMEM((feats, mixer_shape[1]), bf), pltpu.VMEM((count, w_gate_b.shape[1]), bf)]
+    mine, other = call(mixer_kernel, (pltpu.VMEM(halves, bf),) * 2, pos, (normed, conv_taps, gathered), 16, scratch)
 
     def over_tp(mine, other):
         got = lax.ppermute(other, "core", SWAP)

time: 208 us -> 210 us (level)
  blocking collectives: 17.2 us -> 52.5 us
  waiting for transfers between devices: 64.4 us -> 40.4 us
  starting transfers between devices: 94.7 us -> 84 us
  other arithmetic: 2.61 us -> 5.8 us
  local copies, waits for them, and re-layouts: 6.35 us -> 3.43 us
    all_to_all x1 -> x2, blocking collectives: 17.2 us -> 52.5 us  [exchange(): return lax.all_to_all(blocks, axis, 0, 0, tiled=True)]
    all_to_all x4 -> x3, waiting for transfers between devices: 42.1 us -> 16.5 us  [exchange(): return lax.all_to_all(blocks, axis, 0, 0, tiled=True)]
    ppermute x15 -> x11, starting transfers between devices: 63.1 us -> 47.1 us  [shift(): lax.ppermute(value, axis, [((k + distance) % size, k) for k in range(size)])]
    ppermute x2, starting transfers between devices: 11.5 us -> 17.9 us  [over_tp(): got = lax.ppermute(other, 'core', SWAP)]
    unnamed x22 -> x14, local copies, waits for them, and re-layouts: 5.33 us -> 2.41 us
    pallas_call x2 -> x3, Pallas kernels: 3.3 us -> 6.09 us  [for_exchange(): pl.pallas_call(kernel, grid=(count,), out_shape=space((count, *shape), dt...]
    all_to_all x4 -> x3, starting transfers between devices: 15.3 us -> 12.8 us  [exchange(): return lax.all_to_all(blocks, axis, 0, 0, tiled=True)]
    ppermute x2, waiting for transfers between devices: 2.27 us -> 4.53 us  [over_tp(): got = lax.ppermute(other, 'core', SWAP)]
  transfers between devices with their start and end apart: 22 -> 17, of which waited for: 9 -> 9; matrix products, arithmetic and copies ran while one was open for 1% -> 2% of each run, Pallas kernels for 5% -> 5%
where the time goes in v3:
time: 210 us; the launch traced here: 209 us
  starting transfers between devices  84 us (40%)
  blocking collectives  52.5 us (25%)
  waiting for transfers between devices  40.4 us (19%)
  Pallas kernels  22.6 us (11%)
  other arithmetic  5.8 us (3%)
  local copies, waits for them, and re-layouts  3.43 us (2%)
    all_to_all x2, blocking collectives, exchange(): return lax.all_to_all(blocks, axis, 0, 0, tiled=True)  52.5 us
    ppermute x11, starting transfers between devices, shift(): lax.ppermute(value, axis, [((k + distance) % size, k) for k in range(size)])  47.1 us
    ppermute x11, waiting for transfers between devices, shift(): lax.ppermute(value, axis, [((k + distance) % size, k) for k in range(size)])  19.3 us
    ppermute x2, starting transfers between devices, over_tp(): got = lax.ppermute(other, 'core', SWAP)  17.9 us
    all_to_all x3, waiting for transfers between devices, exchange(): return lax.all_to_all(blocks, axis, 0, 0, tiled=True)  16.5 us
    pallas_call x6, Pallas kernels, call(): pl.pallas_call(kernel, out_shape=outs, in_specs=specs, out_specs=(VMEM,)...  13.1 us
    all_to_all x3, starting transfers between devices, exchange(): return lax.all_to_all(blocks, axis, 0, 0, tiled=True)  12.8 us
    ppermute x1, starting transfers between devices, local(): acts_other = lax.ppermute(acts, 'core', SWAP)  6.25 us
  transfers between devices with their start and end apart: 17, of which 9 were waited for; matrix products, arithmetic and copies ran while one was open for 2% of the time, Pallas kernels for 5%

profile of v3, /device:TPU:1, one launch (start us, length us, event | category | flops | bytes accessed | tf_op | source)
XLA Modules:
  0.0 209.0 jit_solution(6412119629707452188)
XLA Ops:
  0.0 3.3 %shard_map.110 = bf16[8,64,512]{2,1,0:T(8,128)(2,1)} custom-call(bf16[64,128]{1,0:T(8,128)(2,1)} %refs_0_.2, bf16[64,128]{1,0:T(8,128)(2,1)} %refs_1_.2, bf16[64,128]{1,0:T(8,128)(2,1)} %refs_2_.1, bf16[64,128]{1,0:T(8,128)(2,1)} %bitcast.24), custom_call_target="tpu_custom_call" | custom-call | tf_op jit(solution)/shard_map/pallas_call | solution.py:114
  3.3 35.3 %all_to_all.25.block = bf16[8,64,512]{2,1,0:T(8,128)(2,1)S(1)} all-to-all(bf16[8,64,512]{2,1,0:T(8,128)(2,1)} %shard_map.110), channel_id=1, replica_groups=mesh['rep'=4,'zl'=8,'y'=4,'x'=4,'core'=2] {'zl'}, dimensions={0} | all-to-all | bytes 1048576 | tf_op jit(solution)/shard_map/all_to_all | solution.py:23
  40.5 4.7 %all-to-all-start.1 = ((bf16[32,64,512]{2,1,0:T(8,128)(2,1)}), bf16[32,64,512]{2,1,0:T(8,128)(2,1)S(1)}, u32[]{:S(2)}, u32[]{:S(2)}) async-start(bf16[32,64,512]{2,1,0:T(8,128)(2,1)} %bitcast.22), calls=%async_computation.1 | async-start | bytes 4194304 | tf_op jit(solution)/shard_map/all_to_all | solution.py:23
  50.4 13.7 %all-to-all-done.1 = bf16[32,64,512]{2,1,0:T(8,128)(2,1)S(1)} async-done(((bf16[32,64,512]{2,1,0:T(8,128)(2,1)}), bf16[32,64,512]{2,1,0:T(8,128)(2,1)S(1)}, u32[]{:S(2)}, u32[]{:S(2)}) %all-to-all-start.1) | async-done | bytes 2097184 | tf_op jit(solution)/shard_map/all_to_all | solution.py:23
  65.6 3.4 %shard_map.112 = (bf16[4,64,2048]{2,1,0:T(8,128)(2,1)S(1)}, bf16[4,64,2048]{2,1,0:T(8,128)(2,1)S(1)}) custom-call(s32[3]{0:T(128)S(1)} %shard_map.109.pos, bf16[512,2048]{1,0:T(8,128)(2,1)S(1)} %copy-done, f32[3,128]{1,0:T(4,128)S(1)} %copy-done.4, bf16[4,8,64,512]{3,2,1,0:T(8,128)(2,1)S(1)} %bitcast.12), custom_call_target="tpu_custom_call" | custom-call | tf_op jit(solution)/shard_map/pallas_call | solution.py:43
  69.0 10.3 %collective-permute-start = (bf16[4,64,2048]{2,1,0:T(8,128)(2,1)S(1)}, bf16[4,64,2048]{2,1,0:T(8,128)(2,1)S(1)}, u32[]{:S(2)}, u32[]{:S(2)}) collective-permute-start(bf16[4,64,2048]{2,1,0:T(8,128)(2,1)S(1)} %get-tuple-element.12), channel_id=1, source_target_pairs={{0,1},{1,0},{2,3},{3,2},{4,5},{5,4},{6,7},{7,6},{8,9},{9,8},{10,11... | collective-permute-start | bytes 3145736 | tf_op jit(solution)/shard_map/ppermute | solution.py:219
  79.4 2.3 %collective-permute-done = bf16[4,64,2048]{2,1,0:T(8,128)(2,1)S(1)} collective-permute-done((bf16[4,64,2048]{2,1,0:T(8,128)(2,1)S(1)}, bf16[4,64,2048]{2,1,0:T(8,128)(2,1)S(1)}, u32[]{:S(2)}, u32[]{:S(2)}) %collective-permute-start) | collective-permute-done | bytes 1048608 | tf_op jit(solution)/shard_map/ppermute | solution.py:219
  83.1 4.2 %all-to-all-start.2 = ((bf16[4,64,2048]{2,1,0:T(8,128)(2,1)}), bf16[4,64,2048]{2,1,0:T(8,128)(2,1)S(1)}, u32[]{:S(2)}, u32[]{:S(2)}) async-start(bf16[4,64,2048]{2,1,0:T(8,128)(2,1)} %add_convert_fusion.1), calls=%async_computation.2 | async-start | bytes 2097152 | tf_op jit(solution)/shard_map/all_to_all | solution.py:23
  90.3 4.3 %collective-permute-start.3 = (bf16[64,1152]{1,0:T(8,128)(2,1)S(1)}, bf16[64,1152]{1,0:T(8,128)(2,1)S(1)}, u32[]{:S(2)}, u32[]{:S(2)}) collective-permute-start(bf16[64,1152]{1,0:T(8,128)(2,1)S(1)} %bitcast.18), channel_id=1, source_target_pairs={{8,0},{16,8},{24,16},{0,24},{9,1},{17,9},{25,17},{1,25},{10,2},{18... | collective-permute-start | bytes 442376 | tf_op jit(solution)/shard_map/ppermute | solution.py:19
  98.1 3.9 %collective-permute-done.4.refs_4_ = bf16[64,1152]{1,0:T(8,128)(2,1)S(1)} collective-permute-done((bf16[64,1152]{1,0:T(8,128)(2,1)S(1)}, bf16[64,1152]{1,0:T(8,128)(2,1)S(1)}, u32[]{:S(2)}, u32[]{:S(2)}) %collective-permute-start.4) | collective-permute-done | bytes 147488 | tf_op jit(solution)/shard_map/ppermute | solution.py:19
  102.6 16.1 %collective-permute-start.5 = (bf16[256,1152]{1,0:T(8,128)(2,1)S(1)}, bf16[256,1152]{1,0:T(8,128)(2,1)S(1)}, u32[]{:S(2)}, u32[]{:S(2)}) collective-permute-start(bf16[256,1152]{1,0:T(8,128)(2,1)S(1)} %shard_map.117.refs_2_), channel_id=1, source_target_pairs={{32,0},{64,32},{96,64},{128,96},{160,128},{192,160},{224,192},{256... | collective-permute-start | bytes 1769480 | tf_op jit(solution)/shard_map/ppermute | solution.py:19
  123.7 3.9 %all-to-all-start.3 = ((bf16[4,64,2048]{2,1,0:T(8,128)(2,1)}), bf16[4,64,2048]{2,1,0:T(8,128)(2,1)S(1)}, u32[]{:S(2)}, u32[]{:S(2)}) async-start(bf16[4,64,2048]{2,1,0:T(8,128)(2,1)} %get-tuple-element.13), calls=%async_computation.3 | async-start | bytes 2097152 | tf_op jit(solution)/shard_map/all_to_all | solution.py:23
  129.3 5.3 %collective-permute-start.7 = (bf16[256,1152]{1,0:T(8,128)(2,1)S(1)}, bf16[256,1152]{1,0:T(8,128)(2,1)S(1)}, u32[]{:S(2)}, u32[]{:S(2)}) collective-permute-start(bf16[256,1152]{1,0:T(8,128)(2,1)S(1)} %collective-permute-done.5.refs_3_), channel_id=1, source_target_pairs={{32,0},{64,32},{96,64},{128,96},{160,128},{192,160},{224,192},{256... | collective-permute-start | bytes 1769480 | tf_op jit(solution)/shard_map/ppermute | solution.py:19
  136.5 2.8 %all-to-all-done.3 = bf16[4,64,2048]{2,1,0:T(8,128)(2,1)S(1)} async-done(((bf16[4,64,2048]{2,1,0:T(8,128)(2,1)}), bf16[4,64,2048]{2,1,0:T(8,128)(2,1)S(1)}, u32[]{:S(2)}, u32[]{:S(2)}) %all-to-all-start.3) | async-done | bytes 1048608 | tf_op jit(solution)/shard_map/all_to_all | solution.py:23
  139.3 6.3 %collective-permute-start.1 = (bf16[256,2048]{1,0:T(8,128)(2,1)S(1)}, bf16[256,2048]{1,0:T(8,128)(2,1)S(1)}, u32[]{:S(2)}, u32[]{:S(2)}) collective-permute-start(bf16[256,2048]{1,0:T(8,128)(2,1)S(1)} %bitcast.14), channel_id=1, source_target_pairs={{0,1},{1,0},{2,3},{3,2},{4,5},{5,4},{6,7},{7,6},{8,9},{9,8},{10,11... | collective-permute-start | bytes 3145736 | tf_op jit(solution)/shard_map/ppermute | solution.py:234
  145.6 4.6 %collective-permute-start.9 = (bf16[256,1152]{1,0:T(8,128)(2,1)S(1)}, bf16[256,1152]{1,0:T(8,128)(2,1)S(1)}, u32[]{:S(2)}, u32[]{:S(2)}) collective-permute-start(bf16[256,1152]{1,0:T(8,128)(2,1)S(1)} %collective-permute-done.7.refs_5_), channel_id=1, source_target_pairs={{32,0},{64,32},{96,64},{128,96},{160,128},{192,160},{224,192},{256... | collective-permute-start | bytes 1769480 | tf_op jit(solution)/shard_map/ppermute | solution.py:19
  152.1 7.8 %collective-permute-done.9.refs_7_ = bf16[256,1152]{1,0:T(8,128)(2,1)S(1)} collective-permute-done((bf16[256,1152]{1,0:T(8,128)(2,1)S(1)}, bf16[256,1152]{1,0:T(8,128)(2,1)S(1)}, u32[]{:S(2)}, u32[]{:S(2)}) %collective-permute-start.9) | collective-permute-done | bytes 589856 | tf_op jit(solution)/shard_map/ppermute | solution.py:19
  160.0 5.0 %collective-permute-start.11 = (bf16[128,1152]{1,0:T(8,128)(2,1)S(1)}, bf16[128,1152]{1,0:T(8,128)(2,1)S(1)}, u32[]{:S(2)}, u32[]{:S(2)}) collective-permute-start(bf16[128,1152]{1,0:T(8,128)(2,1)S(1)} %slice.8), channel_id=1, source_target_pairs={{32,0},{64,32},{96,64},{128,96},{160,128},{192,160},{224,192},{256... | collective-permute-start | bytes 884744 | tf_op jit(solution)/shard_map/ppermute | solution.py:19
  169.3 4.4 %collective-permute-done.12.refs_10_ = bf16[128,1152]{1,0:T(8,128)(2,1)S(1)} collective-permute-done((bf16[128,1152]{1,0:T(8,128)(2,1)S(1)}, bf16[128,1152]{1,0:T(8,128)(2,1)S(1)}, u32[]{:S(2)}, u32[]{:S(2)}) %collective-permute-start.12) | collective-permute-done | bytes 294944 | tf_op jit(solution)/shard_map/ppermute | solution.py:19
  173.7 3.4 %shard_map.118 = bf16[256,2048]{1,0:T(8,128)(2,1)S(1)} custom-call(s32[3]{0:T(128)S(1)} %shard_map.115.refs_0_, bf16[256,2048]{1,0:T(8,128)(2,1)S(1)} %bitcast.15, bf16[256,1152]{1,0:T(8,128)(2,1)S(1)} %shard_map.117.refs_2_, bf16[256,1152]{1,0:T(8,128)(2,1)S(1)} %collective-permute-done.5.refs_3_, bf16[256,1152]{1,0:T(8,128)(2,1)S(1)} %collective-permute-done.6.refs_4_, ...), custom_call_target="tpu_custom_call" | custom-call | tf_op jit(solution)/shard_map/pallas_call | solution.py:43
  177.2 3.4 %shard_map.119 = bf16[256,2048]{1,0:T(8,128)(2,1)S(1)} custom-call(s32[3]{0:T(128)S(1)} %shard_map.115.refs_0_, bf16[256,2048]{1,0:T(8,128)(2,1)S(1)} %collective-permute-done.1.refs_1_, bf16[256,1152]{1,0:T(8,128)(2,1)S(1)} %shard_map.117.refs_2_, bf16[256,1152]{1,0:T(8,128)(2,1)S(1)} %collective-permute-done.5.refs_3_, ...), custom_call_target="tpu_custom_call" | custom-call | tf_op jit(solution)/shard_map/pallas_call | solution.py:43
  180.6 7.5 %collective-permute-start.13 = (bf16[4,64,2048]{2,1,0:T(8,128)(2,1)S(1)}, bf16[4,64,2048]{2,1,0:T(8,128)(2,1)S(1)}, u32[]{:S(2)}, u32[]{:S(2)}) collective-permute-start(bf16[4,64,2048]{2,1,0:T(8,128)(2,1)S(1)} %bitcast.16), channel_id=1, source_target_pairs={{0,1},{1,0},{2,3},{3,2},{4,5},{5,4},{6,7},{7,6},{8,9},{9,8},{10,11... | collective-permute-start | bytes 3145736 | tf_op jit(solution)/shard_map/ppermute | solution.py:219
  188.2 2.3 %collective-permute-done.13 = bf16[4,64,2048]{2,1,0:T(8,128)(2,1)S(1)} collective-permute-done((bf16[4,64,2048]{2,1,0:T(8,128)(2,1)S(1)}, bf16[4,64,2048]{2,1,0:T(8,128)(2,1)S(1)}, u32[]{:S(2)}, u32[]{:S(2)}) %collective-permute-start.13) | collective-permute-done | bytes 1048608 | tf_op jit(solution)/shard_map/ppermute | solution.py:219
  190.8 17.2 %all_to_all.26.blocks = bf16[4,64,2048]{2,1,0:T(8,128)(2,1)S(1)} all-to-all(bf16[4,64,2048]{2,1,0:T(8,128)(2,1)S(1)} %add_convert_fusion), channel_id=1, replica_groups=mesh['rep'=4,'zl'=8,'y'=4,'x'=4,'core'=2] {'x'}, dimensions={0} | all-to-all | bytes 2097152 | tf_op jit(solution)/shard_map/all_to_all | solution.py:23
  (47 shorter events, 33.2 us)
Async XLA Ops:
  40.5 23.5 %all-to-all-start.1 = ((bf16[32,64,512]{2,1,0:T(8,128)(2,1)}), bf16[32,64,512]{2,1,0:T(8,128)(2,1)S(1)}, u32[]{:S(2)}, u32[]{:S(2)}) async-start(bf16[32,64,512]{2,1,0:T(8,128)(2,1)} %bitcast.22), calls=%async_computation.1 | async-start | bytes 4194304 | tf_op jit(solution)/shard_map/all_to_all | solution.py:23
  45.2 3.3 %copy-start.6 = (f32[2048]{0:T(1024)S(1)}, f32[2048]{0:T(1024)}, u32[]{:S(2)}) copy-start(f32[2048]{0:T(1024)} %param.12) | copy-start | bytes 24580
  45.2 3.3 %copy-start.5 = (bf16[512,2048]{1,0:T(8,128)(2,1)S(1)}, bf16[512,2048]{1,0:T(8,128)(2,1)}, u32[]{:S(2)}) copy-start(bf16[512,2048]{1,0:T(8,128)(2,1)} %param.11) | copy-start | bytes 6291460
  48.5 15.5 %copy-start.4 = (f32[3,128]{1,0:T(4,128)S(1)}, f32[3,128]{1,0:T(4,128)}, u32[]{:S(2)}) copy-start(f32[3,128]{1,0:T(4,128)} %taps.1) | copy-start | bytes 4612
  64.0 1.6 copy-start
  69.0 12.6 %collective-permute-start = (bf16[4,64,2048]{2,1,0:T(8,128)(2,1)S(1)}, bf16[4,64,2048]{2,1,0:T(8,128)(2,1)S(1)}, u32[]{:S(2)}, u32[]{:S(2)}) collective-permute-start(bf16[4,64,2048]{2,1,0:T(8,128)(2,1)S(1)} %get-tuple-element.12), channel_id=1, source_target_pairs={{0,1},{1,0},{2,3},{3,2},{4,5},{5,4},{6,7},{7,6},{8,9},{9,8},{10,11... | collective-permute-start | bytes 3145736 | tf_op jit(solution)/shard_map/ppermute | solution.py:219
  83.1 38.5 %copy-start.3 = (f32[2048]{0:T(1024)S(1)}, f32[2048]{0:T(1024)}, u32[]{:S(2)}) copy-start(f32[2048]{0:T(1024)} %param.18) | copy-start | bytes 24580
  83.1 38.5 %all-to-all-start.2 = ((bf16[4,64,2048]{2,1,0:T(8,128)(2,1)}), bf16[4,64,2048]{2,1,0:T(8,128)(2,1)S(1)}, u32[]{:S(2)}, u32[]{:S(2)}) async-start(bf16[4,64,2048]{2,1,0:T(8,128)(2,1)} %add_convert_fusion.1), calls=%async_computation.2 | async-start | bytes 2097152 | tf_op jit(solution)/shard_map/all_to_all | solution.py:23
  88.1 8.4 %collective-permute-start.2 = (bf16[64,1152]{1,0:T(8,128)(2,1)S(1)}, bf16[64,1152]{1,0:T(8,128)(2,1)S(1)}, u32[]{:S(2)}, u32[]{:S(2)}) collective-permute-start(bf16[64,1152]{1,0:T(8,128)(2,1)S(1)} %bitcast.17), channel_id=1, source_target_pairs={{16,0},{24,8},{0,16},{8,24},{17,1},{25,9},{1,17},{9,25},{18,2},{26... | collective-permute-start | bytes 442376 | tf_op jit(solution)/shard_map/ppermute | solution.py:19
  90.3 7.8 %collective-permute-start.3 = (bf16[64,1152]{1,0:T(8,128)(2,1)S(1)}, bf16[64,1152]{1,0:T(8,128)(2,1)S(1)}, u32[]{:S(2)}, u32[]{:S(2)}) collective-permute-start(bf16[64,1152]{1,0:T(8,128)(2,1)S(1)} %bitcast.18), channel_id=1, source_target_pairs={{8,0},{16,8},{24,16},{0,24},{9,1},{17,9},{25,17},{1,25},{10,2},{18... | collective-permute-start | bytes 442376 | tf_op jit(solution)/shard_map/ppermute | solution.py:19
  94.6 7.4 %collective-permute-start.4 = (bf16[64,1152]{1,0:T(8,128)(2,1)S(1)}, bf16[64,1152]{1,0:T(8,128)(2,1)S(1)}, u32[]{:S(2)}, u32[]{:S(2)}) collective-permute-start(bf16[64,1152]{1,0:T(8,128)(2,1)S(1)} %bitcast.19), channel_id=1, source_target_pairs={{24,0},{0,8},{8,16},{16,24},{25,1},{1,9},{9,17},{17,25},{26,2},{2,... | collective-permute-start | bytes 442376 | tf_op jit(solution)/shard_map/ppermute | solution.py:19
  102.6 26.7 %collective-permute-start.5 = (bf16[256,1152]{1,0:T(8,128)(2,1)S(1)}, bf16[256,1152]{1,0:T(8,128)(2,1)S(1)}, u32[]{:S(2)}, u32[]{:S(2)}) collective-permute-start(bf16[256,1152]{1,0:T(8,128)(2,1)S(1)} %shard_map.117.refs_2_), channel_id=1, source_target_pairs={{32,0},{64,32},{96,64},{128,96},{160,128},{192,160},{224,192},{256... | collective-permute-start | bytes 1769480 | tf_op jit(solution)/shard_map/ppermute | solution.py:19
  118.7 15.9 %collective-permute-start.6 = (bf16[256,1152]{1,0:T(8,128)(2,1)S(1)}, bf16[256,1152]{1,0:T(8,128)(2,1)S(1)}, u32[]{:S(2)}, u32[]{:S(2)}) collective-permute-start(bf16[256,1152]{1,0:T(8,128)(2,1)S(1)} %shard_map.117.refs_2_), channel_id=1, source_target_pairs={{992,0},{0,32},{32,64},{64,96},{96,128},{128,160},{160,192},{192,2... | collective-permute-start | bytes 1769480 | tf_op jit(solution)/shard_map/ppermute | solution.py:19
  122.9 0.8 copy-start.1
  123.7 15.6 %all-to-all-start.3 = ((bf16[4,64,2048]{2,1,0:T(8,128)(2,1)}), bf16[4,64,2048]{2,1,0:T(8,128)(2,1)S(1)}, u32[]{:S(2)}, u32[]{:S(2)}) async-start(bf16[4,64,2048]{2,1,0:T(8,128)(2,1)} %get-tuple-element.13), calls=%async_computation.3 | async-start | bytes 2097152 | tf_op jit(solution)/shard_map/all_to_all | solution.py:23
  129.3 16.3 %collective-permute-start.7 = (bf16[256,1152]{1,0:T(8,128)(2,1)S(1)}, bf16[256,1152]{1,0:T(8,128)(2,1)S(1)}, u32[]{:S(2)}, u32[]{:S(2)}) collective-permute-start(bf16[256,1152]{1,0:T(8,128)(2,1)S(1)} %collective-permute-done.5.refs_3_), channel_id=1, source_target_pairs={{32,0},{64,32},{96,64},{128,96},{160,128},{192,160},{224,192},{256... | collective-permute-start | bytes 1769480 | tf_op jit(solution)/shard_map/ppermute | solution.py:19
  134.6 15.6 %collective-permute-start.8 = (bf16[256,1152]{1,0:T(8,128)(2,1)S(1)}, bf16[256,1152]{1,0:T(8,128)(2,1)}, u32[]{:S(2)}, u32[]{:S(2)}) collective-permute-start(bf16[256,1152]{1,0:T(8,128)(2,1)S(1)} %collective-permute-done.6.refs_4_), channel_id=1, source_target_pairs={{992,0},{0,32},{32,64},{64,96},{96,128},{128,160},{160,192},{192,2... | collective-permute-start | bytes 1769480 | tf_op jit(solution)/shard_map/ppermute | solution.py:19
  139.3 37.8 %collective-permute-start.1 = (bf16[256,2048]{1,0:T(8,128)(2,1)S(1)}, bf16[256,2048]{1,0:T(8,128)(2,1)S(1)}, u32[]{:S(2)}, u32[]{:S(2)}) collective-permute-start(bf16[256,2048]{1,0:T(8,128)(2,1)S(1)} %bitcast.14), channel_id=1, source_target_pairs={{0,1},{1,0},{2,3},{3,2},{4,5},{5,4},{6,7},{7,6},{8,9},{9,8},{10,11... | collective-permute-start | bytes 3145736 | tf_op jit(solution)/shard_map/ppermute | solution.py:234
  145.6 14.3 %collective-permute-start.9 = (bf16[256,1152]{1,0:T(8,128)(2,1)S(1)}, bf16[256,1152]{1,0:T(8,128)(2,1)S(1)}, u32[]{:S(2)}, u32[]{:S(2)}) collective-permute-start(bf16[256,1152]{1,0:T(8,128)(2,1)S(1)} %collective-permute-done.7.refs_5_), channel_id=1, source_target_pairs={{32,0},{64,32},{96,64},{128,96},{160,128},{192,160},{224,192},{256... | collective-permute-start | bytes 1769480 | tf_op jit(solution)/shard_map/ppermute | solution.py:19
  150.2 14.8 %collective-permute-start.10 = (bf16[256,1152]{1,0:T(8,128)(2,1)}, bf16[256,1152]{1,0:T(8,128)(2,1)S(1)}, u32[]{:S(2)}, u32[]{:S(2)}) collective-permute-start(bf16[256,1152]{1,0:T(8,128)(2,1)} %collective-permute-done.8.refs_6_), channel_id=1, source_target_pairs={{992,0},{0,32},{32,64},{64,96},{96,128},{128,160},{160,192},{192,2... | collective-permute-start | bytes 1769480 | tf_op jit(solution)/shard_map/ppermute | solution.py:19
  160.0 9.3 %collective-permute-start.11 = (bf16[128,1152]{1,0:T(8,128)(2,1)S(1)}, bf16[128,1152]{1,0:T(8,128)(2,1)S(1)}, u32[]{:S(2)}, u32[]{:S(2)}) collective-permute-start(bf16[128,1152]{1,0:T(8,128)(2,1)S(1)} %slice.8), channel_id=1, source_target_pairs={{32,0},{64,32},{96,64},{128,96},{160,128},{192,160},{224,192},{256... | collective-permute-start | bytes 884744 | tf_op jit(solution)/shard_map/ppermute | solution.py:19
  165.0 8.7 %collective-permute-start.12 = (bf16[128,1152]{1,0:T(8,128)(2,1)S(1)}, bf16[128,1152]{1,0:T(8,128)(2,1)S(1)}, u32[]{:S(2)}, u32[]{:S(2)}) collective-permute-start(bf16[128,1152]{1,0:T(8,128)(2,1)S(1)} %slice.9), channel_id=1, source_target_pairs={{992,0},{0,32},{32,64},{64,96},{96,128},{128,160},{160,192},{192,2... | collective-permute-start | bytes 884744 | tf_op jit(solution)/shard_map/ppermute | solution.py:19
  180.6 27.5 %copy-start.2 = (f32[64,2048]{1,0:T(8,128)S(1)}, f32[64,2048]{1,0:T(8,128)}, u32[]{:S(2)}) copy-start(f32[64,2048]{1,0:T(8,128)} %copy-done.1) | copy-start | bytes 1572868
  180.6 9.8 %collective-permute-start.13 = (bf16[4,64,2048]{2,1,0:T(8,128)(2,1)S(1)}, bf16[4,64,2048]{2,1,0:T(8,128)(2,1)S(1)}, u32[]{:S(2)}, u32[]{:S(2)}) collective-permute-start(bf16[4,64,2048]{2,1,0:T(8,128)(2,1)S(1)} %bitcast.16), channel_id=1, source_target_pairs={{0,1},{1,0},{2,3},{3,2},{4,5},{5,4},{6,7},{7,6},{8,9},{9,8},{10,11... | collective-permute-start | bytes 3145736 | tf_op jit(solution)/shard_map/ppermute | solution.py:219

commit v4 on v3

--- a/solution.py
+++ b/solution.py
@@ -35,8 +35,9 @@
     return jnp.dot(acts, weight, preferred_element_type=jnp.float32)
 
 
-def call(kernel, outs, pos, args, mib, scratch=()):
-    args = [pltpu.with_memory_space_constraint(a, pltpu.VMEM) for a in args]
+def call(kernel, outs, pos, args, mib, scratch=(), placed=True):
+    if placed:
+        args = [pltpu.with_memory_space_constraint(a, pltpu.VMEM) for a in args]
     specs = [VMEM] * len(args)
     if pos is not None:
         args, specs = [pos, *args], [SMEM, *specs]
@@ -138,8 +139,8 @@
     out[...] = total.astype(jnp.bfloat16)
 
 
-def ffn_kernel(places, n_ff, pos, acts, *refs):
-    chunks, out = refs[: len(places)], refs[len(places)]
+def ffn_kernel(places, n_ff, pos, acts, acts_other, *refs):
+    chunks, out, out_other = refs[: len(places)], refs[len(places)], refs[len(places) + 1]
     depth = acts.shape[1] // Z_LO
     step = chunks[0].shape[1] // 3
     both = None
@@ -148,12 +149,17 @@
         z = lax.rem(pos[0] + (d + Z_LO), Z_LO)
         first = pl.multiple_of(z * depth + row, chunk.shape[0])
         firsts.append(first)
-        part = dot(acts[:, pl.ds(first, chunk.shape[0])], chunk[:, : 2 * step])
+        columns = pl.ds(first, chunk.shape[0])
+        values = jnp.concatenate([acts[:, columns], acts_other[:, columns]], axis=0)
+        part = dot(values, chunk[:, : 2 * step])
         both = part if both is None else both + part
     hidden = (jax.nn.silu(both[:, :n_ff]) * both[:, step : step + n_ff]).astype(jnp.bfloat16)
+    half = acts.shape[0]
     for first, chunk in zip(firsts, chunks):
-        part = dot_t(hidden, chunk[:, 2 * step : 2 * step + n_ff])
-        out[:, pl.ds(first, chunk.shape[0])] = part.astype(jnp.bfloat16)
+        part = dot_t(hidden, chunk[:, 2 * step : 2 * step + n_ff]).astype(jnp.bfloat16)
+        columns = pl.ds(first, chunk.shape[0])
+        out[:, columns] = part[:half]
+        out_other[:, columns] = part[half:]
 
 
 def local(
@@ -177,9 +183,9 @@
     half_rows = count // 2
     own_rows = half_rows // nx
 
-    parts = (w_gate_b, w_gate_c, w_conv_in, w_mix_out.T)
-    mixer_shape = (w_gate_b.shape[0], sum(part.shape[1] for part in parts))
-    sent = for_exchange(bundle_kernel, parts, Z_LO, mixer_shape, w_gate_b.dtype)
+    mixer = jnp.concatenate([w_gate_b, w_gate_c, w_conv_in, w_mix_out.T], axis=1)
+    mixer_shape = mixer.shape
+    sent = jnp.broadcast_to(mixer[None], (Z_LO, *mixer_shape))
     along_z = exchange(sent, "zl")
     sent = for_exchange(copy_kernel, (along_z,), ny, along_z.shape, along_z.dtype, source=pltpu.VMEM)
     normed = rms_scale(tokens.astype(jnp.float32), mix_gain).astype(jnp.bfloat16)
@@ -197,7 +203,7 @@
     def ordered_body(*refs):
         ordered_kernel(y_places, *refs)
 
-    (ffn_y,) = call(ordered_body, (jax.ShapeDtypeStruct((ny * ffn_shape[0], width), ffn.dtype),), pos, blocks, 4)
+    (ffn_y,) = call(ordered_body, (jax.ShapeDtypeStruct((ny * ffn_shape[0], width), ffn.dtype),), pos, blocks, 4, placed=False)
     chunks, ffn_places = [ffn_y], [(0, 0)]
     up = down = ffn_y
     for k in (1, 2, 3):
@@ -236,13 +242,8 @@
     def ffn_body(*refs):
         ffn_kernel(ffn_places, n_ff, *refs)
 
-    def feed_forward(values):
-        (out,) = call(ffn_body, (pltpu.VMEM((half_rows, feats), bf),), pos, (values, *chunks), 12)
-        return out.reshape(nx, own_rows, feats)
-
-    ffn_mine = feed_forward(acts)
-    acts_other, ffn_mine = lax.optimization_barrier((acts_other, ffn_mine))
-    blocks = over_tp(ffn_mine, feed_forward(acts_other))
+    pair = call(ffn_body, (pltpu.VMEM((half_rows, feats), bf),) * 2, pos, (acts, acts_other, *chunks), 24)
+    blocks = over_tp(*(part.reshape(halves) for part in pair))
     return call(last_kernel, (jax.ShapeDtypeStruct((own_rows, feats), bf),), None, (blocks, stream), 8)[0]
 
 

time: 210 us -> 206 us (0.981)
  Pallas kernels: 22.6 us -> 18 us
    pallas_call x3 -> x2, Pallas kernels: 6.09 us -> 2.74 us  [for_exchange(): pl.pallas_call(kernel, grid=(count,), out_shape=space((count, *shape), dt...]
    pallas_call x6 -> x5, Pallas kernels: 13.1 us -> 11.8 us  [call(): pl.pallas_call(kernel, out_shape=outs, in_specs=specs, out_specs=(VMEM,)...]
  transfers between devices with their start and end apart: 17 -> 17, of which waited for: 9 -> 9; matrix products, arithmetic and copies ran while one was open for 2% -> 2% of each run, Pallas kernels for 5% -> 3%
where the time goes in v4:
time: 206 us; the launch traced here: 205 us
  starting transfers between devices  83.8 us (41%)
  blocking collectives  52.3 us (25%)
  waiting for transfers between devices  40.6 us (20%)
  Pallas kernels  18 us (9%)
  other arithmetic  6.57 us (3%)
  local copies, waits for them, and re-layouts  3.48 us (2%)
    all_to_all x2, blocking collectives, exchange(): return lax.all_to_all(blocks, axis, 0, 0, tiled=True)  52.3 us
    ppermute x11, starting transfers between devices, shift(): lax.ppermute(value, axis, [((k + distance) % size, k) for k in range(size)])  47 us
    ppermute x11, waiting for transfers between devices, shift(): lax.ppermute(value, axis, [((k + distance) % size, k) for k in range(size)])  19.5 us
    ppermute x2, starting transfers between devices, over_tp(): got = lax.ppermute(other, 'core', SWAP)  17.8 us
    all_to_all x3, waiting for transfers between devices, exchange(): return lax.all_to_all(blocks, axis, 0, 0, tiled=True)  16.5 us
    all_to_all x3, starting transfers between devices, exchange(): return lax.all_to_all(blocks, axis, 0, 0, tiled=True)  12.7 us
    pallas_call x5, Pallas kernels, call(): pl.pallas_call(kernel, out_shape=outs, in_specs=specs, out_specs=(VMEM,)...  11.8 us
    ppermute x1, starting transfers between devices, local(): acts_other = lax.ppermute(acts, 'core', SWAP)  6.25 us
  transfers between devices with their start and end apart: 17, of which 9 were waited for; matrix products, arithmetic and copies ran while one was open for 2% of the time, Pallas kernels for 3%

profile of v4, /device:TPU:1, one launch (start us, length us, event | category | flops | bytes accessed | tf_op | source)
XLA Modules:
  0.0 205.0 jit_solution(12492751855777884020)
XLA Ops:
  0.8 35.1 %all_to_all.25.block = bf16[8,64,512]{2,1,0:T(8,128)(2,1)S(1)} all-to-all(bf16[8,64,512]{2,1,0:T(8,128)(2,1)S(1)} %broadcast_in_dim.2), channel_id=1, replica_groups=mesh['rep'=4,'zl'=8,'y'=4,'x'=4,'core'=2] {'zl'}, dimensions={0} | all-to-all | bytes 1048576 | tf_op jit(solution)/shard_map/all_to_all | solution.py:23
  37.8 4.7 %all-to-all-start.1 = ((bf16[32,64,512]{2,1,0:T(8,128)(2,1)}), bf16[32,64,512]{2,1,0:T(8,128)(2,1)S(1)}, u32[]{:S(2)}, u32[]{:S(2)}) async-start(bf16[32,64,512]{2,1,0:T(8,128)(2,1)} %bitcast.23), calls=%async_computation.1 | async-start | bytes 4194304 | tf_op jit(solution)/shard_map/all_to_all | solution.py:23
  43.7 2.1 %fusion = f32[512]{0:T(512)S(1)} fusion(bf16[512,2048]{1,0:T(8,128)(2,1)} %param.11), kind=kLoop, calls=%fused_computation.2 | loop fusion | flops 3145216 | bytes 2099200 | tf_op jit(solution)/shard_map/reduce_sum | solution.py:27
  47.6 13.7 %all-to-all-done.1 = bf16[32,64,512]{2,1,0:T(8,128)(2,1)S(1)} async-done(((bf16[32,64,512]{2,1,0:T(8,128)(2,1)}), bf16[32,64,512]{2,1,0:T(8,128)(2,1)S(1)}, u32[]{:S(2)}, u32[]{:S(2)}) %all-to-all-start.1) | async-done | bytes 2097184 | tf_op jit(solution)/shard_map/all_to_all | solution.py:23
  62.9 3.4 %shard_map.113 = (bf16[4,64,2048]{2,1,0:T(8,128)(2,1)S(1)}, bf16[4,64,2048]{2,1,0:T(8,128)(2,1)S(1)}) custom-call(s32[3]{0:T(128)S(1)} %shard_map.109.pos, bf16[512,2048]{1,0:T(8,128)(2,1)S(1)} %copy-done, f32[3,128]{1,0:T(4,128)S(1)} %copy-done.4, bf16[4,8,64,512]{3,2,1,0:T(8,128)(2,1)S(1)} %bitcast.13), custom_call_target="tpu_custom_call" | custom-call | tf_op jit(solution)/shard_map/pallas_call | solution.py:44
  66.3 10.3 %collective-permute-start = (bf16[4,64,2048]{2,1,0:T(8,128)(2,1)S(1)}, bf16[4,64,2048]{2,1,0:T(8,128)(2,1)S(1)}, u32[]{:S(2)}, u32[]{:S(2)}) collective-permute-start(bf16[4,64,2048]{2,1,0:T(8,128)(2,1)S(1)} %get-tuple-element.12), channel_id=1, source_target_pairs={{0,1},{1,0},{2,3},{3,2},{4,5},{5,4},{6,7},{7,6},{8,9},{9,8},{10,11... | collective-permute-start | bytes 3145736 | tf_op jit(solution)/shard_map/ppermute | solution.py:225
  76.7 2.3 %collective-permute-done = bf16[4,64,2048]{2,1,0:T(8,128)(2,1)S(1)} collective-permute-done((bf16[4,64,2048]{2,1,0:T(8,128)(2,1)S(1)}, bf16[4,64,2048]{2,1,0:T(8,128)(2,1)S(1)}, u32[]{:S(2)}, u32[]{:S(2)}) %collective-permute-start) | collective-permute-done | bytes 1048608 | tf_op jit(solution)/shard_map/ppermute | solution.py:225
  80.3 4.1 %all-to-all-start.2 = ((bf16[4,64,2048]{2,1,0:T(8,128)(2,1)}), bf16[4,64,2048]{2,1,0:T(8,128)(2,1)S(1)}, u32[]{:S(2)}, u32[]{:S(2)}) async-start(bf16[4,64,2048]{2,1,0:T(8,128)(2,1)} %add_convert_fusion), calls=%async_computation.2 | async-start | bytes 2097152 | tf_op jit(solution)/shard_map/all_to_all | solution.py:23
  85.3 2.2 %collective-permute-start.2 = (bf16[64,1152]{1,0:T(8,128)(2,1)S(1)}, bf16[64,1152]{1,0:T(8,128)(2,1)S(1)}, u32[]{:S(2)}, u32[]{:S(2)}) collective-permute-start(bf16[64,1152]{1,0:T(8,128)(2,1)S(1)} %bitcast.17), channel_id=1, source_target_pairs={{16,0},{24,8},{0,16},{8,24},{17,1},{25,9},{1,17},{9,25},{18,2},{26... | collective-permute-start | bytes 442376 | tf_op jit(solution)/shard_map/ppermute | solution.py:19
  87.6 4.3 %collective-permute-start.3 = (bf16[64,1152]{1,0:T(8,128)(2,1)S(1)}, bf16[64,1152]{1,0:T(8,128)(2,1)S(1)}, u32[]{:S(2)}, u32[]{:S(2)}) collective-permute-start(bf16[64,1152]{1,0:T(8,128)(2,1)S(1)} %bitcast.18), channel_id=1, source_target_pairs={{8,0},{16,8},{24,16},{0,24},{9,1},{17,9},{25,17},{1,25},{10,2},{18... | collective-permute-start | bytes 442376 | tf_op jit(solution)/shard_map/ppermute | solution.py:19
  95.3 3.9 %collective-permute-done.4.refs_4_ = bf16[64,1152]{1,0:T(8,128)(2,1)S(1)} collective-permute-done((bf16[64,1152]{1,0:T(8,128)(2,1)S(1)}, bf16[64,1152]{1,0:T(8,128)(2,1)S(1)}, u32[]{:S(2)}, u32[]{:S(2)}) %collective-permute-start.4) | collective-permute-done | bytes 147488 | tf_op jit(solution)/shard_map/ppermute | solution.py:19
  99.8 16.1 %collective-permute-start.5 = (bf16[256,1152]{1,0:T(8,128)(2,1)S(1)}, bf16[256,1152]{1,0:T(8,128)(2,1)S(1)}, u32[]{:S(2)}, u32[]{:S(2)}) collective-permute-start(bf16[256,1152]{1,0:T(8,128)(2,1)S(1)} %shard_map.116.refs_3_), channel_id=1, source_target_pairs={{32,0},{64,32},{96,64},{128,96},{160,128},{192,160},{224,192},{256... | collective-permute-start | bytes 1769480 | tf_op jit(solution)/shard_map/ppermute | solution.py:19
  121.0 3.9 %all-to-all-start.3 = ((bf16[4,64,2048]{2,1,0:T(8,128)(2,1)}), bf16[4,64,2048]{2,1,0:T(8,128)(2,1)S(1)}, u32[]{:S(2)}, u32[]{:S(2)}) async-start(bf16[4,64,2048]{2,1,0:T(8,128)(2,1)} %get-tuple-element.13), calls=%async_computation.3 | async-start | bytes 2097152 | tf_op jit(solution)/shard_map/all_to_all | solution.py:23
  126.5 5.3 %collective-permute-start.7 = (bf16[256,1152]{1,0:T(8,128)(2,1)S(1)}, bf16[256,1152]{1,0:T(8,128)(2,1)}, u32[]{:S(2)}, u32[]{:S(2)}) collective-permute-start(bf16[256,1152]{1,0:T(8,128)(2,1)S(1)} %collective-permute-done.5.refs_4_), channel_id=1, source_target_pairs={{32,0},{64,32},{96,64},{128,96},{160,128},{192,160},{224,192},{256... | collective-permute-start | bytes 1769480 | tf_op jit(solution)/shard_map/ppermute | solution.py:19
  133.8 2.8 %all-to-all-done.3 = bf16[4,64,2048]{2,1,0:T(8,128)(2,1)S(1)} async-done(((bf16[4,64,2048]{2,1,0:T(8,128)(2,1)}), bf16[4,64,2048]{2,1,0:T(8,128)(2,1)S(1)}, u32[]{:S(2)}, u32[]{:S(2)}) %all-to-all-start.3) | async-done | bytes 1048608 | tf_op jit(solution)/shard_map/all_to_all | solution.py:23
  136.6 6.3 %collective-permute-start.1 = (bf16[256,2048]{1,0:T(8,128)(2,1)S(1)}, bf16[256,2048]{1,0:T(8,128)(2,1)S(1)}, u32[]{:S(2)}, u32[]{:S(2)}) collective-permute-start(bf16[256,2048]{1,0:T(8,128)(2,1)S(1)} %bitcast.14), channel_id=1, source_target_pairs={{0,1},{1,0},{2,3},{3,2},{4,5},{5,4},{6,7},{7,6},{8,9},{9,8},{10,11... | collective-permute-start | bytes 3145736 | tf_op jit(solution)/shard_map/ppermute | solution.py:240
  142.9 4.6 %collective-permute-start.9 = (bf16[256,1152]{1,0:T(8,128)(2,1)}, bf16[256,1152]{1,0:T(8,128)(2,1)S(1)}, u32[]{:S(2)}, u32[]{:S(2)}) collective-permute-start(bf16[256,1152]{1,0:T(8,128)(2,1)} %collective-permute-done.7.refs_6_), channel_id=1, source_target_pairs={{32,0},{64,32},{96,64},{128,96},{160,128},{192,160},{224,192},{256... | collective-permute-start | bytes 1769480 | tf_op jit(solution)/shard_map/ppermute | solution.py:19
  149.4 8.0 %collective-permute-done.9.refs_8_ = bf16[256,1152]{1,0:T(8,128)(2,1)S(1)} collective-permute-done((bf16[256,1152]{1,0:T(8,128)(2,1)}, bf16[256,1152]{1,0:T(8,128)(2,1)S(1)}, u32[]{:S(2)}, u32[]{:S(2)}) %collective-permute-start.9) | collective-permute-done | bytes 589856 | tf_op jit(solution)/shard_map/ppermute | solution.py:19
  157.5 4.9 %collective-permute-start.11 = (bf16[128,1152]{1,0:T(8,128)(2,1)S(1)}, bf16[128,1152]{1,0:T(8,128)(2,1)S(1)}, u32[]{:S(2)}, u32[]{:S(2)}) collective-permute-start(bf16[128,1152]{1,0:T(8,128)(2,1)S(1)} %slice.8), channel_id=1, source_target_pairs={{32,0},{64,32},{96,64},{128,96},{160,128},{192,160},{224,192},{256... | collective-permute-start | bytes 884744 | tf_op jit(solution)/shard_map/ppermute | solution.py:19
  166.7 4.4 %collective-permute-done.12.refs_11_ = bf16[128,1152]{1,0:T(8,128)(2,1)S(1)} collective-permute-done((bf16[128,1152]{1,0:T(8,128)(2,1)S(1)}, bf16[128,1152]{1,0:T(8,128)(2,1)S(1)}, u32[]{:S(2)}, u32[]{:S(2)}) %collective-permute-start.12) | collective-permute-done | bytes 294944 | tf_op jit(solution)/shard_map/ppermute | solution.py:19
  171.1 5.6 %shard_map.117 = (bf16[256,2048]{1,0:T(8,128)(2,1)S(1)}, bf16[256,2048]{1,0:T(8,128)(2,1)S(1)}) custom-call(s32[3]{0:T(128)S(1)} %shard_map.111.refs_0_, bf16[256,2048]{1,0:T(8,128)(2,1)S(1)} %bitcast.15, bf16[256,2048]{1,0:T(8,128)(2,1)S(1)} %collective-permute-done.1.refs_2_, bf16[256,1152]{1,0:T(8,128)(2,1)S(1)} %shard_map.116.refs_3_, ...), custom_call_target="tpu_custom_call" | custom-call | tf_op jit(solution)/shard_map/pallas_call | solution.py:44
  176.8 7.5 %collective-permute-start.13 = (bf16[4,64,2048]{2,1,0:T(8,128)(2,1)S(1)}, bf16[4,64,2048]{2,1,0:T(8,128)(2,1)S(1)}, u32[]{:S(2)}, u32[]{:S(2)}) collective-permute-start(bf16[4,64,2048]{2,1,0:T(8,128)(2,1)S(1)} %bitcast.22), channel_id=1, source_target_pairs={{0,1},{1,0},{2,3},{3,2},{4,5},{5,4},{6,7},{7,6},{8,9},{9,8},{10,11... | collective-permute-start | bytes 3145736 | tf_op jit(solution)/shard_map/ppermute | solution.py:225
  184.3 2.3 %collective-permute-done.13 = bf16[4,64,2048]{2,1,0:T(8,128)(2,1)S(1)} collective-permute-done((bf16[4,64,2048]{2,1,0:T(8,128)(2,1)S(1)}, bf16[4,64,2048]{2,1,0:T(8,128)(2,1)S(1)}, u32[]{:S(2)}, u32[]{:S(2)}) %collective-permute-start.13) | collective-permute-done | bytes 1048608 | tf_op jit(solution)/shard_map/ppermute | solution.py:225
  186.9 17.2 %all_to_all.26.blocks = bf16[4,64,2048]{2,1,0:T(8,128)(2,1)S(1)} all-to-all(bf16[4,64,2048]{2,1,0:T(8,128)(2,1)S(1)} %fusion.3), channel_id=1, replica_groups=mesh['rep'=4,'zl'=8,'y'=4,'x'=4,'core'=2] {'x'}, dimensions={0} | all-to-all | bytes 2097152 | tf_op jit(solution)/shard_map/all_to_all | solution.py:23
  (47 shorter events, 29.7 us)
Async XLA Ops:
  37.8 23.5 %all-to-all-start.1 = ((bf16[32,64,512]{2,1,0:T(8,128)(2,1)}), bf16[32,64,512]{2,1,0:T(8,128)(2,1)S(1)}, u32[]{:S(2)}, u32[]{:S(2)}) async-start(bf16[32,64,512]{2,1,0:T(8,128)(2,1)} %bitcast.23), calls=%async_computation.1 | async-start | bytes 4194304 | tf_op jit(solution)/shard_map/all_to_all | solution.py:23
  42.4 3.3 %copy-start.6 = (f32[2048]{0:T(1024)S(1)}, f32[2048]{0:T(1024)}, u32[]{:S(2)}) copy-start(f32[2048]{0:T(1024)} %param.12) | copy-start | bytes 24580
  42.4 3.3 %copy-start.5 = (bf16[512,2048]{1,0:T(8,128)(2,1)S(1)}, bf16[512,2048]{1,0:T(8,128)(2,1)}, u32[]{:S(2)}) copy-start(bf16[512,2048]{1,0:T(8,128)(2,1)} %param.11) | copy-start | bytes 6291460
  45.8 15.5 %copy-start.4 = (f32[3,128]{1,0:T(4,128)S(1)}, f32[3,128]{1,0:T(4,128)}, u32[]{:S(2)}) copy-start(f32[3,128]{1,0:T(4,128)} %taps.1) | copy-start | bytes 4612
  61.3 1.6 copy-start
  66.3 12.6 %collective-permute-start = (bf16[4,64,2048]{2,1,0:T(8,128)(2,1)S(1)}, bf16[4,64,2048]{2,1,0:T(8,128)(2,1)S(1)}, u32[]{:S(2)}, u32[]{:S(2)}) collective-permute-start(bf16[4,64,2048]{2,1,0:T(8,128)(2,1)S(1)} %get-tuple-element.12), channel_id=1, source_target_pairs={{0,1},{1,0},{2,3},{3,2},{4,5},{5,4},{6,7},{7,6},{8,9},{9,8},{10,11... | collective-permute-start | bytes 3145736 | tf_op jit(solution)/shard_map/ppermute | solution.py:225
  80.3 38.5 %copy-start.3 = (f32[2048]{0:T(1024)S(1)}, f32[2048]{0:T(1024)}, u32[]{:S(2)}) copy-start(f32[2048]{0:T(1024)} %param.18) | copy-start | bytes 24580
  80.3 38.5 %all-to-all-start.2 = ((bf16[4,64,2048]{2,1,0:T(8,128)(2,1)}), bf16[4,64,2048]{2,1,0:T(8,128)(2,1)S(1)}, u32[]{:S(2)}, u32[]{:S(2)}) async-start(bf16[4,64,2048]{2,1,0:T(8,128)(2,1)} %add_convert_fusion), calls=%async_computation.2 | async-start | bytes 2097152 | tf_op jit(solution)/shard_map/all_to_all | solution.py:23
  85.3 8.4 %collective-permute-start.2 = (bf16[64,1152]{1,0:T(8,128)(2,1)S(1)}, bf16[64,1152]{1,0:T(8,128)(2,1)S(1)}, u32[]{:S(2)}, u32[]{:S(2)}) collective-permute-start(bf16[64,1152]{1,0:T(8,128)(2,1)S(1)} %bitcast.17), channel_id=1, source_target_pairs={{16,0},{24,8},{0,16},{8,24},{17,1},{25,9},{1,17},{9,25},{18,2},{26... | collective-permute-start | bytes 442376 | tf_op jit(solution)/shard_map/ppermute | solution.py:19
  87.6 7.8 %collective-permute-start.3 = (bf16[64,1152]{1,0:T(8,128)(2,1)S(1)}, bf16[64,1152]{1,0:T(8,128)(2,1)S(1)}, u32[]{:S(2)}, u32[]{:S(2)}) collective-permute-start(bf16[64,1152]{1,0:T(8,128)(2,1)S(1)} %bitcast.18), channel_id=1, source_target_pairs={{8,0},{16,8},{24,16},{0,24},{9,1},{17,9},{25,17},{1,25},{10,2},{18... | collective-permute-start | bytes 442376 | tf_op jit(solution)/shard_map/ppermute | solution.py:19
  91.8 7.4 %collective-permute-start.4 = (bf16[64,1152]{1,0:T(8,128)(2,1)S(1)}, bf16[64,1152]{1,0:T(8,128)(2,1)S(1)}, u32[]{:S(2)}, u32[]{:S(2)}) collective-permute-start(bf16[64,1152]{1,0:T(8,128)(2,1)S(1)} %bitcast.19), channel_id=1, source_target_pairs={{24,0},{0,8},{8,16},{16,24},{25,1},{1,9},{9,17},{17,25},{26,2},{2,... | collective-permute-start | bytes 442376 | tf_op jit(solution)/shard_map/ppermute | solution.py:19
  99.8 26.7 %collective-permute-start.5 = (bf16[256,1152]{1,0:T(8,128)(2,1)S(1)}, bf16[256,1152]{1,0:T(8,128)(2,1)S(1)}, u32[]{:S(2)}, u32[]{:S(2)}) collective-permute-start(bf16[256,1152]{1,0:T(8,128)(2,1)S(1)} %shard_map.116.refs_3_), channel_id=1, source_target_pairs={{32,0},{64,32},{96,64},{128,96},{160,128},{192,160},{224,192},{256... | collective-permute-start | bytes 1769480 | tf_op jit(solution)/shard_map/ppermute | solution.py:19
  115.9 15.9 %collective-permute-start.6 = (bf16[256,1152]{1,0:T(8,128)(2,1)S(1)}, bf16[256,1152]{1,0:T(8,128)(2,1)S(1)}, u32[]{:S(2)}, u32[]{:S(2)}) collective-permute-start(bf16[256,1152]{1,0:T(8,128)(2,1)S(1)} %shard_map.116.refs_3_), channel_id=1, source_target_pairs={{992,0},{0,32},{32,64},{64,96},{96,128},{128,160},{160,192},{192,2... | collective-permute-start | bytes 1769480 | tf_op jit(solution)/shard_map/ppermute | solution.py:19
  120.2 0.8 copy-start.1
  121.0 15.6 %all-to-all-start.3 = ((bf16[4,64,2048]{2,1,0:T(8,128)(2,1)}), bf16[4,64,2048]{2,1,0:T(8,128)(2,1)S(1)}, u32[]{:S(2)}, u32[]{:S(2)}) async-start(bf16[4,64,2048]{2,1,0:T(8,128)(2,1)} %get-tuple-element.13), calls=%async_computation.3 | async-start | bytes 2097152 | tf_op jit(solution)/shard_map/all_to_all | solution.py:23
  126.5 16.4 %collective-permute-start.7 = (bf16[256,1152]{1,0:T(8,128)(2,1)S(1)}, bf16[256,1152]{1,0:T(8,128)(2,1)}, u32[]{:S(2)}, u32[]{:S(2)}) collective-permute-start(bf16[256,1152]{1,0:T(8,128)(2,1)S(1)} %collective-permute-done.5.refs_4_), channel_id=1, source_target_pairs={{32,0},{64,32},{96,64},{128,96},{160,128},{192,160},{224,192},{256... | collective-permute-start | bytes 1769480 | tf_op jit(solution)/shard_map/ppermute | solution.py:19
  131.9 15.6 %collective-permute-start.8 = (bf16[256,1152]{1,0:T(8,128)(2,1)S(1)}, bf16[256,1152]{1,0:T(8,128)(2,1)}, u32[]{:S(2)}, u32[]{:S(2)}) collective-permute-start(bf16[256,1152]{1,0:T(8,128)(2,1)S(1)} %collective-permute-done.6.refs_5_), channel_id=1, source_target_pairs={{992,0},{0,32},{32,64},{64,96},{96,128},{128,160},{160,192},{192,2... | collective-permute-start | bytes 1769480 | tf_op jit(solution)/shard_map/ppermute | solution.py:19
  136.6 34.5 %collective-permute-start.1 = (bf16[256,2048]{1,0:T(8,128)(2,1)S(1)}, bf16[256,2048]{1,0:T(8,128)(2,1)S(1)}, u32[]{:S(2)}, u32[]{:S(2)}) collective-permute-start(bf16[256,2048]{1,0:T(8,128)(2,1)S(1)} %bitcast.14), channel_id=1, source_target_pairs={{0,1},{1,0},{2,3},{3,2},{4,5},{5,4},{6,7},{7,6},{8,9},{9,8},{10,11... | collective-permute-start | bytes 3145736 | tf_op jit(solution)/shard_map/ppermute | solution.py:240
  142.9 14.5 %collective-permute-start.9 = (bf16[256,1152]{1,0:T(8,128)(2,1)}, bf16[256,1152]{1,0:T(8,128)(2,1)S(1)}, u32[]{:S(2)}, u32[]{:S(2)}) collective-permute-start(bf16[256,1152]{1,0:T(8,128)(2,1)} %collective-permute-done.7.refs_6_), channel_id=1, source_target_pairs={{32,0},{64,32},{96,64},{128,96},{160,128},{192,160},{224,192},{256... | collective-permute-start | bytes 1769480 | tf_op jit(solution)/shard_map/ppermute | solution.py:19
  147.5 14.9 %collective-permute-start.10 = (bf16[256,1152]{1,0:T(8,128)(2,1)}, bf16[256,1152]{1,0:T(8,128)(2,1)S(1)}, u32[]{:S(2)}, u32[]{:S(2)}) collective-permute-start(bf16[256,1152]{1,0:T(8,128)(2,1)} %collective-permute-done.8.refs_7_), channel_id=1, source_target_pairs={{992,0},{0,32},{32,64},{64,96},{96,128},{128,160},{160,192},{192,2... | collective-permute-start | bytes 1769480 | tf_op jit(solution)/shard_map/ppermute | solution.py:19
  157.5 9.2 %collective-permute-start.11 = (bf16[128,1152]{1,0:T(8,128)(2,1)S(1)}, bf16[128,1152]{1,0:T(8,128)(2,1)S(1)}, u32[]{:S(2)}, u32[]{:S(2)}) collective-permute-start(bf16[128,1152]{1,0:T(8,128)(2,1)S(1)} %slice.8), channel_id=1, source_target_pairs={{32,0},{64,32},{96,64},{128,96},{160,128},{192,160},{224,192},{256... | collective-permute-start | bytes 884744 | tf_op jit(solution)/shard_map/ppermute | solution.py:19
  162.4 8.7 %collective-permute-start.12 = (bf16[128,1152]{1,0:T(8,128)(2,1)S(1)}, bf16[128,1152]{1,0:T(8,128)(2,1)S(1)}, u32[]{:S(2)}, u32[]{:S(2)}) collective-permute-start(bf16[128,1152]{1,0:T(8,128)(2,1)S(1)} %slice.9), channel_id=1, source_target_pairs={{992,0},{0,32},{32,64},{64,96},{96,128},{128,160},{160,192},{192,2... | collective-permute-start | bytes 884744 | tf_op jit(solution)/shard_map/ppermute | solution.py:19
  176.8 9.8 %collective-permute-start.13 = (bf16[4,64,2048]{2,1,0:T(8,128)(2,1)S(1)}, bf16[4,64,2048]{2,1,0:T(8,128)(2,1)S(1)}, u32[]{:S(2)}, u32[]{:S(2)}) collective-permute-start(bf16[4,64,2048]{2,1,0:T(8,128)(2,1)S(1)} %bitcast.22), channel_id=1, source_target_pairs={{0,1},{1,0},{2,3},{3,2},{4,5},{5,4},{6,7},{7,6},{8,9},{9,8},{10,11... | collective-permute-start | bytes 3145736 | tf_op jit(solution)/shard_map/ppermute | solution.py:225
  186.5 17.6 %copy-start.2 = (f32[64,2048]{1,0:T(8,128)S(1)}, f32[64,2048]{1,0:T(8,128)}, u32[]{:S(2)}) copy-start(f32[64,2048]{1,0:T(8,128)} %copy-done.1) | copy-start | bytes 1572868

commit v5 on v4

--- a/solution.py
+++ b/solution.py
@@ -12,6 +12,7 @@
 SWAP = [(0, 1), (1, 0)]
 
 VMEM = pl.BlockSpec(memory_space=pltpu.VMEM)
+ANY = pl.BlockSpec(memory_space=pl.ANY)
 SMEM = pl.BlockSpec(memory_space=pltpu.SMEM)
 
 
@@ -35,10 +36,10 @@
     return jnp.dot(acts, weight, preferred_element_type=jnp.float32)
 
 
-def call(kernel, outs, pos, args, mib, scratch=(), placed=True):
-    if placed:
-        args = [pltpu.with_memory_space_constraint(a, pltpu.VMEM) for a in args]
-    specs = [VMEM] * len(args)
+def call(kernel, outs, pos, args, mib, scratch=(), far=()):
+    args = [pltpu.with_memory_space_constraint(a, pltpu.VMEM) for a in args]
+    specs = [VMEM] * len(args) + [ANY] * len(far)
+    args += [pltpu.with_memory_space_constraint(a, pltpu.HBM) for a in far]
     if pos is not None:
         args, specs = [pos, *args], [SMEM, *specs]
     return pl.pallas_call(
@@ -51,14 +52,19 @@
     )(*args)
 
 
-def mixer_kernel(pos, normed, taps, gathered, mine, other, weights, gated):
+def mixer_kernel(pos, normed, taps, gathered, mine, other, weights, gated, sems):
     core = pos[1]
     n_y, n_z, rows, _ = gathered.shape
+    fetches = [
+        pltpu.make_async_copy(gathered.at[y, z], weights.at[pl.ds((z * n_y + y) * rows, rows)], sems.at[y, z])
+        for y in range(n_y)
+        for z in range(n_z)
+    ]
+    for fetch in fetches:
+        fetch.start()
+    for fetch in fetches:
+        fetch.wait()
     width = taps.shape[1]
-    for z in range(n_z):
-        for y in range(n_y):
-            first = (z * n_y + y) * rows
-            weights[first : first + rows, :] = gathered[y, z]
     products = dot(normed[...], weights[:, : 3 * width])
     p = products[:, width : 2 * width] * products[:, 2 * width : 3 * width]
     place = lax.broadcasted_iota(jnp.int32, p.shape, 0) % LEN
@@ -140,22 +146,28 @@
 
 
 def ffn_kernel(places, n_ff, pos, acts, acts_other, *refs):
-    chunks, out, out_other = refs[: len(places)], refs[len(places)], refs[len(places) + 1]
+    count = len(places)
+    chunks, (out, out_other, *rest) = refs[:count], refs[count:]
+    weights, sems = rest[:count], rest[count]
     depth = acts.shape[1] // Z_LO
     step = chunks[0].shape[1] // 3
+    fetches = [pltpu.make_async_copy(chunks[k], weights[k], sems.at[k]) for k in range(count)]
+    for fetch in fetches:
+        fetch.start()
     both = None
     firsts = []
-    for (d, row), chunk in zip(places, chunks):
+    for (d, row), chunk, fetch in zip(places, weights, fetches):
         z = lax.rem(pos[0] + (d + Z_LO), Z_LO)
         first = pl.multiple_of(z * depth + row, chunk.shape[0])
         firsts.append(first)
         columns = pl.ds(first, chunk.shape[0])
         values = jnp.concatenate([acts[:, columns], acts_other[:, columns]], axis=0)
+        fetch.wait()
         part = dot(values, chunk[:, : 2 * step])
         both = part if both is None else both + part
     hidden = (jax.nn.silu(both[:, :n_ff]) * both[:, step : step + n_ff]).astype(jnp.bfloat16)
     half = acts.shape[0]
-    for first, chunk in zip(firsts, chunks):
+    for first, chunk in zip(firsts, weights):
         part = dot_t(hidden, chunk[:, 2 * step : 2 * step + n_ff]).astype(jnp.bfloat16)
         columns = pl.ds(first, chunk.shape[0])
         out[:, columns] = part[:half]
@@ -203,7 +215,7 @@
     def ordered_body(*refs):
         ordered_kernel(y_places, *refs)
 
-    (ffn_y,) = call(ordered_body, (jax.ShapeDtypeStruct((ny * ffn_shape[0], width), ffn.dtype),), pos, blocks, 4, placed=False)
+    (ffn_y,) = call(ordered_body, (jax.ShapeDtypeStruct((ny * ffn_shape[0], width), ffn.dtype),), pos, blocks, 4)
     chunks, ffn_places = [ffn_y], [(0, 0)]
     up = down = ffn_y
     for k in (1, 2, 3):
@@ -218,8 +230,14 @@
     halves = (nx, own_rows, feats)
 
     pos = tick(pos)
-    scratch = [pltpu.VMEM((feats, mixer_shape[1]), bf), pltpu.VMEM((count, w_gate_b.shape[1]), bf)]
-    mine, other = call(mixer_kernel, (pltpu.VMEM(halves, bf),) * 2, pos, (normed, conv_taps, gathered), 16, scratch)
+    scratch = [
+        pltpu.VMEM((feats, mixer_shape[1]), bf),
+        pltpu.VMEM((count, w_gate_b.shape[1]), bf),
+        pltpu.SemaphoreType.DMA((ny, Z_LO)),
+    ]
+    mine, other = call(
+        mixer_kernel, (pltpu.VMEM(halves, bf),) * 2, pos, (normed, conv_taps), 16, scratch, (gathered,)
+    )
 
     def over_tp(mine, other):
         got = lax.ppermute(other, "core", SWAP)
@@ -242,7 +260,8 @@
     def ffn_body(*refs):
         ffn_kernel(ffn_places, n_ff, *refs)
 
-    pair = call(ffn_body, (pltpu.VMEM((half_rows, feats), bf),) * 2, pos, (acts, acts_other, *chunks), 24)
+    room = [pltpu.VMEM(chunk.shape, bf) for chunk in chunks] + [pltpu.SemaphoreType.DMA((len(chunks),))]
+    pair = call(ffn_body, (pltpu.VMEM((half_rows, feats), bf),) * 2, pos, (acts, acts_other), 24, room, chunks)
     blocks = over_tp(*(part.reshape(halves) for part in pair))
     return call(last_kernel, (jax.ShapeDtypeStruct((own_rows, feats), bf),), None, (blocks, stream), 8)[0]
 

time: 206 us -> 208 us (level)
  other arithmetic: 6.57 us -> 3.65 us
  Pallas kernels: 18 us -> 20.7 us
  waiting for transfers between devices: 40.6 us -> 43.2 us
    pallas_call x5, Pallas kernels: 11.8 us -> 14.5 us  [call(): pl.pallas_call(kernel, out_shape=outs, in_specs=specs, out_specs=(VMEM,)...]
    all_to_all x3, waiting for transfers between devices: 16.5 us -> 19 us  [exchange(): return lax.all_to_all(blocks, axis, 0, 0, tiled=True)]
  transfers between devices with their start and end apart: 17 -> 17, of which waited for: 9 -> 9; matrix products, arithmetic and copies ran while one was open for 2% -> 1% of each run, Pallas kernels for 3% -> 3%
where the time goes in v5:
time: 208 us; the launch traced here: 207 us
  starting transfers between devices  85 us (41%)
  blocking collectives  51.9 us (25%)
  waiting for transfers between devices  43.2 us (21%)
  Pallas kernels  20.7 us (10%)
  other arithmetic  3.65 us (2%)
    all_to_all x2, blocking collectives, exchange(): return lax.all_to_all(blocks, axis, 0, 0, tiled=True)  51.9 us
    ppermute x11, starting transfers between devices, shift(): lax.ppermute(value, axis, [((k + distance) % size, k) for k in range(size)])  47.7 us
    ppermute x11, waiting for transfers between devices, shift(): lax.ppermute(value, axis, [((k + distance) % size, k) for k in range(size)])  19.6 us
    all_to_all x3, waiting for transfers between devices, exchange(): return lax.all_to_all(blocks, axis, 0, 0, tiled=True)  19 us
    ppermute x2, starting transfers between devices, over_tp(): got = lax.ppermute(other, 'core', SWAP)  18.1 us
    pallas_call x5, Pallas kernels, call(): pl.pallas_call(kernel, out_shape=outs, in_specs=specs, out_specs=(VMEM,)...  14.5 us
    all_to_all x3, starting transfers between devices, exchange(): return lax.all_to_all(blocks, axis, 0, 0, tiled=True)  12.9 us
    ppermute x1, starting transfers between devices, local(): acts_other = lax.ppermute(acts, 'core', SWAP)  6.25 us
  transfers between devices with their start and end apart: 17, of which 9 were waited for; matrix products, arithmetic and copies ran while one was open for 1% of the time, Pallas kernels for 3%

profile of v5, /device:TPU:1, one launch (start us, length us, event | category | flops | bytes accessed | tf_op | source)
XLA Modules:
  0.0 206.6 jit_solution(9890927995764088633)
XLA Ops:
  0.8 35.1 %all_to_all.25.block = bf16[8,64,512]{2,1,0:T(8,128)(2,1)S(1)} all-to-all(bf16[8,64,512]{2,1,0:T(8,128)(2,1)S(1)} %broadcast_in_dim.2), channel_id=1, replica_groups=mesh['rep'=4,'zl'=8,'y'=4,'x'=4,'core'=2] {'zl'}, dimensions={0} | all-to-all | bytes 1048576 | tf_op jit(solution)/shard_map/all_to_all | solution.py:24
  37.8 4.8 %all-to-all-start.1 = ((bf16[32,64,512]{2,1,0:T(8,128)(2,1)}), bf16[32,64,512]{2,1,0:T(8,128)(2,1)}, u32[]{:S(2)}, u32[]{:S(2)}) async-start(bf16[32,64,512]{2,1,0:T(8,128)(2,1)} %bitcast.22), calls=%async_computation.1 | async-start | bytes 4194304 | tf_op jit(solution)/shard_map/all_to_all | solution.py:24
  44.9 17.0 %all-to-all-done.1 = bf16[32,64,512]{2,1,0:T(8,128)(2,1)} async-done(((bf16[32,64,512]{2,1,0:T(8,128)(2,1)}), bf16[32,64,512]{2,1,0:T(8,128)(2,1)}, u32[]{:S(2)}, u32[]{:S(2)}) %all-to-all-start.1) | async-done | bytes 2097184 | tf_op jit(solution)/shard_map/all_to_all | solution.py:24
  61.9 5.2 %shard_map.113 = (bf16[4,64,2048]{2,1,0:T(8,128)(2,1)S(1)}, bf16[4,64,2048]{2,1,0:T(8,128)(2,1)S(1)}) custom-call(s32[3]{0:T(128)S(1)} %shard_map.109.pos, bf16[512,2048]{1,0:T(8,128)(2,1)S(1)} %fusion.2.normed, f32[3,128]{1,0:T(4,128)S(1)} %copy-done.2, bf16[4,8,64,512]{3,2,1,0:T(8,128)(2,1)} %bitcast.5.gathered), custom_call_target="tpu_custom_call" | custom-call | tf_op jit(solution)/shard_map/pallas_call | solution.py:45
  67.1 10.2 %collective-permute-start = (bf16[4,64,2048]{2,1,0:T(8,128)(2,1)S(1)}, bf16[4,64,2048]{2,1,0:T(8,128)(2,1)S(1)}, u32[]{:S(2)}, u32[]{:S(2)}) collective-permute-start(bf16[4,64,2048]{2,1,0:T(8,128)(2,1)S(1)} %get-tuple-element.12), channel_id=1, source_target_pairs={{0,1},{1,0},{2,3},{3,2},{4,5},{5,4},{6,7},{7,6},{8,9},{9,8},{10,11... | collective-permute-start | bytes 3145736 | tf_op jit(solution)/shard_map/ppermute | solution.py:243
  77.3 2.3 %collective-permute-done = bf16[4,64,2048]{2,1,0:T(8,128)(2,1)S(1)} collective-permute-done((bf16[4,64,2048]{2,1,0:T(8,128)(2,1)S(1)}, bf16[4,64,2048]{2,1,0:T(8,128)(2,1)S(1)}, u32[]{:S(2)}, u32[]{:S(2)}) %collective-permute-start) | collective-permute-done | bytes 1048608 | tf_op jit(solution)/shard_map/ppermute | solution.py:243
  80.9 4.2 %all-to-all-start.2 = ((bf16[4,64,2048]{2,1,0:T(8,128)(2,1)}), bf16[4,64,2048]{2,1,0:T(8,128)(2,1)S(1)}, u32[]{:S(2)}, u32[]{:S(2)}) async-start(bf16[4,64,2048]{2,1,0:T(8,128)(2,1)} %add_convert_fusion), calls=%async_computation.2 | async-start | bytes 2097152 | tf_op jit(solution)/shard_map/all_to_all | solution.py:24
  85.9 2.3 %collective-permute-start.2 = (bf16[64,1152]{1,0:T(8,128)(2,1)S(1)}, bf16[64,1152]{1,0:T(8,128)(2,1)S(1)}, u32[]{:S(2)}, u32[]{:S(2)}) collective-permute-start(bf16[64,1152]{1,0:T(8,128)(2,1)S(1)} %bitcast.16), channel_id=1, source_target_pairs={{16,0},{24,8},{0,16},{8,24},{17,1},{25,9},{1,17},{9,25},{18,2},{26... | collective-permute-start | bytes 442376 | tf_op jit(solution)/shard_map/ppermute | solution.py:20
  88.2 4.3 %collective-permute-start.3 = (bf16[64,1152]{1,0:T(8,128)(2,1)S(1)}, bf16[64,1152]{1,0:T(8,128)(2,1)S(1)}, u32[]{:S(2)}, u32[]{:S(2)}) collective-permute-start(bf16[64,1152]{1,0:T(8,128)(2,1)S(1)} %bitcast.17), channel_id=1, source_target_pairs={{8,0},{16,8},{24,16},{0,24},{9,1},{17,9},{25,17},{1,25},{10,2},{18... | collective-permute-start | bytes 442376 | tf_op jit(solution)/shard_map/ppermute | solution.py:20
  96.0 3.9 %collective-permute-done.4.refs_4_ = bf16[64,1152]{1,0:T(8,128)(2,1)S(1)} collective-permute-done((bf16[64,1152]{1,0:T(8,128)(2,1)S(1)}, bf16[64,1152]{1,0:T(8,128)(2,1)S(1)}, u32[]{:S(2)}, u32[]{:S(2)}) %collective-permute-start.4) | collective-permute-done | bytes 147488 | tf_op jit(solution)/shard_map/ppermute | solution.py:20
  100.5 16.1 %collective-permute-start.5 = (bf16[256,1152]{1,0:T(8,128)(2,1)S(1)}, bf16[256,1152]{1,0:T(8,128)(2,1)S(1)}, u32[]{:S(2)}, u32[]{:S(2)}) collective-permute-start(bf16[256,1152]{1,0:T(8,128)(2,1)S(1)} %shard_map.116.refs_3_), channel_id=1, source_target_pairs={{32,0},{64,32},{96,64},{128,96},{160,128},{192,160},{224,192},{256... | collective-permute-start | bytes 1769480 | tf_op jit(solution)/shard_map/ppermute | solution.py:20
  120.8 3.9 %all-to-all-start.3 = ((bf16[4,64,2048]{2,1,0:T(8,128)(2,1)}), bf16[4,64,2048]{2,1,0:T(8,128)(2,1)S(1)}, u32[]{:S(2)}, u32[]{:S(2)}) async-start(bf16[4,64,2048]{2,1,0:T(8,128)(2,1)} %get-tuple-element.13), calls=%async_computation.3 | async-start | bytes 2097152 | tf_op jit(solution)/shard_map/all_to_all | solution.py:24
  124.8 2.4 %collective-permute-done.5.refs_4_ = bf16[256,1152]{1,0:T(8,128)(2,1)S(1)} collective-permute-done((bf16[256,1152]{1,0:T(8,128)(2,1)S(1)}, bf16[256,1152]{1,0:T(8,128)(2,1)S(1)}, u32[]{:S(2)}, u32[]{:S(2)}) %collective-permute-start.5) | collective-permute-done | bytes 589856 | tf_op jit(solution)/shard_map/ppermute | solution.py:20
  127.2 5.3 %collective-permute-start.7 = (bf16[256,1152]{1,0:T(8,128)(2,1)S(1)}, bf16[256,1152]{1,0:T(8,128)(2,1)}, u32[]{:S(2)}, u32[]{:S(2)}) collective-permute-start(bf16[256,1152]{1,0:T(8,128)(2,1)S(1)} %collective-permute-done.5.refs_4_), channel_id=1, source_target_pairs={{32,0},{64,32},{96,64},{128,96},{160,128},{192,160},{224,192},{256... | collective-permute-start | bytes 1769480 | tf_op jit(solution)/shard_map/ppermute | solution.py:20
  134.5 2.0 all-to-all-done.3
  136.5 6.3 %collective-permute-start.1 = (bf16[256,2048]{1,0:T(8,128)(2,1)S(1)}, bf16[256,2048]{1,0:T(8,128)(2,1)S(1)}, u32[]{:S(2)}, u32[]{:S(2)}) collective-permute-start(bf16[256,2048]{1,0:T(8,128)(2,1)S(1)} %bitcast.13), channel_id=1, source_target_pairs={{0,1},{1,0},{2,3},{3,2},{4,5},{5,4},{6,7},{7,6},{8,9},{9,8},{10,11... | collective-permute-start | bytes 3145736 | tf_op jit(solution)/shard_map/ppermute | solution.py:258
  142.8 4.9 %collective-permute-start.9 = (bf16[256,1152]{1,0:T(8,128)(2,1)}, bf16[256,1152]{1,0:T(8,128)(2,1)S(1)}, u32[]{:S(2)}, u32[]{:S(2)}) collective-permute-start(bf16[256,1152]{1,0:T(8,128)(2,1)} %collective-permute-done.7.refs_6_), channel_id=1, source_target_pairs={{32,0},{64,32},{96,64},{128,96},{160,128},{192,160},{224,192},{256... | collective-permute-start | bytes 1769480 | tf_op jit(solution)/shard_map/ppermute | solution.py:20
  149.6 7.3 %collective-permute-done.9.refs_8_ = bf16[256,1152]{1,0:T(8,128)(2,1)S(1)} collective-permute-done((bf16[256,1152]{1,0:T(8,128)(2,1)}, bf16[256,1152]{1,0:T(8,128)(2,1)S(1)}, u32[]{:S(2)}, u32[]{:S(2)}) %collective-permute-start.9) | collective-permute-done | bytes 589856 | tf_op jit(solution)/shard_map/ppermute | solution.py:20
  156.9 5.2 %collective-permute-start.11 = (bf16[128,1152]{1,0:T(8,128)(2,1)S(1)}, bf16[128,1152]{1,0:T(8,128)(2,1)S(1)}, u32[]{:S(2)}, u32[]{:S(2)}) collective-permute-start(bf16[128,1152]{1,0:T(8,128)(2,1)S(1)} %slice.8), channel_id=1, source_target_pairs={{32,0},{64,32},{96,64},{128,96},{160,128},{192,160},{224,192},{256... | collective-permute-start | bytes 884744 | tf_op jit(solution)/shard_map/ppermute | solution.py:20
  166.4 4.4 %collective-permute-done.12.refs_11_ = bf16[128,1152]{1,0:T(8,128)(2,1)S(1)} collective-permute-done((bf16[128,1152]{1,0:T(8,128)(2,1)S(1)}, bf16[128,1152]{1,0:T(8,128)(2,1)S(1)}, u32[]{:S(2)}, u32[]{:S(2)}) %collective-permute-start.12) | collective-permute-done | bytes 294944 | tf_op jit(solution)/shard_map/ppermute | solution.py:20
  171.6 6.6 %shard_map.117 = (bf16[256,2048]{1,0:T(8,128)(2,1)S(1)}, bf16[256,2048]{1,0:T(8,128)(2,1)S(1)}) custom-call(s32[3]{0:T(128)S(1)} %shard_map.111.refs_0_, bf16[256,2048]{1,0:T(8,128)(2,1)S(1)} %bitcast.14, bf16[256,2048]{1,0:T(8,128)(2,1)S(1)} %collective-permute-done.1.refs_2_, bf16[256,1152]{1,0:T(8,128)(2,1)} %copy-done, bf16[256,1152]{1,0:T(8,128)(2,1)} %copy-done.7, ...), custom_call_target="tpu_custom_call" | custom-call | tf_op jit(solution)/shard_map/pallas_call | solution.py:45
  178.3 8.0 %collective-permute-start.13 = (bf16[4,64,2048]{2,1,0:T(8,128)(2,1)S(1)}, bf16[4,64,2048]{2,1,0:T(8,128)(2,1)S(1)}, u32[]{:S(2)}, u32[]{:S(2)}) collective-permute-start(bf16[4,64,2048]{2,1,0:T(8,128)(2,1)S(1)} %bitcast.21), channel_id=1, source_target_pairs={{0,1},{1,0},{2,3},{3,2},{4,5},{5,4},{6,7},{7,6},{8,9},{9,8},{10,11... | collective-permute-start | bytes 3145736 | tf_op jit(solution)/shard_map/ppermute | solution.py:243
  186.2 2.3 %collective-permute-done.13 = bf16[4,64,2048]{2,1,0:T(8,128)(2,1)S(1)} collective-permute-done((bf16[4,64,2048]{2,1,0:T(8,128)(2,1)S(1)}, bf16[4,64,2048]{2,1,0:T(8,128)(2,1)S(1)}, u32[]{:S(2)}, u32[]{:S(2)}) %collective-permute-start.13) | collective-permute-done | bytes 1048608 | tf_op jit(solution)/shard_map/ppermute | solution.py:243
  188.9 16.8 %all_to_all.26.blocks = bf16[4,64,2048]{2,1,0:T(8,128)(2,1)S(1)} all-to-all(bf16[4,64,2048]{2,1,0:T(8,128)(2,1)S(1)} %fusion.3), channel_id=1, replica_groups=mesh['rep'=4,'zl'=8,'y'=4,'x'=4,'core'=2] {'x'}, dimensions={0} | all-to-all | bytes 2097152 | tf_op jit(solution)/shard_map/all_to_all | solution.py:24
  (55 shorter events, 25.4 us)
Async XLA Ops:
  37.8 6.0 %copy-start.3 = (bf16[512,2048]{1,0:T(8,128)(2,1)S(1)}, bf16[512,2048]{1,0:T(8,128)(2,1)}, u32[]{:S(2)}) copy-start(bf16[512,2048]{1,0:T(8,128)(2,1)} %param.11) | copy-start | bytes 6291460
  37.8 24.1 %all-to-all-start.1 = ((bf16[32,64,512]{2,1,0:T(8,128)(2,1)}), bf16[32,64,512]{2,1,0:T(8,128)(2,1)}, u32[]{:S(2)}, u32[]{:S(2)}) async-start(bf16[32,64,512]{2,1,0:T(8,128)(2,1)} %bitcast.22), calls=%async_computation.1 | async-start | bytes 4194304 | tf_op jit(solution)/shard_map/all_to_all | solution.py:24
  44.3 17.6 %copy-start.2 = (f32[3,128]{1,0:T(4,128)S(1)}, f32[3,128]{1,0:T(4,128)}, u32[]{:S(2)}) copy-start(f32[3,128]{1,0:T(4,128)} %taps.1) | copy-start | bytes 4612
  67.1 12.4 %collective-permute-start = (bf16[4,64,2048]{2,1,0:T(8,128)(2,1)S(1)}, bf16[4,64,2048]{2,1,0:T(8,128)(2,1)S(1)}, u32[]{:S(2)}, u32[]{:S(2)}) collective-permute-start(bf16[4,64,2048]{2,1,0:T(8,128)(2,1)S(1)} %get-tuple-element.12), channel_id=1, source_target_pairs={{0,1},{1,0},{2,3},{3,2},{4,5},{5,4},{6,7},{7,6},{8,9},{9,8},{10,11... | collective-permute-start | bytes 3145736 | tf_op jit(solution)/shard_map/ppermute | solution.py:243
  80.9 38.6 %copy-start.1 = (f32[2048]{0:T(1024)S(1)}, f32[2048]{0:T(1024)}, u32[]{:S(2)}) copy-start(f32[2048]{0:T(1024)} %param.18) | copy-start | bytes 24580
  80.9 38.6 %all-to-all-start.2 = ((bf16[4,64,2048]{2,1,0:T(8,128)(2,1)}), bf16[4,64,2048]{2,1,0:T(8,128)(2,1)S(1)}, u32[]{:S(2)}, u32[]{:S(2)}) async-start(bf16[4,64,2048]{2,1,0:T(8,128)(2,1)} %add_convert_fusion), calls=%async_computation.2 | async-start | bytes 2097152 | tf_op jit(solution)/shard_map/all_to_all | solution.py:24
  85.9 8.5 %collective-permute-start.2 = (bf16[64,1152]{1,0:T(8,128)(2,1)S(1)}, bf16[64,1152]{1,0:T(8,128)(2,1)S(1)}, u32[]{:S(2)}, u32[]{:S(2)}) collective-permute-start(bf16[64,1152]{1,0:T(8,128)(2,1)S(1)} %bitcast.16), channel_id=1, source_target_pairs={{16,0},{24,8},{0,16},{8,24},{17,1},{25,9},{1,17},{9,25},{18,2},{26... | collective-permute-start | bytes 442376 | tf_op jit(solution)/shard_map/ppermute | solution.py:20
  88.2 7.8 %collective-permute-start.3 = (bf16[64,1152]{1,0:T(8,128)(2,1)S(1)}, bf16[64,1152]{1,0:T(8,128)(2,1)S(1)}, u32[]{:S(2)}, u32[]{:S(2)}) collective-permute-start(bf16[64,1152]{1,0:T(8,128)(2,1)S(1)} %bitcast.17), channel_id=1, source_target_pairs={{8,0},{16,8},{24,16},{0,24},{9,1},{17,9},{25,17},{1,25},{10,2},{18... | collective-permute-start | bytes 442376 | tf_op jit(solution)/shard_map/ppermute | solution.py:20
  92.5 7.4 %collective-permute-start.4 = (bf16[64,1152]{1,0:T(8,128)(2,1)S(1)}, bf16[64,1152]{1,0:T(8,128)(2,1)S(1)}, u32[]{:S(2)}, u32[]{:S(2)}) collective-permute-start(bf16[64,1152]{1,0:T(8,128)(2,1)S(1)} %bitcast.18), channel_id=1, source_target_pairs={{24,0},{0,8},{8,16},{16,24},{25,1},{1,9},{9,17},{17,25},{26,2},{2,... | collective-permute-start | bytes 442376 | tf_op jit(solution)/shard_map/ppermute | solution.py:20
  100.5 56.4 %copy-start = (bf16[256,1152]{1,0:T(8,128)(2,1)}, bf16[256,1152]{1,0:T(8,128)(2,1)S(1)}, u32[]{:S(2)}) copy-start(bf16[256,1152]{1,0:T(8,128)(2,1)S(1)} %shard_map.116.refs_3_) | copy-start | bytes 1769476
  100.5 26.7 %collective-permute-start.5 = (bf16[256,1152]{1,0:T(8,128)(2,1)S(1)}, bf16[256,1152]{1,0:T(8,128)(2,1)S(1)}, u32[]{:S(2)}, u32[]{:S(2)}) collective-permute-start(bf16[256,1152]{1,0:T(8,128)(2,1)S(1)} %shard_map.116.refs_3_), channel_id=1, source_target_pairs={{32,0},{64,32},{96,64},{128,96},{160,128},{192,160},{224,192},{256... | collective-permute-start | bytes 1769480 | tf_op jit(solution)/shard_map/ppermute | solution.py:20
  116.6 15.9 %collective-permute-start.6 = (bf16[256,1152]{1,0:T(8,128)(2,1)S(1)}, bf16[256,1152]{1,0:T(8,128)(2,1)}, u32[]{:S(2)}, u32[]{:S(2)}) collective-permute-start(bf16[256,1152]{1,0:T(8,128)(2,1)S(1)} %shard_map.116.refs_3_), channel_id=1, source_target_pairs={{992,0},{0,32},{32,64},{64,96},{96,128},{128,160},{160,192},{192,2... | collective-permute-start | bytes 1769480 | tf_op jit(solution)/shard_map/ppermute | solution.py:20
  120.8 15.6 %all-to-all-start.3 = ((bf16[4,64,2048]{2,1,0:T(8,128)(2,1)}), bf16[4,64,2048]{2,1,0:T(8,128)(2,1)S(1)}, u32[]{:S(2)}, u32[]{:S(2)}) async-start(bf16[4,64,2048]{2,1,0:T(8,128)(2,1)} %get-tuple-element.13), calls=%async_computation.3 | async-start | bytes 2097152 | tf_op jit(solution)/shard_map/all_to_all | solution.py:24
  127.2 43.7 %copy-start.7 = (bf16[256,1152]{1,0:T(8,128)(2,1)}, bf16[256,1152]{1,0:T(8,128)(2,1)S(1)}, u32[]{:S(2)}) copy-start(bf16[256,1152]{1,0:T(8,128)(2,1)S(1)} %collective-permute-done.5.refs_4_) | copy-start | bytes 1769476
  127.2 15.5 %collective-permute-start.7 = (bf16[256,1152]{1,0:T(8,128)(2,1)S(1)}, bf16[256,1152]{1,0:T(8,128)(2,1)}, u32[]{:S(2)}, u32[]{:S(2)}) collective-permute-start(bf16[256,1152]{1,0:T(8,128)(2,1)S(1)} %collective-permute-done.5.refs_4_), channel_id=1, source_target_pairs={{32,0},{64,32},{96,64},{128,96},{160,128},{192,160},{224,192},{256... | collective-permute-start | bytes 1769480 | tf_op jit(solution)/shard_map/ppermute | solution.py:20
  132.5 15.2 %collective-permute-start.8 = (bf16[256,1152]{1,0:T(8,128)(2,1)}, bf16[256,1152]{1,0:T(8,128)(2,1)}, u32[]{:S(2)}, u32[]{:S(2)}) collective-permute-start(bf16[256,1152]{1,0:T(8,128)(2,1)} %collective-permute-done.6.refs_5_), channel_id=1, source_target_pairs={{992,0},{0,32},{32,64},{64,96},{96,128},{128,160},{160,192},{192,2... | collective-permute-start | bytes 1769480 | tf_op jit(solution)/shard_map/ppermute | solution.py:20
  136.5 34.4 %collective-permute-start.1 = (bf16[256,2048]{1,0:T(8,128)(2,1)S(1)}, bf16[256,2048]{1,0:T(8,128)(2,1)S(1)}, u32[]{:S(2)}, u32[]{:S(2)}) collective-permute-start(bf16[256,2048]{1,0:T(8,128)(2,1)S(1)} %bitcast.13), channel_id=1, source_target_pairs={{0,1},{1,0},{2,3},{3,2},{4,5},{5,4},{6,7},{7,6},{8,9},{9,8},{10,11... | collective-permute-start | bytes 3145736 | tf_op jit(solution)/shard_map/ppermute | solution.py:258
  142.8 14.1 %collective-permute-start.9 = (bf16[256,1152]{1,0:T(8,128)(2,1)}, bf16[256,1152]{1,0:T(8,128)(2,1)S(1)}, u32[]{:S(2)}, u32[]{:S(2)}) collective-permute-start(bf16[256,1152]{1,0:T(8,128)(2,1)} %collective-permute-done.7.refs_6_), channel_id=1, source_target_pairs={{32,0},{64,32},{96,64},{128,96},{160,128},{192,160},{224,192},{256... | collective-permute-start | bytes 1769480 | tf_op jit(solution)/shard_map/ppermute | solution.py:20
  147.7 14.5 %collective-permute-start.10 = (bf16[256,1152]{1,0:T(8,128)(2,1)}, bf16[256,1152]{1,0:T(8,128)(2,1)S(1)}, u32[]{:S(2)}, u32[]{:S(2)}) collective-permute-start(bf16[256,1152]{1,0:T(8,128)(2,1)} %collective-permute-done.8.refs_7_), channel_id=1, source_target_pairs={{992,0},{0,32},{32,64},{64,96},{96,128},{128,160},{160,192},{192,2... | collective-permute-start | bytes 1769480 | tf_op jit(solution)/shard_map/ppermute | solution.py:20
  156.9 14.0 %copy-start.5 = (bf16[256,1152]{1,0:T(8,128)(2,1)}, bf16[256,1152]{1,0:T(8,128)(2,1)S(1)}, u32[]{:S(2)}) copy-start(bf16[256,1152]{1,0:T(8,128)(2,1)S(1)} %collective-permute-done.9.refs_8_) | copy-start | bytes 1769476
  156.9 9.5 %collective-permute-start.11 = (bf16[128,1152]{1,0:T(8,128)(2,1)S(1)}, bf16[128,1152]{1,0:T(8,128)(2,1)S(1)}, u32[]{:S(2)}, u32[]{:S(2)}) collective-permute-start(bf16[128,1152]{1,0:T(8,128)(2,1)S(1)} %slice.8), channel_id=1, source_target_pairs={{32,0},{64,32},{96,64},{128,96},{160,128},{192,160},{224,192},{256... | collective-permute-start | bytes 884744 | tf_op jit(solution)/shard_map/ppermute | solution.py:20
  162.2 8.7 %copy-start.6 = (bf16[256,1152]{1,0:T(8,128)(2,1)}, bf16[256,1152]{1,0:T(8,128)(2,1)S(1)}, u32[]{:S(2)}) copy-start(bf16[256,1152]{1,0:T(8,128)(2,1)S(1)} %collective-permute-done.10.refs_9_) | copy-start | bytes 1769476
  162.2 8.7 %collective-permute-start.12 = (bf16[128,1152]{1,0:T(8,128)(2,1)S(1)}, bf16[128,1152]{1,0:T(8,128)(2,1)S(1)}, u32[]{:S(2)}, u32[]{:S(2)}) collective-permute-start(bf16[128,1152]{1,0:T(8,128)(2,1)S(1)} %slice.9), channel_id=1, source_target_pairs={{992,0},{0,32},{32,64},{64,96},{96,128},{128,160},{160,192},{192,2... | collective-permute-start | bytes 884744 | tf_op jit(solution)/shard_map/ppermute | solution.py:20
  178.3 10.2 %collective-permute-start.13 = (bf16[4,64,2048]{2,1,0:T(8,128)(2,1)S(1)}, bf16[4,64,2048]{2,1,0:T(8,128)(2,1)S(1)}, u32[]{:S(2)}, u32[]{:S(2)}) collective-permute-start(bf16[4,64,2048]{2,1,0:T(8,128)(2,1)S(1)} %bitcast.21), channel_id=1, source_target_pairs={{0,1},{1,0},{2,3},{3,2},{4,5},{5,4},{6,7},{7,6},{8,9},{9,8},{10,11... | collective-permute-start | bytes 3145736 | tf_op jit(solution)/shard_map/ppermute | solution.py:243
  (4 other events, 8.7 us)

commit v6 on v4

--- a/solution.py
+++ b/solution.py
@@ -12,6 +12,7 @@
 SWAP = [(0, 1), (1, 0)]
 
 VMEM = pl.BlockSpec(memory_space=pltpu.VMEM)
+ANY = pl.BlockSpec(memory_space=pl.ANY)
 SMEM = pl.BlockSpec(memory_space=pltpu.SMEM)
 
 
@@ -35,10 +36,10 @@
     return jnp.dot(acts, weight, preferred_element_type=jnp.float32)
 
 
-def call(kernel, outs, pos, args, mib, scratch=(), placed=True):
-    if placed:
-        args = [pltpu.with_memory_space_constraint(a, pltpu.VMEM) for a in args]
-    specs = [VMEM] * len(args)
+def call(kernel, outs, pos, args, mib, scratch=(), far=()):
+    args = [pltpu.with_memory_space_constraint(a, pltpu.VMEM) for a in args]
+    specs = [VMEM] * len(args) + [ANY] * len(far)
+    args += [pltpu.with_memory_space_constraint(a, pltpu.HBM) for a in far]
     if pos is not None:
         args, specs = [pos, *args], [SMEM, *specs]
     return pl.pallas_call(
@@ -97,8 +98,12 @@
         out[pl.ds(pl.multiple_of(y * block.shape[0], block.shape[0]), block.shape[0]), :] = block[...]
 
 
-def copy_kernel(block, out):
-    out[0] = block[...]
+def copies_kernel(block, out, sems):
+    fetches = [pltpu.make_async_copy(block, out.at[k], sems.at[k]) for k in range(out.shape[0])]
+    for fetch in fetches:
+        fetch.start()
+    for fetch in fetches:
+        fetch.wait()
 
 
 def bundle_kernel(*refs):
@@ -140,24 +145,35 @@
 
 
 def ffn_kernel(places, n_ff, pos, acts, acts_other, *refs):
-    chunks, out, out_other = refs[: len(places)], refs[len(places)], refs[len(places) + 1]
+    count = len(places)
+    chunks, (out, out_other, weights, values, sems) = refs[:count], refs[count:]
+    half = acts.shape[0]
     depth = acts.shape[1] // Z_LO
-    step = chunks[0].shape[1] // 3
-    both = None
-    firsts = []
-    for (d, row), chunk in zip(places, chunks):
+    step = weights.shape[1] // 3
+    fetches, spans = [], []
+    at = 0
+    for k, ((d, row), chunk) in enumerate(zip(places, chunks)):
+        rows = chunk.shape[0]
+        fetches.append(pltpu.make_async_copy(chunk, weights.at[at : at + rows], sems.at[k]))
+        fetches[-1].start()
         z = lax.rem(pos[0] + (d + Z_LO), Z_LO)
-        first = pl.multiple_of(z * depth + row, chunk.shape[0])
-        firsts.append(first)
-        columns = pl.ds(first, chunk.shape[0])
-        values = jnp.concatenate([acts[:, columns], acts_other[:, columns]], axis=0)
-        part = dot(values, chunk[:, : 2 * step])
-        both = part if both is None else both + part
+        spans.append((at, rows, pl.ds(pl.multiple_of(z * depth + row, rows), rows)))
+        at += rows
+    for first, rows, columns in spans:
+        values[:half, first : first + rows] = acts[:, columns]
+        values[half:, first : first + rows] = acts_other[:, columns]
+    middle = at // 2
+    for fetch, (first, _, _) in zip(fetches, spans):
+        if first < middle:
+            fetch.wait()
+    both = dot(values[:, :middle], weights[:middle, : 2 * step])
+    for fetch, (first, _, _) in zip(fetches, spans):
+        if first >= middle:
+            fetch.wait()
+    both += dot(values[:, middle:], weights[middle:, : 2 * step])
     hidden = (jax.nn.silu(both[:, :n_ff]) * both[:, step : step + n_ff]).astype(jnp.bfloat16)
-    half = acts.shape[0]
-    for first, chunk in zip(firsts, chunks):
-        part = dot_t(hidden, chunk[:, 2 * step : 2 * step + n_ff]).astype(jnp.bfloat16)
-        columns = pl.ds(first, chunk.shape[0])
+    for first, rows, columns in spans:
+        part = dot_t(hidden, weights[first : first + rows, 2 * step : 2 * step + n_ff]).astype(jnp.bfloat16)
         out[:, columns] = part[:half]
         out_other[:, columns] = part[half:]
 
@@ -187,7 +203,14 @@
     mixer_shape = mixer.shape
     sent = jnp.broadcast_to(mixer[None], (Z_LO, *mixer_shape))
     along_z = exchange(sent, "zl")
-    sent = for_exchange(copy_kernel, (along_z,), ny, along_z.shape, along_z.dtype, source=pltpu.VMEM)
+    sent = pl.pallas_call(
+        copies_kernel,
+        out_shape=pltpu.HBM((ny, *along_z.shape), along_z.dtype),
+        in_specs=[VMEM],
+        out_specs=ANY,
+        scratch_shapes=[pltpu.SemaphoreType.DMA((ny,))],
+        compiler_params=pltpu.CompilerParams(vmem_limit_bytes=4 * 1024 * 1024),
+    )(pltpu.with_memory_space_constraint(along_z, pltpu.VMEM))
     normed = rms_scale(tokens.astype(jnp.float32), mix_gain).astype(jnp.bfloat16)
     own = lax.dynamic_slice_in_dim(tokens, (lax.axis_index("x") * 2 + core) * own_rows, own_rows, 0)
     gathered = exchange(sent.reshape(-1, *mixer_shape), "y").reshape(ny, Z_LO, *mixer_shape)
@@ -203,7 +226,7 @@
     def ordered_body(*refs):
         ordered_kernel(y_places, *refs)
 
-    (ffn_y,) = call(ordered_body, (jax.ShapeDtypeStruct((ny * ffn_shape[0], width), ffn.dtype),), pos, blocks, 4, placed=False)
+    (ffn_y,) = call(ordered_body, (jax.ShapeDtypeStruct((ny * ffn_shape[0], width), ffn.dtype),), pos, blocks, 4)
     chunks, ffn_places = [ffn_y], [(0, 0)]
     up = down = ffn_y
     for k in (1, 2, 3):
@@ -218,8 +241,13 @@
     halves = (nx, own_rows, feats)
 
     pos = tick(pos)
-    scratch = [pltpu.VMEM((feats, mixer_shape[1]), bf), pltpu.VMEM((count, w_gate_b.shape[1]), bf)]
-    mine, other = call(mixer_kernel, (pltpu.VMEM(halves, bf),) * 2, pos, (normed, conv_taps, gathered), 16, scratch)
+    scratch = [
+        pltpu.VMEM((feats, mixer_shape[1]), bf),
+        pltpu.VMEM((count, w_gate_b.shape[1]), bf),
+    ]
+    mine, other = call(
+        mixer_kernel, (pltpu.VMEM(halves, bf),) * 2, pos, (normed, conv_taps, gathered), 16, scratch
+    )
 
     def over_tp(mine, other):
         got = lax.ppermute(other, "core", SWAP)
@@ -242,7 +270,12 @@
     def ffn_body(*refs):
         ffn_kernel(ffn_places, n_ff, *refs)
 
-    pair = call(ffn_body, (pltpu.VMEM((half_rows, feats), bf),) * 2, pos, (acts, acts_other, *chunks), 24)
+    room = [
+        pltpu.VMEM((feats, width), bf),
+        pltpu.VMEM((count, feats), bf),
+        pltpu.SemaphoreType.DMA((len(chunks),)),
+    ]
+    pair = call(ffn_body, (pltpu.VMEM((half_rows, feats), bf),) * 2, pos, (acts, acts_other), 24, room, chunks)
     blocks = over_tp(*(part.reshape(halves) for part in pair))
     return call(last_kernel, (jax.ShapeDtypeStruct((own_rows, feats), bf),), None, (blocks, stream), 8)[0]
 

time: 206 us -> 207 us (level)
  no operation moved by 1% of the time
where the time goes in v6:
time: 207 us; the launch traced here: 206 us
  starting transfers between devices  84.9 us (41%)
  blocking collectives  51.9 us (25%)
  waiting for transfers between devices  39.8 us (19%)
  Pallas kernels  18.8 us (9%)
  other arithmetic  6.56 us (3%)
  local copies, waits for them, and re-layouts  3.38 us (2%)
    all_to_all x2, blocking collectives, exchange(): return lax.all_to_all(blocks, axis, 0, 0, tiled=True)  51.9 us
    ppermute x11, starting transfers between devices, shift(): lax.ppermute(value, axis, [((k + distance) % size, k) for k in range(size)])  47.6 us
    ppermute x11, waiting for transfers between devices, shift(): lax.ppermute(value, axis, [((k + distance) % size, k) for k in range(size)])  19.6 us
    ppermute x2, starting transfers between devices, over_tp(): got = lax.ppermute(other, 'core', SWAP)  18.3 us
    all_to_all x3, waiting for transfers between devices, exchange(): return lax.all_to_all(blocks, axis, 0, 0, tiled=True)  15.7 us
    pallas_call x5, Pallas kernels, call(): pl.pallas_call(kernel, out_shape=outs, in_specs=specs, out_specs=(VMEM,)...  13.1 us
    all_to_all x3, starting transfers between devices, exchange(): return lax.all_to_all(blocks, axis, 0, 0, tiled=True)  12.8 us
    ppermute x1, starting transfers between devices, local(): acts_other = lax.ppermute(acts, 'core', SWAP)  6.25 us
  transfers between devices with their start and end apart: 17, of which 9 were waited for; matrix products, arithmetic and copies ran while one was open for 2% of the time, Pallas kernels for 3%

profile of v6, /device:TPU:1, one launch (start us, length us, event | category | flops | bytes accessed | tf_op | source)
XLA Modules:
  0.0 205.7 jit_solution(2559134542273280323)
XLA Ops:
  0.8 35.1 %all_to_all.25.block = bf16[8,64,512]{2,1,0:T(8,128)(2,1)S(1)} all-to-all(bf16[8,64,512]{2,1,0:T(8,128)(2,1)S(1)} %broadcast_in_dim.2), channel_id=1, replica_groups=mesh['rep'=4,'zl'=8,'y'=4,'x'=4,'core'=2] {'zl'}, dimensions={0} | all-to-all | bytes 1048576 | tf_op jit(solution)/shard_map/all_to_all | solution.py:24
  37.3 4.7 %all-to-all-start.1 = ((bf16[32,64,512]{2,1,0:T(8,128)(2,1)}), bf16[32,64,512]{2,1,0:T(8,128)(2,1)S(1)}, u32[]{:S(2)}, u32[]{:S(2)}) async-start(bf16[32,64,512]{2,1,0:T(8,128)(2,1)} %bitcast.23), calls=%async_computation.1 | async-start | bytes 4194304 | tf_op jit(solution)/shard_map/all_to_all | solution.py:24
  43.2 2.1 %fusion = f32[512]{0:T(512)S(1)} fusion(bf16[512,2048]{1,0:T(8,128)(2,1)} %param.11), kind=kLoop, calls=%fused_computation.2 | loop fusion | flops 3145216 | bytes 2099200 | tf_op jit(solution)/shard_map/reduce_sum | solution.py:28
  47.2 13.6 %all-to-all-done.1 = bf16[32,64,512]{2,1,0:T(8,128)(2,1)S(1)} async-done(((bf16[32,64,512]{2,1,0:T(8,128)(2,1)}), bf16[32,64,512]{2,1,0:T(8,128)(2,1)S(1)}, u32[]{:S(2)}, u32[]{:S(2)}) %all-to-all-start.1) | async-done | bytes 2097184 | tf_op jit(solution)/shard_map/all_to_all | solution.py:24
  62.4 3.4 %shard_map.113 = (bf16[4,64,2048]{2,1,0:T(8,128)(2,1)S(1)}, bf16[4,64,2048]{2,1,0:T(8,128)(2,1)S(1)}) custom-call(s32[3]{0:T(128)S(1)} %shard_map.109.pos, bf16[512,2048]{1,0:T(8,128)(2,1)S(1)} %copy-done, f32[3,128]{1,0:T(4,128)S(1)} %copy-done.3, bf16[4,8,64,512]{3,2,1,0:T(8,128)(2,1)S(1)} %bitcast.13), custom_call_target="tpu_custom_call" | custom-call | tf_op jit(solution)/shard_map/pallas_call | solution.py:45
  65.9 10.3 %collective-permute-start = (bf16[4,64,2048]{2,1,0:T(8,128)(2,1)S(1)}, bf16[4,64,2048]{2,1,0:T(8,128)(2,1)S(1)}, u32[]{:S(2)}, u32[]{:S(2)}) collective-permute-start(bf16[4,64,2048]{2,1,0:T(8,128)(2,1)S(1)} %get-tuple-element.12), channel_id=1, source_target_pairs={{0,1},{1,0},{2,3},{3,2},{4,5},{5,4},{6,7},{7,6},{8,9},{9,8},{10,11... | collective-permute-start | bytes 3145736 | tf_op jit(solution)/shard_map/ppermute | solution.py:253
  76.2 2.3 %collective-permute-done = bf16[4,64,2048]{2,1,0:T(8,128)(2,1)S(1)} collective-permute-done((bf16[4,64,2048]{2,1,0:T(8,128)(2,1)S(1)}, bf16[4,64,2048]{2,1,0:T(8,128)(2,1)S(1)}, u32[]{:S(2)}, u32[]{:S(2)}) %collective-permute-start) | collective-permute-done | bytes 1048608 | tf_op jit(solution)/shard_map/ppermute | solution.py:253
  79.8 4.1 %all-to-all-start.2 = ((bf16[4,64,2048]{2,1,0:T(8,128)(2,1)}), bf16[4,64,2048]{2,1,0:T(8,128)(2,1)S(1)}, u32[]{:S(2)}, u32[]{:S(2)}) async-start(bf16[4,64,2048]{2,1,0:T(8,128)(2,1)} %add_convert_fusion), calls=%async_computation.2 | async-start | bytes 2097152 | tf_op jit(solution)/shard_map/all_to_all | solution.py:24
  84.8 2.2 %collective-permute-start.2 = (bf16[64,1152]{1,0:T(8,128)(2,1)S(1)}, bf16[64,1152]{1,0:T(8,128)(2,1)S(1)}, u32[]{:S(2)}, u32[]{:S(2)}) collective-permute-start(bf16[64,1152]{1,0:T(8,128)(2,1)S(1)} %bitcast.17), channel_id=1, source_target_pairs={{16,0},{24,8},{0,16},{8,24},{17,1},{25,9},{1,17},{9,25},{18,2},{26... | collective-permute-start | bytes 442376 | tf_op jit(solution)/shard_map/ppermute | solution.py:20
  87.1 4.3 %collective-permute-start.3 = (bf16[64,1152]{1,0:T(8,128)(2,1)S(1)}, bf16[64,1152]{1,0:T(8,128)(2,1)S(1)}, u32[]{:S(2)}, u32[]{:S(2)}) collective-permute-start(bf16[64,1152]{1,0:T(8,128)(2,1)S(1)} %bitcast.18), channel_id=1, source_target_pairs={{8,0},{16,8},{24,16},{0,24},{9,1},{17,9},{25,17},{1,25},{10,2},{18... | collective-permute-start | bytes 442376 | tf_op jit(solution)/shard_map/ppermute | solution.py:20
  94.9 3.9 %collective-permute-done.4.refs_4_ = bf16[64,1152]{1,0:T(8,128)(2,1)S(1)} collective-permute-done((bf16[64,1152]{1,0:T(8,128)(2,1)S(1)}, bf16[64,1152]{1,0:T(8,128)(2,1)S(1)}, u32[]{:S(2)}, u32[]{:S(2)}) %collective-permute-start.4) | collective-permute-done | bytes 147488 | tf_op jit(solution)/shard_map/ppermute | solution.py:20
  99.4 16.1 %collective-permute-start.5 = (bf16[256,1152]{1,0:T(8,128)(2,1)S(1)}, bf16[256,1152]{1,0:T(8,128)(2,1)S(1)}, u32[]{:S(2)}, u32[]{:S(2)}) collective-permute-start(bf16[256,1152]{1,0:T(8,128)(2,1)S(1)} %shard_map.116.refs_3_), channel_id=1, source_target_pairs={{32,0},{64,32},{96,64},{128,96},{160,128},{192,160},{224,192},{256... | collective-permute-start | bytes 1769480 | tf_op jit(solution)/shard_map/ppermute | solution.py:20
  119.7 3.9 %all-to-all-start.3 = ((bf16[4,64,2048]{2,1,0:T(8,128)(2,1)}), bf16[4,64,2048]{2,1,0:T(8,128)(2,1)S(1)}, u32[]{:S(2)}, u32[]{:S(2)}) async-start(bf16[4,64,2048]{2,1,0:T(8,128)(2,1)} %get-tuple-element.13), calls=%async_computation.3 | async-start | bytes 2097152 | tf_op jit(solution)/shard_map/all_to_all | solution.py:24
  123.6 2.4 %collective-permute-done.5.refs_4_ = bf16[256,1152]{1,0:T(8,128)(2,1)S(1)} collective-permute-done((bf16[256,1152]{1,0:T(8,128)(2,1)S(1)}, bf16[256,1152]{1,0:T(8,128)(2,1)S(1)}, u32[]{:S(2)}, u32[]{:S(2)}) %collective-permute-start.5) | collective-permute-done | bytes 589856 | tf_op jit(solution)/shard_map/ppermute | solution.py:20
  126.0 5.3 %collective-permute-start.7 = (bf16[256,1152]{1,0:T(8,128)(2,1)S(1)}, bf16[256,1152]{1,0:T(8,128)(2,1)}, u32[]{:S(2)}, u32[]{:S(2)}) collective-permute-start(bf16[256,1152]{1,0:T(8,128)(2,1)S(1)} %collective-permute-done.5.refs_4_), channel_id=1, source_target_pairs={{32,0},{64,32},{96,64},{128,96},{160,128},{192,160},{224,192},{256... | collective-permute-start | bytes 1769480 | tf_op jit(solution)/shard_map/ppermute | solution.py:20
  135.3 6.3 %collective-permute-start.1 = (bf16[256,2048]{1,0:T(8,128)(2,1)S(1)}, bf16[256,2048]{1,0:T(8,128)(2,1)S(1)}, u32[]{:S(2)}, u32[]{:S(2)}) collective-permute-start(bf16[256,2048]{1,0:T(8,128)(2,1)S(1)} %bitcast.14), channel_id=1, source_target_pairs={{0,1},{1,0},{2,3},{3,2},{4,5},{5,4},{6,7},{7,6},{8,9},{9,8},{10,11... | collective-permute-start | bytes 3145736 | tf_op jit(solution)/shard_map/ppermute | solution.py:268
  141.6 4.9 %collective-permute-start.9 = (bf16[256,1152]{1,0:T(8,128)(2,1)}, bf16[256,1152]{1,0:T(8,128)(2,1)S(1)}, u32[]{:S(2)}, u32[]{:S(2)}) collective-permute-start(bf16[256,1152]{1,0:T(8,128)(2,1)} %collective-permute-done.7.refs_6_), channel_id=1, source_target_pairs={{32,0},{64,32},{96,64},{128,96},{160,128},{192,160},{224,192},{256... | collective-permute-start | bytes 1769480 | tf_op jit(solution)/shard_map/ppermute | solution.py:20
  148.5 7.3 %collective-permute-done.9.refs_8_ = bf16[256,1152]{1,0:T(8,128)(2,1)S(1)} collective-permute-done((bf16[256,1152]{1,0:T(8,128)(2,1)}, bf16[256,1152]{1,0:T(8,128)(2,1)S(1)}, u32[]{:S(2)}, u32[]{:S(2)}) %collective-permute-start.9) | collective-permute-done | bytes 589856 | tf_op jit(solution)/shard_map/ppermute | solution.py:20
  155.8 5.2 %collective-permute-start.11 = (bf16[128,1152]{1,0:T(8,128)(2,1)S(1)}, bf16[128,1152]{1,0:T(8,128)(2,1)S(1)}, u32[]{:S(2)}, u32[]{:S(2)}) collective-permute-start(bf16[128,1152]{1,0:T(8,128)(2,1)S(1)} %slice.8), channel_id=1, source_target_pairs={{32,0},{64,32},{96,64},{128,96},{160,128},{192,160},{224,192},{256... | collective-permute-start | bytes 884744 | tf_op jit(solution)/shard_map/ppermute | solution.py:20
  165.3 4.4 %collective-permute-done.12.refs_11_ = bf16[128,1152]{1,0:T(8,128)(2,1)S(1)} collective-permute-done((bf16[128,1152]{1,0:T(8,128)(2,1)S(1)}, bf16[128,1152]{1,0:T(8,128)(2,1)S(1)}, u32[]{:S(2)}, u32[]{:S(2)}) %collective-permute-start.12) | collective-permute-done | bytes 294944 | tf_op jit(solution)/shard_map/ppermute | solution.py:20
  170.4 6.9 %shard_map.117 = (bf16[256,2048]{1,0:T(8,128)(2,1)S(1)}, bf16[256,2048]{1,0:T(8,128)(2,1)S(1)}) custom-call(s32[3]{0:T(128)S(1)} %shard_map.111.refs_0_, bf16[256,2048]{1,0:T(8,128)(2,1)S(1)} %bitcast.15, bf16[256,2048]{1,0:T(8,128)(2,1)S(1)} %collective-permute-done.1.refs_2_, bf16[256,1152]{1,0:T(8,128)(2,1)} %copy-done.1, bf16[256,1152]{1,0:T(8,128)(2,1)} %copy-done.7, ...), custom_call_target="tpu_custom_call" | custom-call | tf_op jit(solution)/shard_map/pallas_call | solution.py:45
  177.4 8.0 %collective-permute-start.13 = (bf16[4,64,2048]{2,1,0:T(8,128)(2,1)S(1)}, bf16[4,64,2048]{2,1,0:T(8,128)(2,1)S(1)}, u32[]{:S(2)}, u32[]{:S(2)}) collective-permute-start(bf16[4,64,2048]{2,1,0:T(8,128)(2,1)S(1)} %bitcast.22), channel_id=1, source_target_pairs={{0,1},{1,0},{2,3},{3,2},{4,5},{5,4},{6,7},{7,6},{8,9},{9,8},{10,11... | collective-permute-start | bytes 3145736 | tf_op jit(solution)/shard_map/ppermute | solution.py:253
  185.4 2.3 %collective-permute-done.13 = bf16[4,64,2048]{2,1,0:T(8,128)(2,1)S(1)} collective-permute-done((bf16[4,64,2048]{2,1,0:T(8,128)(2,1)S(1)}, bf16[4,64,2048]{2,1,0:T(8,128)(2,1)S(1)}, u32[]{:S(2)}, u32[]{:S(2)}) %collective-permute-start.13) | collective-permute-done | bytes 1048608 | tf_op jit(solution)/shard_map/ppermute | solution.py:253
  188.0 16.8 %all_to_all.26.blocks = bf16[4,64,2048]{2,1,0:T(8,128)(2,1)S(1)} all-to-all(bf16[4,64,2048]{2,1,0:T(8,128)(2,1)S(1)} %fusion.3), channel_id=1, replica_groups=mesh['rep'=4,'zl'=8,'y'=4,'x'=4,'core'=2] {'x'}, dimensions={0} | all-to-all | bytes 2097152 | tf_op jit(solution)/shard_map/all_to_all | solution.py:24
  (55 shorter events, 29.5 us)
Async XLA Ops:
  37.3 23.5 %all-to-all-start.1 = ((bf16[32,64,512]{2,1,0:T(8,128)(2,1)}), bf16[32,64,512]{2,1,0:T(8,128)(2,1)S(1)}, u32[]{:S(2)}, u32[]{:S(2)}) async-start(bf16[32,64,512]{2,1,0:T(8,128)(2,1)} %bitcast.23), calls=%async_computation.1 | async-start | bytes 4194304 | tf_op jit(solution)/shard_map/all_to_all | solution.py:24
  45.3 15.5 %copy-start.3 = (f32[3,128]{1,0:T(4,128)S(1)}, f32[3,128]{1,0:T(4,128)}, u32[]{:S(2)}) copy-start(f32[3,128]{1,0:T(4,128)} %taps.1) | copy-start | bytes 4612
  65.9 12.6 %collective-permute-start = (bf16[4,64,2048]{2,1,0:T(8,128)(2,1)S(1)}, bf16[4,64,2048]{2,1,0:T(8,128)(2,1)S(1)}, u32[]{:S(2)}, u32[]{:S(2)}) collective-permute-start(bf16[4,64,2048]{2,1,0:T(8,128)(2,1)S(1)} %get-tuple-element.12), channel_id=1, source_target_pairs={{0,1},{1,0},{2,3},{3,2},{4,5},{5,4},{6,7},{7,6},{8,9},{9,8},{10,11... | collective-permute-start | bytes 3145736 | tf_op jit(solution)/shard_map/ppermute | solution.py:253
  79.8 38.5 %copy-start.2 = (f32[2048]{0:T(1024)S(1)}, f32[2048]{0:T(1024)}, u32[]{:S(2)}) copy-start(f32[2048]{0:T(1024)} %param.18) | copy-start | bytes 24580
  79.8 38.5 %all-to-all-start.2 = ((bf16[4,64,2048]{2,1,0:T(8,128)(2,1)}), bf16[4,64,2048]{2,1,0:T(8,128)(2,1)S(1)}, u32[]{:S(2)}, u32[]{:S(2)}) async-start(bf16[4,64,2048]{2,1,0:T(8,128)(2,1)} %add_convert_fusion), calls=%async_computation.2 | async-start | bytes 2097152 | tf_op jit(solution)/shard_map/all_to_all | solution.py:24
  84.8 8.5 %collective-permute-start.2 = (bf16[64,1152]{1,0:T(8,128)(2,1)S(1)}, bf16[64,1152]{1,0:T(8,128)(2,1)S(1)}, u32[]{:S(2)}, u32[]{:S(2)}) collective-permute-start(bf16[64,1152]{1,0:T(8,128)(2,1)S(1)} %bitcast.17), channel_id=1, source_target_pairs={{16,0},{24,8},{0,16},{8,24},{17,1},{25,9},{1,17},{9,25},{18,2},{26... | collective-permute-start | bytes 442376 | tf_op jit(solution)/shard_map/ppermute | solution.py:20
  87.1 7.8 %collective-permute-start.3 = (bf16[64,1152]{1,0:T(8,128)(2,1)S(1)}, bf16[64,1152]{1,0:T(8,128)(2,1)S(1)}, u32[]{:S(2)}, u32[]{:S(2)}) collective-permute-start(bf16[64,1152]{1,0:T(8,128)(2,1)S(1)} %bitcast.18), channel_id=1, source_target_pairs={{8,0},{16,8},{24,16},{0,24},{9,1},{17,9},{25,17},{1,25},{10,2},{18... | collective-permute-start | bytes 442376 | tf_op jit(solution)/shard_map/ppermute | solution.py:20
  91.4 7.4 %collective-permute-start.4 = (bf16[64,1152]{1,0:T(8,128)(2,1)S(1)}, bf16[64,1152]{1,0:T(8,128)(2,1)S(1)}, u32[]{:S(2)}, u32[]{:S(2)}) collective-permute-start(bf16[64,1152]{1,0:T(8,128)(2,1)S(1)} %bitcast.19), channel_id=1, source_target_pairs={{24,0},{0,8},{8,16},{16,24},{25,1},{1,9},{9,17},{17,25},{26,2},{2,... | collective-permute-start | bytes 442376 | tf_op jit(solution)/shard_map/ppermute | solution.py:20
  99.4 56.4 %copy-start.1 = (bf16[256,1152]{1,0:T(8,128)(2,1)}, bf16[256,1152]{1,0:T(8,128)(2,1)S(1)}, u32[]{:S(2)}) copy-start(bf16[256,1152]{1,0:T(8,128)(2,1)S(1)} %shard_map.116.refs_3_) | copy-start | bytes 1769476
  99.4 26.7 %collective-permute-start.5 = (bf16[256,1152]{1,0:T(8,128)(2,1)S(1)}, bf16[256,1152]{1,0:T(8,128)(2,1)S(1)}, u32[]{:S(2)}, u32[]{:S(2)}) collective-permute-start(bf16[256,1152]{1,0:T(8,128)(2,1)S(1)} %shard_map.116.refs_3_), channel_id=1, source_target_pairs={{32,0},{64,32},{96,64},{128,96},{160,128},{192,160},{224,192},{256... | collective-permute-start | bytes 1769480 | tf_op jit(solution)/shard_map/ppermute | solution.py:20
  115.4 15.9 %collective-permute-start.6 = (bf16[256,1152]{1,0:T(8,128)(2,1)S(1)}, bf16[256,1152]{1,0:T(8,128)(2,1)}, u32[]{:S(2)}, u32[]{:S(2)}) collective-permute-start(bf16[256,1152]{1,0:T(8,128)(2,1)S(1)} %shard_map.116.refs_3_), channel_id=1, source_target_pairs={{992,0},{0,32},{32,64},{64,96},{96,128},{128,160},{160,192},{192,2... | collective-permute-start | bytes 1769480 | tf_op jit(solution)/shard_map/ppermute | solution.py:20
  119.7 15.6 %all-to-all-start.3 = ((bf16[4,64,2048]{2,1,0:T(8,128)(2,1)}), bf16[4,64,2048]{2,1,0:T(8,128)(2,1)S(1)}, u32[]{:S(2)}, u32[]{:S(2)}) async-start(bf16[4,64,2048]{2,1,0:T(8,128)(2,1)} %get-tuple-element.13), calls=%async_computation.3 | async-start | bytes 2097152 | tf_op jit(solution)/shard_map/all_to_all | solution.py:24
  126.0 43.7 %copy-start.7 = (bf16[256,1152]{1,0:T(8,128)(2,1)}, bf16[256,1152]{1,0:T(8,128)(2,1)S(1)}, u32[]{:S(2)}) copy-start(bf16[256,1152]{1,0:T(8,128)(2,1)S(1)} %collective-permute-done.5.refs_4_) | copy-start | bytes 1769476
  126.0 15.5 %collective-permute-start.7 = (bf16[256,1152]{1,0:T(8,128)(2,1)S(1)}, bf16[256,1152]{1,0:T(8,128)(2,1)}, u32[]{:S(2)}, u32[]{:S(2)}) collective-permute-start(bf16[256,1152]{1,0:T(8,128)(2,1)S(1)} %collective-permute-done.5.refs_4_), channel_id=1, source_target_pairs={{32,0},{64,32},{96,64},{128,96},{160,128},{192,160},{224,192},{256... | collective-permute-start | bytes 1769480 | tf_op jit(solution)/shard_map/ppermute | solution.py:20
  131.4 15.2 %collective-permute-start.8 = (bf16[256,1152]{1,0:T(8,128)(2,1)}, bf16[256,1152]{1,0:T(8,128)(2,1)}, u32[]{:S(2)}, u32[]{:S(2)}) collective-permute-start(bf16[256,1152]{1,0:T(8,128)(2,1)} %collective-permute-done.6.refs_5_), channel_id=1, source_target_pairs={{992,0},{0,32},{32,64},{64,96},{96,128},{128,160},{160,192},{192,2... | collective-permute-start | bytes 1769480 | tf_op jit(solution)/shard_map/ppermute | solution.py:20
  135.3 34.4 %collective-permute-start.1 = (bf16[256,2048]{1,0:T(8,128)(2,1)S(1)}, bf16[256,2048]{1,0:T(8,128)(2,1)S(1)}, u32[]{:S(2)}, u32[]{:S(2)}) collective-permute-start(bf16[256,2048]{1,0:T(8,128)(2,1)S(1)} %bitcast.14), channel_id=1, source_target_pairs={{0,1},{1,0},{2,3},{3,2},{4,5},{5,4},{6,7},{7,6},{8,9},{9,8},{10,11... | collective-permute-start | bytes 3145736 | tf_op jit(solution)/shard_map/ppermute | solution.py:268
  141.6 14.1 %collective-permute-start.9 = (bf16[256,1152]{1,0:T(8,128)(2,1)}, bf16[256,1152]{1,0:T(8,128)(2,1)S(1)}, u32[]{:S(2)}, u32[]{:S(2)}) collective-permute-start(bf16[256,1152]{1,0:T(8,128)(2,1)} %collective-permute-done.7.refs_6_), channel_id=1, source_target_pairs={{32,0},{64,32},{96,64},{128,96},{160,128},{192,160},{224,192},{256... | collective-permute-start | bytes 1769480 | tf_op jit(solution)/shard_map/ppermute | solution.py:20
  146.5 14.5 %collective-permute-start.10 = (bf16[256,1152]{1,0:T(8,128)(2,1)}, bf16[256,1152]{1,0:T(8,128)(2,1)S(1)}, u32[]{:S(2)}, u32[]{:S(2)}) collective-permute-start(bf16[256,1152]{1,0:T(8,128)(2,1)} %collective-permute-done.8.refs_7_), channel_id=1, source_target_pairs={{992,0},{0,32},{32,64},{64,96},{96,128},{128,160},{160,192},{192,2... | collective-permute-start | bytes 1769480 | tf_op jit(solution)/shard_map/ppermute | solution.py:20
  155.7 14.0 %copy-start.5 = (bf16[256,1152]{1,0:T(8,128)(2,1)}, bf16[256,1152]{1,0:T(8,128)(2,1)S(1)}, u32[]{:S(2)}) copy-start(bf16[256,1152]{1,0:T(8,128)(2,1)S(1)} %collective-permute-done.9.refs_8_) | copy-start | bytes 1769476
  155.8 9.5 %collective-permute-start.11 = (bf16[128,1152]{1,0:T(8,128)(2,1)S(1)}, bf16[128,1152]{1,0:T(8,128)(2,1)S(1)}, u32[]{:S(2)}, u32[]{:S(2)}) collective-permute-start(bf16[128,1152]{1,0:T(8,128)(2,1)S(1)} %slice.8), channel_id=1, source_target_pairs={{32,0},{64,32},{96,64},{128,96},{160,128},{192,160},{224,192},{256... | collective-permute-start | bytes 884744 | tf_op jit(solution)/shard_map/ppermute | solution.py:20
  161.0 8.7 %copy-start.6 = (bf16[256,1152]{1,0:T(8,128)(2,1)}, bf16[256,1152]{1,0:T(8,128)(2,1)S(1)}, u32[]{:S(2)}) copy-start(bf16[256,1152]{1,0:T(8,128)(2,1)S(1)} %collective-permute-done.10.refs_9_) | copy-start | bytes 1769476
  161.0 8.7 %collective-permute-start.12 = (bf16[128,1152]{1,0:T(8,128)(2,1)S(1)}, bf16[128,1152]{1,0:T(8,128)(2,1)S(1)}, u32[]{:S(2)}, u32[]{:S(2)}) collective-permute-start(bf16[128,1152]{1,0:T(8,128)(2,1)S(1)} %slice.9), channel_id=1, source_target_pairs={{992,0},{0,32},{32,64},{64,96},{96,128},{128,160},{160,192},{192,2... | collective-permute-start | bytes 884744 | tf_op jit(solution)/shard_map/ppermute | solution.py:20
  165.3 4.5 %copy-start.8 = (bf16[128,1152]{1,0:T(8,128)(2,1)}, bf16[128,1152]{1,0:T(8,128)(2,1)S(1)}, u32[]{:S(2)}) copy-start(bf16[128,1152]{1,0:T(8,128)(2,1)S(1)} %collective-permute-done.11.refs_10_) | copy-start | bytes 884740
  177.4 10.2 %collective-permute-start.13 = (bf16[4,64,2048]{2,1,0:T(8,128)(2,1)S(1)}, bf16[4,64,2048]{2,1,0:T(8,128)(2,1)S(1)}, u32[]{:S(2)}, u32[]{:S(2)}) collective-permute-start(bf16[4,64,2048]{2,1,0:T(8,128)(2,1)S(1)} %bitcast.22), channel_id=1, source_target_pairs={{0,1},{1,0},{2,3},{3,2},{4,5},{5,4},{6,7},{7,6},{8,9},{9,8},{10,11... | collective-permute-start | bytes 3145736 | tf_op jit(solution)/shard_map/ppermute | solution.py:253
  (4 other events, 9.0 us)

commit v7 on v6

--- a/solution.py
+++ b/solution.py
@@ -144,32 +144,32 @@
     out[...] = total.astype(jnp.bfloat16)
 
 
-def ffn_kernel(places, n_ff, pos, acts, acts_other, *refs):
+def ffn_kernel(places, n_late, n_ff, pos, acts, acts_other, *refs):
     count = len(places)
     chunks, (out, out_other, weights, values, sems) = refs[:count], refs[count:]
     half = acts.shape[0]
     depth = acts.shape[1] // Z_LO
     step = weights.shape[1] // 3
     fetches, spans = [], []
-    at = 0
+    at = middle = 0
     for k, ((d, row), chunk) in enumerate(zip(places, chunks)):
         rows = chunk.shape[0]
-        fetches.append(pltpu.make_async_copy(chunk, weights.at[at : at + rows], sems.at[k]))
-        fetches[-1].start()
+        if k >= n_late:
+            fetches.append(pltpu.make_async_copy(chunk, weights.at[at : at + rows], sems.at[k - n_late]))
+            fetches[-1].start()
         z = lax.rem(pos[0] + (d + Z_LO), Z_LO)
         spans.append((at, rows, pl.ds(pl.multiple_of(z * depth + row, rows), rows)))
         at += rows
-    for first, rows, columns in spans:
+        if k < n_late:
+            middle = at
+    for k, (first, rows, columns) in enumerate(spans):
+        if k < n_late:
+            weights[first : first + rows, :] = chunks[k][...]
         values[:half, first : first + rows] = acts[:, columns]
         values[half:, first : first + rows] = acts_other[:, columns]
-    middle = at // 2
-    for fetch, (first, _, _) in zip(fetches, spans):
-        if first < middle:
-            fetch.wait()
     both = dot(values[:, :middle], weights[:middle, : 2 * step])
-    for fetch, (first, _, _) in zip(fetches, spans):
-        if first >= middle:
-            fetch.wait()
+    for fetch in fetches:
+        fetch.wait()
     both += dot(values[:, middle:], weights[middle:, : 2 * step])
     hidden = (jax.nn.silu(both[:, :n_ff]) * both[:, step : step + n_ff]).astype(jnp.bfloat16)
     for first, rows, columns in spans:
@@ -267,15 +267,19 @@
     acts = exchange(sent, "x").reshape(half_rows, feats)
     acts_other = lax.ppermute(acts, "core", SWAP)
 
+    n_early = len(chunks) - 4
+    order = [*range(n_early, len(chunks)), *range(n_early)]
+
     def ffn_body(*refs):
-        ffn_kernel(ffn_places, n_ff, *refs)
+        ffn_kernel([ffn_places[k] for k in order], 4, n_ff, *refs)
 
     room = [
         pltpu.VMEM((feats, width), bf),
         pltpu.VMEM((count, feats), bf),
-        pltpu.SemaphoreType.DMA((len(chunks),)),
+        pltpu.SemaphoreType.DMA((n_early,)),
     ]
-    pair = call(ffn_body, (pltpu.VMEM((half_rows, feats), bf),) * 2, pos, (acts, acts_other), 24, room, chunks)
+    near, far = (acts, acts_other, *chunks[n_early:]), chunks[:n_early]
+    pair = call(ffn_body, (pltpu.VMEM((half_rows, feats), bf),) * 2, pos, near, 14, room, far)
     blocks = over_tp(*(part.reshape(halves) for part in pair))
     return call(last_kernel, (jax.ShapeDtypeStruct((own_rows, feats), bf),), None, (blocks, stream), 8)[0]
 

time: 207 us -> 206 us (level)
  no operation moved by 1% of the time
where the time goes in v7:
time: 206 us; the launch traced here: 205 us
  starting transfers between devices  84.9 us (41%)
  blocking collectives  51.9 us (25%)
  waiting for transfers between devices  39.8 us (19%)
  Pallas kernels  18.3 us (9%)
  other arithmetic  6.57 us (3%)
  local copies, waits for them, and re-layouts  2.68 us (1%)
    all_to_all x2, blocking collectives, exchange(): return lax.all_to_all(blocks, axis, 0, 0, tiled=True)  51.9 us
    ppermute x11, starting transfers between devices, shift(): lax.ppermute(value, axis, [((k + distance) % size, k) for k in range(size)])  47.6 us
    ppermute x11, waiting for transfers between devices, shift(): lax.ppermute(value, axis, [((k + distance) % size, k) for k in range(size)])  19.6 us
    ppermute x2, starting transfers between devices, over_tp(): got = lax.ppermute(other, 'core', SWAP)  18.3 us
    all_to_all x3, waiting for transfers between devices, exchange(): return lax.all_to_all(blocks, axis, 0, 0, tiled=True)  15.7 us
    all_to_all x3, starting transfers between devices, exchange(): return lax.all_to_all(blocks, axis, 0, 0, tiled=True)  12.8 us
    pallas_call x5, Pallas kernels, call(): pl.pallas_call(kernel, out_shape=outs, in_specs=specs, out_specs=(VMEM,)...  12.7 us
    ppermute x1, starting transfers between devices, local(): acts_other = lax.ppermute(acts, 'core', SWAP)  6.25 us
  transfers between devices with their start and end apart: 17, of which 9 were waited for; matrix products, arithmetic and copies ran while one was open for 2% of the time, Pallas kernels for 3%

profile of v7, /device:TPU:1, one launch (start us, length us, event | category | flops | bytes accessed | tf_op | source)
XLA Modules:
  0.0 204.6 jit_solution(13678779072227826575)
XLA Ops:
  0.8 35.1 %all_to_all.25.block = bf16[8,64,512]{2,1,0:T(8,128)(2,1)S(1)} all-to-all(bf16[8,64,512]{2,1,0:T(8,128)(2,1)S(1)} %broadcast_in_dim.2), channel_id=1, replica_groups=mesh['rep'=4,'zl'=8,'y'=4,'x'=4,'core'=2] {'zl'}, dimensions={0} | all-to-all | bytes 1048576 | tf_op jit(solution)/shard_map/all_to_all | solution.py:24
  37.3 4.7 %all-to-all-start.1 = ((bf16[32,64,512]{2,1,0:T(8,128)(2,1)}), bf16[32,64,512]{2,1,0:T(8,128)(2,1)S(1)}, u32[]{:S(2)}, u32[]{:S(2)}) async-start(bf16[32,64,512]{2,1,0:T(8,128)(2,1)} %bitcast.23), calls=%async_computation.1 | async-start | bytes 4194304 | tf_op jit(solution)/shard_map/all_to_all | solution.py:24
  43.2 2.1 %fusion = f32[512]{0:T(512)S(1)} fusion(bf16[512,2048]{1,0:T(8,128)(2,1)} %param.11), kind=kLoop, calls=%fused_computation.2 | loop fusion | flops 3145216 | bytes 2099200 | tf_op jit(solution)/shard_map/reduce_sum | solution.py:28
  47.1 13.7 %all-to-all-done.1 = bf16[32,64,512]{2,1,0:T(8,128)(2,1)S(1)} async-done(((bf16[32,64,512]{2,1,0:T(8,128)(2,1)}), bf16[32,64,512]{2,1,0:T(8,128)(2,1)S(1)}, u32[]{:S(2)}, u32[]{:S(2)}) %all-to-all-start.1) | async-done | bytes 2097184 | tf_op jit(solution)/shard_map/all_to_all | solution.py:24
  62.4 3.4 %shard_map.113 = (bf16[4,64,2048]{2,1,0:T(8,128)(2,1)S(1)}, bf16[4,64,2048]{2,1,0:T(8,128)(2,1)S(1)}) custom-call(s32[3]{0:T(128)S(1)} %shard_map.109.pos, bf16[512,2048]{1,0:T(8,128)(2,1)S(1)} %copy-done, f32[3,128]{1,0:T(4,128)S(1)} %copy-done.3, bf16[4,8,64,512]{3,2,1,0:T(8,128)(2,1)S(1)} %bitcast.13), custom_call_target="tpu_custom_call" | custom-call | tf_op jit(solution)/shard_map/pallas_call | solution.py:45
  65.8 10.3 %collective-permute-start = (bf16[4,64,2048]{2,1,0:T(8,128)(2,1)S(1)}, bf16[4,64,2048]{2,1,0:T(8,128)(2,1)S(1)}, u32[]{:S(2)}, u32[]{:S(2)}) collective-permute-start(bf16[4,64,2048]{2,1,0:T(8,128)(2,1)S(1)} %get-tuple-element.12), channel_id=1, source_target_pairs={{0,1},{1,0},{2,3},{3,2},{4,5},{5,4},{6,7},{7,6},{8,9},{9,8},{10,11... | collective-permute-start | bytes 3145736 | tf_op jit(solution)/shard_map/ppermute | solution.py:253
  76.2 2.3 %collective-permute-done = bf16[4,64,2048]{2,1,0:T(8,128)(2,1)S(1)} collective-permute-done((bf16[4,64,2048]{2,1,0:T(8,128)(2,1)S(1)}, bf16[4,64,2048]{2,1,0:T(8,128)(2,1)S(1)}, u32[]{:S(2)}, u32[]{:S(2)}) %collective-permute-start) | collective-permute-done | bytes 1048608 | tf_op jit(solution)/shard_map/ppermute | solution.py:253
  79.8 4.2 %all-to-all-start.2 = ((bf16[4,64,2048]{2,1,0:T(8,128)(2,1)}), bf16[4,64,2048]{2,1,0:T(8,128)(2,1)S(1)}, u32[]{:S(2)}, u32[]{:S(2)}) async-start(bf16[4,64,2048]{2,1,0:T(8,128)(2,1)} %add_convert_fusion), calls=%async_computation.2 | async-start | bytes 2097152 | tf_op jit(solution)/shard_map/all_to_all | solution.py:24
  84.9 2.2 %collective-permute-start.2 = (bf16[64,1152]{1,0:T(8,128)(2,1)S(1)}, bf16[64,1152]{1,0:T(8,128)(2,1)S(1)}, u32[]{:S(2)}, u32[]{:S(2)}) collective-permute-start(bf16[64,1152]{1,0:T(8,128)(2,1)S(1)} %bitcast.17), channel_id=1, source_target_pairs={{16,0},{24,8},{0,16},{8,24},{17,1},{25,9},{1,17},{9,25},{18,2},{26... | collective-permute-start | bytes 442376 | tf_op jit(solution)/shard_map/ppermute | solution.py:20
  87.1 4.3 %collective-permute-start.3 = (bf16[64,1152]{1,0:T(8,128)(2,1)S(1)}, bf16[64,1152]{1,0:T(8,128)(2,1)S(1)}, u32[]{:S(2)}, u32[]{:S(2)}) collective-permute-start(bf16[64,1152]{1,0:T(8,128)(2,1)S(1)} %bitcast.18), channel_id=1, source_target_pairs={{8,0},{16,8},{24,16},{0,24},{9,1},{17,9},{25,17},{1,25},{10,2},{18... | collective-permute-start | bytes 442376 | tf_op jit(solution)/shard_map/ppermute | solution.py:20
  94.9 3.9 %collective-permute-done.4.refs_4_ = bf16[64,1152]{1,0:T(8,128)(2,1)S(1)} collective-permute-done((bf16[64,1152]{1,0:T(8,128)(2,1)S(1)}, bf16[64,1152]{1,0:T(8,128)(2,1)S(1)}, u32[]{:S(2)}, u32[]{:S(2)}) %collective-permute-start.4) | collective-permute-done | bytes 147488 | tf_op jit(solution)/shard_map/ppermute | solution.py:20
  99.4 16.1 %collective-permute-start.5 = (bf16[256,1152]{1,0:T(8,128)(2,1)S(1)}, bf16[256,1152]{1,0:T(8,128)(2,1)S(1)}, u32[]{:S(2)}, u32[]{:S(2)}) collective-permute-start(bf16[256,1152]{1,0:T(8,128)(2,1)S(1)} %shard_map.116.refs_7_), channel_id=1, source_target_pairs={{32,0},{64,32},{96,64},{128,96},{160,128},{192,160},{224,192},{256... | collective-permute-start | bytes 1769480 | tf_op jit(solution)/shard_map/ppermute | solution.py:20
  119.7 3.9 %all-to-all-start.3 = ((bf16[4,64,2048]{2,1,0:T(8,128)(2,1)}), bf16[4,64,2048]{2,1,0:T(8,128)(2,1)S(1)}, u32[]{:S(2)}, u32[]{:S(2)}) async-start(bf16[4,64,2048]{2,1,0:T(8,128)(2,1)} %get-tuple-element.13), calls=%async_computation.3 | async-start | bytes 2097152 | tf_op jit(solution)/shard_map/all_to_all | solution.py:24
  123.6 2.4 %collective-permute-done.5.refs_8_ = bf16[256,1152]{1,0:T(8,128)(2,1)S(1)} collective-permute-done((bf16[256,1152]{1,0:T(8,128)(2,1)S(1)}, bf16[256,1152]{1,0:T(8,128)(2,1)S(1)}, u32[]{:S(2)}, u32[]{:S(2)}) %collective-permute-start.5) | collective-permute-done | bytes 589856 | tf_op jit(solution)/shard_map/ppermute | solution.py:20
  126.1 5.3 %collective-permute-start.6 = (bf16[256,1152]{1,0:T(8,128)(2,1)S(1)}, bf16[256,1152]{1,0:T(8,128)(2,1)}, u32[]{:S(2)}, u32[]{:S(2)}) collective-permute-start(bf16[256,1152]{1,0:T(8,128)(2,1)S(1)} %collective-permute-done.5.refs_8_), channel_id=1, source_target_pairs={{32,0},{64,32},{96,64},{128,96},{160,128},{192,160},{224,192},{256... | collective-permute-start | bytes 1769480 | tf_op jit(solution)/shard_map/ppermute | solution.py:20
  135.3 6.3 %collective-permute-start.1 = (bf16[256,2048]{1,0:T(8,128)(2,1)S(1)}, bf16[256,2048]{1,0:T(8,128)(2,1)S(1)}, u32[]{:S(2)}, u32[]{:S(2)}) collective-permute-start(bf16[256,2048]{1,0:T(8,128)(2,1)S(1)} %bitcast.14), channel_id=1, source_target_pairs={{0,1},{1,0},{2,3},{3,2},{4,5},{5,4},{6,7},{7,6},{8,9},{9,8},{10,11... | collective-permute-start | bytes 3145736 | tf_op jit(solution)/shard_map/ppermute | solution.py:268
  141.6 4.9 %collective-permute-start.7 = (bf16[256,1152]{1,0:T(8,128)(2,1)}, bf16[256,1152]{1,0:T(8,128)(2,1)S(1)}, u32[]{:S(2)}, u32[]{:S(2)}) collective-permute-start(bf16[256,1152]{1,0:T(8,128)(2,1)} %collective-permute-done.6.refs_10_), channel_id=1, source_target_pairs={{32,0},{64,32},{96,64},{128,96},{160,128},{192,160},{224,192},{256... | collective-permute-start | bytes 1769480 | tf_op jit(solution)/shard_map/ppermute | solution.py:20
  148.5 7.3 %collective-permute-done.7.refs_3_ = bf16[256,1152]{1,0:T(8,128)(2,1)S(1)} collective-permute-done((bf16[256,1152]{1,0:T(8,128)(2,1)}, bf16[256,1152]{1,0:T(8,128)(2,1)S(1)}, u32[]{:S(2)}, u32[]{:S(2)}) %collective-permute-start.7) | collective-permute-done | bytes 589856 | tf_op jit(solution)/shard_map/ppermute | solution.py:20
  155.8 5.2 %collective-permute-start.11 = (bf16[128,1152]{1,0:T(8,128)(2,1)S(1)}, bf16[128,1152]{1,0:T(8,128)(2,1)S(1)}, u32[]{:S(2)}, u32[]{:S(2)}) collective-permute-start(bf16[128,1152]{1,0:T(8,128)(2,1)S(1)} %slice.8), channel_id=1, source_target_pairs={{32,0},{64,32},{96,64},{128,96},{160,128},{192,160},{224,192},{256... | collective-permute-start | bytes 884744 | tf_op jit(solution)/shard_map/ppermute | solution.py:20
  165.3 4.4 %collective-permute-done.12.refs_6_ = bf16[128,1152]{1,0:T(8,128)(2,1)S(1)} collective-permute-done((bf16[128,1152]{1,0:T(8,128)(2,1)S(1)}, bf16[128,1152]{1,0:T(8,128)(2,1)S(1)}, u32[]{:S(2)}, u32[]{:S(2)}) %collective-permute-start.12) | collective-permute-done | bytes 294944 | tf_op jit(solution)/shard_map/ppermute | solution.py:20
  169.7 6.5 %shard_map.117 = (bf16[256,2048]{1,0:T(8,128)(2,1)S(1)}, bf16[256,2048]{1,0:T(8,128)(2,1)S(1)}) custom-call(s32[3]{0:T(128)S(1)} %shard_map.111.refs_0_, bf16[256,2048]{1,0:T(8,128)(2,1)S(1)} %bitcast.15, bf16[256,2048]{1,0:T(8,128)(2,1)S(1)} %collective-permute-done.1.refs_2_, bf16[256,1152]{1,0:T(8,128)(2,1)S(1)} %collective-permute-done.7.refs_3_, ...), custom_call_target="tpu_custom_call" | custom-call | tf_op jit(solution)/shard_map/pallas_call | solution.py:45
  176.3 8.0 %collective-permute-start.13 = (bf16[4,64,2048]{2,1,0:T(8,128)(2,1)S(1)}, bf16[4,64,2048]{2,1,0:T(8,128)(2,1)S(1)}, u32[]{:S(2)}, u32[]{:S(2)}) collective-permute-start(bf16[4,64,2048]{2,1,0:T(8,128)(2,1)S(1)} %bitcast.22), channel_id=1, source_target_pairs={{0,1},{1,0},{2,3},{3,2},{4,5},{5,4},{6,7},{7,6},{8,9},{9,8},{10,11... | collective-permute-start | bytes 3145736 | tf_op jit(solution)/shard_map/ppermute | solution.py:253
  184.3 2.3 %collective-permute-done.13 = bf16[4,64,2048]{2,1,0:T(8,128)(2,1)S(1)} collective-permute-done((bf16[4,64,2048]{2,1,0:T(8,128)(2,1)S(1)}, bf16[4,64,2048]{2,1,0:T(8,128)(2,1)S(1)}, u32[]{:S(2)}, u32[]{:S(2)}) %collective-permute-start.13) | collective-permute-done | bytes 1048608 | tf_op jit(solution)/shard_map/ppermute | solution.py:253
  186.9 16.8 %all_to_all.26.blocks = bf16[4,64,2048]{2,1,0:T(8,128)(2,1)S(1)} all-to-all(bf16[4,64,2048]{2,1,0:T(8,128)(2,1)S(1)} %fusion.3), channel_id=1, replica_groups=mesh['rep'=4,'zl'=8,'y'=4,'x'=4,'core'=2] {'x'}, dimensions={0} | all-to-all | bytes 2097152 | tf_op jit(solution)/shard_map/all_to_all | solution.py:24
  (47 shorter events, 28.8 us)
Async XLA Ops:
  37.3 23.5 %all-to-all-start.1 = ((bf16[32,64,512]{2,1,0:T(8,128)(2,1)}), bf16[32,64,512]{2,1,0:T(8,128)(2,1)S(1)}, u32[]{:S(2)}, u32[]{:S(2)}) async-start(bf16[32,64,512]{2,1,0:T(8,128)(2,1)} %bitcast.23), calls=%async_computation.1 | async-start | bytes 4194304 | tf_op jit(solution)/shard_map/all_to_all | solution.py:24
  42.0 3.3 %copy-start.6 = (f32[2048]{0:T(1024)S(1)}, f32[2048]{0:T(1024)}, u32[]{:S(2)}) copy-start(f32[2048]{0:T(1024)} %param.12) | copy-start | bytes 24580
  42.0 3.3 %copy-start.4 = (bf16[512,2048]{1,0:T(8,128)(2,1)S(1)}, bf16[512,2048]{1,0:T(8,128)(2,1)}, u32[]{:S(2)}) copy-start(bf16[512,2048]{1,0:T(8,128)(2,1)} %param.11) | copy-start | bytes 6291460
  45.3 15.5 %copy-start.3 = (f32[3,128]{1,0:T(4,128)S(1)}, f32[3,128]{1,0:T(4,128)}, u32[]{:S(2)}) copy-start(f32[3,128]{1,0:T(4,128)} %taps.1) | copy-start | bytes 4612
  60.8 1.6 copy-start
  65.8 12.6 %collective-permute-start = (bf16[4,64,2048]{2,1,0:T(8,128)(2,1)S(1)}, bf16[4,64,2048]{2,1,0:T(8,128)(2,1)S(1)}, u32[]{:S(2)}, u32[]{:S(2)}) collective-permute-start(bf16[4,64,2048]{2,1,0:T(8,128)(2,1)S(1)} %get-tuple-element.12), channel_id=1, source_target_pairs={{0,1},{1,0},{2,3},{3,2},{4,5},{5,4},{6,7},{7,6},{8,9},{9,8},{10,11... | collective-permute-start | bytes 3145736 | tf_op jit(solution)/shard_map/ppermute | solution.py:253
  79.8 38.5 %copy-start.2 = (f32[2048]{0:T(1024)S(1)}, f32[2048]{0:T(1024)}, u32[]{:S(2)}) copy-start(f32[2048]{0:T(1024)} %param.18) | copy-start | bytes 24580
  79.8 38.5 %all-to-all-start.2 = ((bf16[4,64,2048]{2,1,0:T(8,128)(2,1)}), bf16[4,64,2048]{2,1,0:T(8,128)(2,1)S(1)}, u32[]{:S(2)}, u32[]{:S(2)}) async-start(bf16[4,64,2048]{2,1,0:T(8,128)(2,1)} %add_convert_fusion), calls=%async_computation.2 | async-start | bytes 2097152 | tf_op jit(solution)/shard_map/all_to_all | solution.py:24
  84.9 8.4 %collective-permute-start.2 = (bf16[64,1152]{1,0:T(8,128)(2,1)S(1)}, bf16[64,1152]{1,0:T(8,128)(2,1)S(1)}, u32[]{:S(2)}, u32[]{:S(2)}) collective-permute-start(bf16[64,1152]{1,0:T(8,128)(2,1)S(1)} %bitcast.17), channel_id=1, source_target_pairs={{16,0},{24,8},{0,16},{8,24},{17,1},{25,9},{1,17},{9,25},{18,2},{26... | collective-permute-start | bytes 442376 | tf_op jit(solution)/shard_map/ppermute | solution.py:20
  87.1 7.8 %collective-permute-start.3 = (bf16[64,1152]{1,0:T(8,128)(2,1)S(1)}, bf16[64,1152]{1,0:T(8,128)(2,1)S(1)}, u32[]{:S(2)}, u32[]{:S(2)}) collective-permute-start(bf16[64,1152]{1,0:T(8,128)(2,1)S(1)} %bitcast.18), channel_id=1, source_target_pairs={{8,0},{16,8},{24,16},{0,24},{9,1},{17,9},{25,17},{1,25},{10,2},{18... | collective-permute-start | bytes 442376 | tf_op jit(solution)/shard_map/ppermute | solution.py:20
  91.4 7.4 %collective-permute-start.4 = (bf16[64,1152]{1,0:T(8,128)(2,1)S(1)}, bf16[64,1152]{1,0:T(8,128)(2,1)S(1)}, u32[]{:S(2)}, u32[]{:S(2)}) collective-permute-start(bf16[64,1152]{1,0:T(8,128)(2,1)S(1)} %bitcast.19), channel_id=1, source_target_pairs={{24,0},{0,8},{8,16},{16,24},{25,1},{1,9},{9,17},{17,25},{26,2},{2,... | collective-permute-start | bytes 442376 | tf_op jit(solution)/shard_map/ppermute | solution.py:20
  99.4 56.4 %copy-start.1 = (bf16[256,1152]{1,0:T(8,128)(2,1)}, bf16[256,1152]{1,0:T(8,128)(2,1)S(1)}, u32[]{:S(2)}) copy-start(bf16[256,1152]{1,0:T(8,128)(2,1)S(1)} %shard_map.116.refs_7_) | copy-start | bytes 1769476
  99.4 26.7 %collective-permute-start.5 = (bf16[256,1152]{1,0:T(8,128)(2,1)S(1)}, bf16[256,1152]{1,0:T(8,128)(2,1)S(1)}, u32[]{:S(2)}, u32[]{:S(2)}) collective-permute-start(bf16[256,1152]{1,0:T(8,128)(2,1)S(1)} %shard_map.116.refs_7_), channel_id=1, source_target_pairs={{32,0},{64,32},{96,64},{128,96},{160,128},{192,160},{224,192},{256... | collective-permute-start | bytes 1769480 | tf_op jit(solution)/shard_map/ppermute | solution.py:20
  115.5 15.9 %collective-permute-start.8 = (bf16[256,1152]{1,0:T(8,128)(2,1)S(1)}, bf16[256,1152]{1,0:T(8,128)(2,1)}, u32[]{:S(2)}, u32[]{:S(2)}) collective-permute-start(bf16[256,1152]{1,0:T(8,128)(2,1)S(1)} %shard_map.116.refs_7_), channel_id=1, source_target_pairs={{992,0},{0,32},{32,64},{64,96},{96,128},{128,160},{160,192},{192,2... | collective-permute-start | bytes 1769480 | tf_op jit(solution)/shard_map/ppermute | solution.py:20
  119.7 15.6 %all-to-all-start.3 = ((bf16[4,64,2048]{2,1,0:T(8,128)(2,1)}), bf16[4,64,2048]{2,1,0:T(8,128)(2,1)S(1)}, u32[]{:S(2)}, u32[]{:S(2)}) async-start(bf16[4,64,2048]{2,1,0:T(8,128)(2,1)} %get-tuple-element.13), calls=%async_computation.3 | async-start | bytes 2097152 | tf_op jit(solution)/shard_map/all_to_all | solution.py:24
  126.1 43.7 %copy-start.5 = (bf16[256,1152]{1,0:T(8,128)(2,1)}, bf16[256,1152]{1,0:T(8,128)(2,1)S(1)}, u32[]{:S(2)}) copy-start(bf16[256,1152]{1,0:T(8,128)(2,1)S(1)} %collective-permute-done.5.refs_8_) | copy-start | bytes 1769476
  126.1 15.5 %collective-permute-start.6 = (bf16[256,1152]{1,0:T(8,128)(2,1)S(1)}, bf16[256,1152]{1,0:T(8,128)(2,1)}, u32[]{:S(2)}, u32[]{:S(2)}) collective-permute-start(bf16[256,1152]{1,0:T(8,128)(2,1)S(1)} %collective-permute-done.5.refs_8_), channel_id=1, source_target_pairs={{32,0},{64,32},{96,64},{128,96},{160,128},{192,160},{224,192},{256... | collective-permute-start | bytes 1769480 | tf_op jit(solution)/shard_map/ppermute | solution.py:20
  131.4 15.2 %collective-permute-start.9 = (bf16[256,1152]{1,0:T(8,128)(2,1)}, bf16[256,1152]{1,0:T(8,128)(2,1)}, u32[]{:S(2)}, u32[]{:S(2)}) collective-permute-start(bf16[256,1152]{1,0:T(8,128)(2,1)} %collective-permute-done.8.refs_9_), channel_id=1, source_target_pairs={{992,0},{0,32},{32,64},{64,96},{96,128},{128,160},{160,192},{192,2... | collective-permute-start | bytes 1769480 | tf_op jit(solution)/shard_map/ppermute | solution.py:20
  135.3 34.4 %collective-permute-start.1 = (bf16[256,2048]{1,0:T(8,128)(2,1)S(1)}, bf16[256,2048]{1,0:T(8,128)(2,1)S(1)}, u32[]{:S(2)}, u32[]{:S(2)}) collective-permute-start(bf16[256,2048]{1,0:T(8,128)(2,1)S(1)} %bitcast.14), channel_id=1, source_target_pairs={{0,1},{1,0},{2,3},{3,2},{4,5},{5,4},{6,7},{7,6},{8,9},{9,8},{10,11... | collective-permute-start | bytes 3145736 | tf_op jit(solution)/shard_map/ppermute | solution.py:268
  141.6 14.1 %collective-permute-start.7 = (bf16[256,1152]{1,0:T(8,128)(2,1)}, bf16[256,1152]{1,0:T(8,128)(2,1)S(1)}, u32[]{:S(2)}, u32[]{:S(2)}) collective-permute-start(bf16[256,1152]{1,0:T(8,128)(2,1)} %collective-permute-done.6.refs_10_), channel_id=1, source_target_pairs={{32,0},{64,32},{96,64},{128,96},{160,128},{192,160},{224,192},{256... | collective-permute-start | bytes 1769480 | tf_op jit(solution)/shard_map/ppermute | solution.py:20
  146.5 14.5 %collective-permute-start.10 = (bf16[256,1152]{1,0:T(8,128)(2,1)}, bf16[256,1152]{1,0:T(8,128)(2,1)S(1)}, u32[]{:S(2)}, u32[]{:S(2)}) collective-permute-start(bf16[256,1152]{1,0:T(8,128)(2,1)} %collective-permute-done.9.refs_11_), channel_id=1, source_target_pairs={{992,0},{0,32},{32,64},{64,96},{96,128},{128,160},{160,192},{192,2... | collective-permute-start | bytes 1769480 | tf_op jit(solution)/shard_map/ppermute | solution.py:20
  155.8 9.5 %collective-permute-start.11 = (bf16[128,1152]{1,0:T(8,128)(2,1)S(1)}, bf16[128,1152]{1,0:T(8,128)(2,1)S(1)}, u32[]{:S(2)}, u32[]{:S(2)}) collective-permute-start(bf16[128,1152]{1,0:T(8,128)(2,1)S(1)} %slice.8), channel_id=1, source_target_pairs={{32,0},{64,32},{96,64},{128,96},{160,128},{192,160},{224,192},{256... | collective-permute-start | bytes 884744 | tf_op jit(solution)/shard_map/ppermute | solution.py:20
  161.0 8.7 %collective-permute-start.12 = (bf16[128,1152]{1,0:T(8,128)(2,1)S(1)}, bf16[128,1152]{1,0:T(8,128)(2,1)S(1)}, u32[]{:S(2)}, u32[]{:S(2)}) collective-permute-start(bf16[128,1152]{1,0:T(8,128)(2,1)S(1)} %slice.9), channel_id=1, source_target_pairs={{992,0},{0,32},{32,64},{64,96},{96,128},{128,160},{160,192},{192,2... | collective-permute-start | bytes 884744 | tf_op jit(solution)/shard_map/ppermute | solution.py:20
  176.3 10.3 %collective-permute-start.13 = (bf16[4,64,2048]{2,1,0:T(8,128)(2,1)S(1)}, bf16[4,64,2048]{2,1,0:T(8,128)(2,1)S(1)}, u32[]{:S(2)}, u32[]{:S(2)}) collective-permute-start(bf16[4,64,2048]{2,1,0:T(8,128)(2,1)S(1)} %bitcast.22), channel_id=1, source_target_pairs={{0,1},{1,0},{2,3},{3,2},{4,5},{5,4},{6,7},{7,6},{8,9},{9,8},{10,11... | collective-permute-start | bytes 3145736 | tf_op jit(solution)/shard_map/ppermute | solution.py:253
